TPU v7x, 512 devices: a whole 4x4x16 slice. The times are simulated.
512 devices in a mesh: ep: 32 (over z, core), tp: 16 (over y, x).
Axes of the slice: x: 4, y: 4, z: 16, core: 2. Of those that a mesh axis runs over, the one named last changes fastest.
Arguments:
- query_in: bfloat16 [1024, 32768], P('tp', 'ep'), may hold values from -6 to 6
- key_in: bfloat16 [1024, 32768], P('tp', 'ep'), may hold values from -10 to 10
- value_in: bfloat16 [1024, 32768], P('tp', 'ep'), may hold values from -6 to 6
- erase_pre: bfloat16 [1024, 32768], P('tp', 'ep'), may hold values from -8 to 5
- decay_pre: bfloat16 [1024, 32768], P('tp', 'ep'), may hold values from -30 to 4.5
- mix_gain: float32 [1024], P('tp'), may hold values from 0.1 to 1.9
- expert_in: bfloat16 [8192, 2048], P('ep'), may hold values from -6 to 6
- expert_gain: float32 [2048], replicated, may hold values from 0.1 to 1.9
- routes: int32 [8192, 2], P('ep'), may hold values from 0 to 31, all different within a row; in each aligned block of 256 rows (0 to 255, 256 to 511, ...) at most 24 rows name the same one
- route_weight: float32 [8192, 2], P('ep'), may hold values from 0.1 to 1
- gate_weight: bfloat16 [32, 2048, 3584], P('ep', None, 'tp'), may hold values from -0.125 to 0.125
- up_weight: bfloat16 [32, 2048, 3584], P('ep', None, 'tp'), may hold values from -0.125 to 0.125
- down_weight: bfloat16 [32, 3584, 2048], P('ep', 'tp'), may hold values from -0.09375 to 0.09375
Outputs:
- mixer_out: bfloat16 [1024, 32768], P('tp', 'ep')
- expert_out: bfloat16 [8192, 2048], P('ep', 'tp')
Inputs may be any that keep to these rules, and one draw needn't show every extreme that they name: `routes`: A row's 2 experts differ. Within the 256 rows of one index of ep, every expert is named at most 24 times; in some of these aligned blocks one expert is named exactly 24 times.
All inputs are finite; a program needn't handle non-finite values.
Results may differ from a plain program's by a relative error of at most 0.015.
Values may be sent and summed in bfloat16 or wider, within the bound.
No kernel may reach another device: no remote copies, remote signals or barrier semaphores. Data moves between devices by JAX's collectives and lax.ppermute only.
A program may use at most 64 MiB of HBM per device.

v0:
```python
import jax
import jax.numpy as jnp
from jax import lax
from jax.experimental import pallas as pl
from jax.experimental.pallas import tpu as pltpu
from jax.sharding import PartitionSpec as P

HEAD_DIM = 64
LANES = 128
SPAN = 128
UNROLL = 2
DECAY_SCALE = 0.6065306597126334


def mm(a, b):
    return jnp.dot(
        a.astype(jnp.bfloat16), b.astype(jnp.bfloat16), preferred_element_type=jnp.float32
    )


def mm_tn(a, b):
    return lax.dot_general(
        a.astype(jnp.bfloat16),
        b.astype(jnp.bfloat16),
        (((0,), (0,)), ((), ())),
        preferred_element_type=jnp.float32,
    )


def mm_nt(a, b):
    return lax.dot_general(
        a.astype(jnp.bfloat16),
        b.astype(jnp.bfloat16),
        (((1,), (1,)), ((), ())),
        preferred_element_type=jnp.float32,
    )


def local_kernel(
    q_ref, k_ref, v_ref, e_ref, d_ref, oloc_ref, qp_ref, maps_ref,
    uk_ref, er_ref, lk_ref, qh_f_ref, qh_b_ref, z_ref, b_ref, dec_ref,
):
    count = q_ref.shape[1] // SPAN
    kf = k_ref[...].astype(jnp.float32)
    uk = kf * lax.rsqrt(jnp.sum(kf * kf, axis=0, keepdims=True) + 1e-05)
    uk_ref[...] = uk
    er_ref[...] = uk * (1.0 / (1.0 + jnp.exp(-e_ref[...].astype(jnp.float32))))
    lk_ref[...] = -DECAY_SCALE / (1.0 + jnp.exp(-d_ref[...].astype(jnp.float32)))

    row = lax.broadcasted_iota(jnp.int32, (SPAN, SPAN), 0)
    col = lax.broadcasted_iota(jnp.int32, (SPAN, SPAN), 1)
    differ = row ^ col
    eye_span = jnp.where(differ == 0, 1.0, 0.0)
    running = jnp.where(row <= col, 1.0, 0.0).astype(jnp.bfloat16)
    eye = jnp.where(
        lax.broadcasted_iota(jnp.int32, (HEAD_DIM, HEAD_DIM), 0)
        == lax.broadcasted_iota(jnp.int32, (HEAD_DIM, HEAD_DIM), 1),
        1.0,
        0.0,
    )
    strict = (row < col, row > col)
    inclusive = (row <= col, row >= col)

    def body(step, carry):
        units = []
        for part in range(UNROLL):
            chunk = step * UNROLL + part
            lanes = pl.ds(pl.multiple_of(chunk * SPAN, SPAN), SPAN)
            q = q_ref[:, lanes].astype(jnp.float32)
            k = k_ref[:, lanes].astype(jnp.float32)
            v = v_ref[:, lanes]
            u, er, lk = uk_ref[:, lanes], er_ref[:, lanes], lk_ref[:, lanes]
            high = lk.astype(jnp.bfloat16)
            rest = lk - high.astype(jnp.float32)
            low = rest.astype(jnp.bfloat16)
            sums = mm(jnp.concatenate([high, low], axis=0), running)
            cum = sums[:HEAD_DIM] + sums[HEAD_DIM:]
            prior = cum - lk
            last = cum[:, SPAN - 1 :]
            to_prior, fade = jnp.exp(prior), jnp.exp(last - cum)
            up_f, up_b = jnp.exp(-cum), jnp.exp(prior - last)
            dec_ref[chunk] = jnp.sum(eye * jnp.exp(last), axis=0, keepdims=True)
            both = (
                (u * to_prior, q * jnp.exp(cum), k * up_f, er * up_f, k * fade, er * fade),
                (u * fade, q * jnp.exp(last - prior), k * up_b, er * up_b, k * to_prior, er * to_prior),
            )
            for way in (0, 1):
                units.append((chunk, lanes, way, v, both[way]))
        state = []
        for chunk, lanes, way, v, (ud, qd, ku, eu, kend, eend) in units:
            gram = mm_tn(
                jnp.concatenate([ku, eu], axis=1), jnp.concatenate([ud, qd], axis=1)
            )
            k_mix = jnp.where(strict[way], gram[:SPAN, :SPAN], 0.0).astype(jnp.bfloat16)
            k_read = jnp.where(inclusive[way], gram[:SPAN, SPAN:], 0.0).astype(jnp.bfloat16)
            e_mix = jnp.where(strict[way], gram[SPAN:, :SPAN], 0.0)
            e_read = jnp.where(inclusive[way], gram[SPAN:, SPAN:], 0.0).astype(jnp.bfloat16)
            inv = (eye_span - jnp.where(differ == 1, e_mix, 0.0)).astype(jnp.bfloat16)
            mixed = mm(v, jnp.concatenate([k_mix, k_read], axis=1))
            state.append([e_mix, inv, mixed, e_read])
        width = 2
        while width < SPAN:
            inside = (differ >= width) & (differ < 2 * width)
            halves = [mm(inv, jnp.where(inside, e_mix, 0.0)) for e_mix, inv, _, _ in state]
            for unit, half in zip(state, halves):
                unit[1] = (unit[1].astype(jnp.float32) - mm(half, unit[1])).astype(jnp.bfloat16)
            width *= 2
        for (chunk, lanes, way, v, (ud, qd, ku, eu, kend, eend)), (_, inv, mixed, e_read) in zip(
            units, state
        ):
            solved = mm(jnp.concatenate([ud, mixed[:, :SPAN]], axis=0), inv).astype(jnp.bfloat16)
            read = mm(solved, e_read)
            ends = mm_nt(solved, eend)
            qh = (qh_f_ref, qh_b_ref)[way]
            qh[:, lanes] = (qd - read[:HEAD_DIM]).astype(jnp.bfloat16)
            out = mixed[:, SPAN:] - read[HEAD_DIM:]
            if way == 0:
                oloc_ref[:, lanes] = out
            else:
                oloc_ref[:, lanes] += out
            z_ref[way, chunk] = ends[:HEAD_DIM].astype(jnp.bfloat16)
            b_ref[way, chunk] = mm_nt(v, kend) - ends[HEAD_DIM:]
        return carry

    lax.fori_loop(0, count // UNROLL, body, 0)

    start = jnp.concatenate([jnp.zeros_like(eye), eye], axis=0)
    carried = [start, start]
    for step in range(count):
        for way, qh in ((0, qh_f_ref), (1, qh_b_ref)):
            chunk = step if way == 0 else count - 1 - step
            lanes = slice(chunk * SPAN, (chunk + 1) * SPAN)
            now = carried[way]
            narrow = now.astype(jnp.bfloat16)
            read = mm(narrow, qh[:, lanes])
            oloc_ref[:, lanes] += read[:HEAD_DIM]
            qp_ref[way * HEAD_DIM : (way + 1) * HEAD_DIM, lanes] = read[HEAD_DIM:].astype(jnp.bfloat16)
            moved = now * dec_ref[chunk] - mm(narrow, z_ref[way, chunk])
            carried[way] = jnp.concatenate(
                [moved[:HEAD_DIM] + b_ref[way, chunk], moved[HEAD_DIM:]], axis=0
            )
    for way in (0, 1):
        maps_ref[way] = jnp.concatenate(
            [carried[way][:HEAD_DIM], carried[way][HEAD_DIM:] - eye], axis=1
        ).astype(jnp.bfloat16)


def local_half(query, key, value, erase, decay):
    tokens = query.shape[1]
    count = tokens // SPAN
    full = lambda kind: jax.ShapeDtypeStruct((HEAD_DIM, tokens), kind)
    whole = lambda kind: pltpu.VMEM((HEAD_DIM, tokens), kind)
    return pl.pallas_call(
        local_kernel,
        out_shape=(
            full(jnp.float32),
            jax.ShapeDtypeStruct((2 * HEAD_DIM, tokens), jnp.bfloat16),
            jax.ShapeDtypeStruct((2, HEAD_DIM, 2 * HEAD_DIM), jnp.bfloat16),
        ),
        scratch_shapes=[
            whole(jnp.float32),
            whole(jnp.float32),
            whole(jnp.float32),
            whole(jnp.bfloat16),
            whole(jnp.bfloat16),
            pltpu.VMEM((2, count, HEAD_DIM, HEAD_DIM), jnp.bfloat16),
            pltpu.VMEM((2, count, HEAD_DIM, HEAD_DIM), jnp.float32),
            pltpu.VMEM((count, 1, HEAD_DIM), jnp.float32),
        ],
        cost_estimate=pl.CostEstimate(
            flops=16 * 22 * 2 * 128**3, bytes_accessed=tokens * 64 * 18, transcendentals=tokens * 64 * 9
        ),
        name="mixer_local",
    )(query, key, value, erase, decay)


def finish_kernel(me_ref, got_ref, oloc_ref, qp_ref, gain_ref, out_ref):
    devices = got_ref.shape[0]
    me = me_ref[0]
    left = lax.broadcasted_iota(jnp.int32, (2 * HEAD_DIM, 2 * HEAD_DIM), 1) < HEAD_DIM
    entering = []
    for way in (0, 1):
        level = []
        for place in range(devices):
            source = place if way == 0 else devices - 1 - place
            wanted = source < me if way == 0 else source > me
            both = got_ref[source].astype(jnp.float32)
            stacked = jnp.concatenate([pltpu.roll(both, HEAD_DIM, 1), both], axis=0)
            level.append(jnp.where(left & wanted, stacked, 0.0))
        while len(level) > 1:
            level = [
                first + mm(first, later) + later
                for first, later in zip(level[::2], level[1::2])
            ]
        entering.append(level[0][HEAD_DIM:])
    states = entering[0] + pltpu.roll(entering[1], HEAD_DIM, 1)
    summed = oloc_ref[...] + mm(states, qp_ref[...])
    center = jnp.mean(summed, axis=0, keepdims=True)
    away = summed - center
    spread = jnp.mean(away * away, axis=0, keepdims=True)
    out_ref[...] = (
        away * lax.rsqrt(spread + HEAD_DIM * 1e-05) * gain_ref[...]
    ).astype(jnp.bfloat16)


def finish_half(me, got, oloc, qp, gain):
    return pl.pallas_call(
        finish_kernel,
        out_shape=jax.ShapeDtypeStruct(oloc.shape, jnp.bfloat16),
        in_specs=[pl.BlockSpec(memory_space=pltpu.SMEM)] + [pl.BlockSpec(memory_space=pltpu.VMEM)] * 4,
        cost_estimate=pl.CostEstimate(
            flops=62 * 2 * 128 * 64 * 64 + 4 * 64 * 64 * 1024, bytes_accessed=2**20, transcendentals=1024
        ),
        name="mixer_finish",
    )(me, got, oloc, qp, gain)


def expert_kernel(rows_ref, gate_ref, up_ref, down_ref, out_ref):
    parts = rows_ref.shape[0]
    rows = jnp.concatenate([rows_ref[j] for j in range(parts)], axis=1)
    gate = mm(rows, gate_ref[...])
    up = mm(rows, up_ref[...])
    hidden = (gate / (1.0 + jnp.exp(-gate)) * up).astype(jnp.bfloat16)
    result = mm(hidden, down_ref[...]).astype(jnp.bfloat16)
    for j in range(parts):
        out_ref[j] = result[:, j * LANES : (j + 1) * LANES]


def expert_rows(rows, gate, up, down):
    parts, total, lanes = rows.shape
    tile = 256 if total % 256 == 0 else total
    block = pl.BlockSpec((parts, tile, lanes), lambda i: (0, i, 0))
    fixed = lambda array: pl.BlockSpec(array.shape, lambda i: (0, 0))
    return pl.pallas_call(
        expert_kernel,
        grid=(total // tile,),
        in_specs=[block, fixed(gate), fixed(up), fixed(down)],
        out_specs=block,
        out_shape=jax.ShapeDtypeStruct(rows.shape, jnp.bfloat16),
        cost_estimate=pl.CostEstimate(
            flops=6 * total * gate.size,
            bytes_accessed=2 * (2 * rows.size + 3 * gate.size),
            transcendentals=total * gate.shape[1],
        ),
        name="expert_rows",
    )(rows, gate, up, down)


def slot_targets(routes, experts_n, capacity):
    onehot = (routes[:, :, None] == jnp.arange(experts_n, dtype=jnp.int32)[None, None, :]).astype(
        jnp.int32
    )
    flat = onehot.reshape(-1, experts_n)
    before = jnp.cumsum(flat, axis=0) - flat
    slot_index = jnp.sum(before * flat, axis=-1).reshape(routes.shape)
    return routes * capacity + slot_index


def dispatch_matrix(targets, slot_total):
    matches = targets[None, :, :] == jnp.arange(slot_total, dtype=jnp.int32)[:, None, None]
    return jnp.sum(matches.astype(jnp.float32), axis=-1).astype(jnp.bfloat16)


def spread(array, axis):
    return lax.all_to_all(array, axis, 0, 0, tiled=True)


def on_device(
    query_in,
    key_in,
    value_in,
    erase_pre,
    decay_pre,
    mix_gain,
    expert_in,
    expert_gain,
    routes,
    route_weight,
    gate_weight,
    up_weight,
    down_weight,
):
    experts_n, shares = lax.axis_size("ep"), lax.axis_size("tp")
    row_count, features = expert_in.shape
    capacity = 3 * routes.shape[1] * row_count // (2 * experts_n)
    slot_total = experts_n * capacity
    col_count = features // shares
    at = lax.axis_index("tp") * col_count
    input_f = expert_in.astype(jnp.float32)
    scale = lax.rsqrt(jnp.mean(input_f * input_f, axis=-1, keepdims=True) + 1e-06)
    own = lax.dynamic_slice_in_dim(expert_in, at, col_count, 1).astype(jnp.float32)
    normed = (own * scale * lax.dynamic_slice_in_dim(expert_gain, at, col_count, 0)).astype(
        jnp.bfloat16
    )
    targets = slot_targets(routes, experts_n, capacity)
    outgoing = mm(dispatch_matrix(targets, slot_total), normed).astype(jnp.bfloat16)
    arrived = spread(outgoing.reshape(experts_n, capacity, col_count), "ep").reshape(
        slot_total, col_count
    )
    shared = spread(jnp.broadcast_to(arrived[None], (shares, *arrived.shape)), "tp")

    oloc, qp, maps = local_half(query_in, key_in, value_in, erase_pre, decay_pre)
    me = lax.axis_index("ep")
    later = jnp.arange(experts_n) > me
    outgoing = jnp.where(later[:, None, None], maps[:1], maps[1:])

    shared, outgoing = lax.optimization_barrier((shared, outgoing))
    partial = expert_rows(shared, gate_weight[0], up_weight[0], down_weight[0])
    got = spread(outgoing, "ep")
    partial, got = lax.optimization_barrier((partial, got))
    pieces = spread(partial, "tp")
    summed = jnp.sum(pieces.astype(jnp.float32), axis=0).astype(jnp.bfloat16)
    returned = spread(summed.reshape(experts_n, capacity, col_count), "ep").reshape(
        slot_total, col_count
    )
    mixer_out = finish_half(
        me.reshape(1).astype(jnp.int32), got, oloc, qp, mix_gain[:, None]
    )
    matches = targets[:, :, None] == jnp.arange(slot_total, dtype=jnp.int32)[None, None, :]
    combine = jnp.sum(matches.astype(jnp.float32) * route_weight[:, :, None], axis=1)
    expert_out = jnp.dot(combine, returned.astype(jnp.float32)).astype(jnp.bfloat16)
    return (mixer_out, expert_out)


def solution(mesh):
    placed = (
        P("tp", "ep"),
        P("tp", "ep"),
        P("tp", "ep"),
        P("tp", "ep"),
        P("tp", "ep"),
        P("tp"),
        P("ep", None),
        P(),
        P("ep", None),
        P("ep", None),
        P("ep", None, "tp"),
        P("ep", None, "tp"),
        P("ep", "tp", None),
    )
    return jax.shard_map(
        on_device,
        mesh=mesh,
        in_specs=placed,
        out_specs=(P("tp", "ep"), P("ep", "tp")),
        check_vma=False,
    )
```

profile of v0, /device:TPU:1, one launch (start us, length us, event | category | flops | bytes accessed | tf_op | source)
XLA Modules:
  0.0 205.7 jit_solution(3980307420524712087)
XLA Ops:
  0.6 0.0 copy-start.1
  0.6 0.9 copy.40
  1.5 0.1 eq.56
  1.7 0.1 eq.52
  1.9 1.2 reduce-window.6
  3.0 0.2 slice_reduce_fusion
  3.3 0.1 fusion.3
  3.4 0.1 reshape.56
  3.6 0.1 copy.43
  3.6 0.7 multiply_add_fusion
  4.3 0.3 convert_reduce_fusion
  4.7 0.0 copy-done.1
  4.7 0.3 multiply_reduce_fusion
  5.0 0.8 dynamic_slice.7
  5.7 0.3 convolution_convert_fusion
  6.1 35.3 %all_to_all.25 = bf16[32,24,128]{2,1,0:T(8,128)(2,1)S(1)} all-to-all(bf16[32,24,128]{2,1,0:T(8,128)(2,1)S(1)} %bitcast.40), channel_id=1, replica_groups=mesh['ep'=32,'tp'=16] {'ep'}, dimensions={0} | all-to-all | bytes 393216 | tf_op jit(solution)/shard_map/all_to_all | solution.py:265
  41.4 2.3 %broadcast_in_dim.49 = bf16[16,768,128]{2,1,0:T(8,128)(2,1)} broadcast(bf16[768,128]{1,0:T(8,128)(2,1)S(1)} %bitcast.38), dimensions={1,2} | broadcast | bytes 3342336 | tf_op jit(solution)/shard_map/broadcast_in_dim | solution.py:300
  43.7 6.8 %all-to-all-start.1 = ((bf16[16,768,128]{2,1,0:T(8,128)(2,1)}), bf16[16,768,128]{2,1,0:T(8,128)(2,1)S(1)}, u32[]{:S(2)}, u32[]{:S(2)}) async-start(bf16[16,768,128]{2,1,0:T(8,128)(2,1)} %broadcast_in_dim.49), calls=%async_computation.1 | async-start | bytes 6291456 | tf_op jit(solution)/shard_map/all_to_all | solution.py:265
  50.4 15.3 %mixer_local.1 = (f32[64,1024]{1,0:T(8,128)}, bf16[128,1024]{1,0:T(8,128)(2,1)}, bf16[2,64,128]{2,1,0:T(8,128)(2,1)}) custom-call(bf16[64,1024]{1,0:T(8,128)(2,1)} %q_ref.1, bf16[64,1024]{1,0:T(8,128)(2,1)} %k_ref.1, bf16[64,1024]{1,0:T(8,128)(2,1)} %v_ref.1, bf16[64,1024]{1,0:T(8,128)(2,1)} %e_ref.1, bf16[64,1024]{1,0:T(8,128)(2,1)} %d_ref.1), custom_call_target="tpu_custom_call" | custom-call | flops 1476395008 | bytes 1179648 | tf_op jit(solution)/shard_map/mixer_local/pallas_call | solution.py:153
  65.8 0.7 slice_bitcast_fusion.1
  66.5 1.0 broadcast_select_fusion
  67.5 27.2 %all-to-all-done.1.rows_ref = bf16[16,768,128]{2,1,0:T(8,128)(2,1)S(1)} async-done(((bf16[16,768,128]{2,1,0:T(8,128)(2,1)}), bf16[16,768,128]{2,1,0:T(8,128)(2,1)S(1)}, u32[]{:S(2)}, u32[]{:S(2)}) %all-to-all-start.1) | async-done | bytes 3145760 | tf_op jit(solution)/shard_map/all_to_all | solution.py:265
  94.7 0.0 copy-start
  94.7 8.2 %all-to-all-start.2 = ((bf16[32,64,128]{2,1,0:T(8,128)(2,1)}), bf16[32,64,128]{2,1,0:T(8,128)(2,1)}, u32[]{:S(2)}, u32[]{:S(2)}) async-start(bf16[32,64,128]{2,1,0:T(8,128)(2,1)} %broadcast_select_fusion), calls=%async_computation.2 | async-start | bytes 1048576 | tf_op jit(solution)/shard_map/all_to_all | solution.py:265
  102.9 2.3 %copy.44 = bf16[1,2048,224]{2,1,0:T(8,128)(2,1)} copy(bf16[1,2048,224]{1,2,0:T(8,128)(2,1)} %param.23) | data formatting | bytes 1835008 | tf_op args[10]
  105.2 2.3 %copy.45 = bf16[1,2048,224]{2,1,0:T(8,128)(2,1)} copy(bf16[1,2048,224]{1,2,0:T(8,128)(2,1)} %param.24) | data formatting | bytes 1835008 | tf_op args[11]
  107.4 0.0 copy-done
  107.4 6.9 %expert_rows.1 = bf16[16,768,128]{2,1,0:T(8,128)(2,1)} custom-call(bf16[16,768,128]{2,1,0:T(8,128)(2,1)} %copy-done, bf16[2048,224]{1,0:T(8,128)(2,1)} %bitcast.35, bf16[2048,224]{1,0:T(8,128)(2,1)} %bitcast.36, bf16[224,2048]{1,0:T(8,128)(2,1)} %bitcast.37), custom_call_target="tpu_custom_call" | custom-call | flops 2113929216 | bytes 9043968 | tf_op jit(solution)/shard_map/expert_rows/pallas_call | solution.py:234
  114.3 22.1 %all-to-all-done.2.got_ref = bf16[32,64,128]{2,1,0:T(8,128)(2,1)} async-done(((bf16[32,64,128]{2,1,0:T(8,128)(2,1)}), bf16[32,64,128]{2,1,0:T(8,128)(2,1)}, u32[]{:S(2)}, u32[]{:S(2)}) %all-to-all-start.2) | async-done | bytes 524320 | tf_op jit(solution)/shard_map/all_to_all | solution.py:265
  136.5 42.8 %all_to_all.26 = bf16[16,768,128]{2,1,0:T(8,128)(2,1)S(1)} all-to-all(bf16[16,768,128]{2,1,0:T(8,128)(2,1)} %expert_rows.1), channel_id=1, replica_groups=mesh['ep'=32,'tp'=16] {'tp'}, dimensions={0} | all-to-all | bytes 6291456 | tf_op jit(solution)/shard_map/all_to_all | solution.py:265
  179.2 0.0 copy-start.3
  179.3 0.0 copy-start.2
  179.3 1.2 reduce_sum.52
  180.4 5.4 %all-to-all-start.4 = ((bf16[32,24,128]{2,1,0:T(8,128)(2,1)}), bf16[32,24,128]{2,1,0:T(8,128)(2,1)S(1)}, u32[]{:S(2)}, u32[]{:S(2)}) async-start(bf16[32,24,128]{2,1,0:T(8,128)(2,1)} %bitcast.10), calls=%async_computation.4 | async-start | bytes 393216 | tf_op jit(solution)/shard_map/all_to_all | solution.py:265
  185.8 0.0 copy-done.3
  185.8 0.7 copy.46.gain_ref
  186.6 0.0 copy-done.2
  186.6 0.2 select_reduce_fusion
  186.8 3.8 %mixer_finish.1 = bf16[64,1024]{1,0:T(8,128)(2,1)} custom-call(s32[1]{0:T(128)} %bitcast.me_ref, bf16[32,64,128]{2,1,0:T(8,128)(2,1)} %all-to-all-done.2.got_ref, f32[64,1024]{1,0:T(8,128)} %get-tuple-element.13.oloc_ref, bf16[128,1024]{1,0:T(8,128)(2,1)} %get-tuple-element.14.qp_ref, f32[64,1]{1,0:T(8,128)} %copy.46.gain_ref), custom_call_target="tpu_custom_call" | custom-call | flops 81788928 | bytes 1048576 | tf_op jit(solution)/shard_map/mixer_finish/pallas_call | solution.py:207
  190.6 14.2 %all-to-all-done.4 = bf16[32,24,128]{2,1,0:T(8,128)(2,1)S(1)} async-done(((bf16[32,24,128]{2,1,0:T(8,128)(2,1)}), bf16[32,24,128]{2,1,0:T(8,128)(2,1)S(1)}, u32[]{:S(2)}, u32[]{:S(2)}) %all-to-all-start.4) | async-done | bytes 196640 | tf_op jit(solution)/shard_map/all_to_all | solution.py:265
  204.8 0.9 fusion.9
  (5 shorter events, 0.1 us)
Async XLA Ops:
  0.6 4.0 %copy-start.1 = (bf16[256,2048]{1,0:T(8,128)(2,1)S(1)}, bf16[256,2048]{1,0:T(8,128)(2,1)}, u32[]{:S(2)}) copy-start(bf16[256,2048]{1,0:T(8,128)(2,1)} %param.19) | copy-start | bytes 3145732
  43.7 51.0 %all-to-all-start.1 = ((bf16[16,768,128]{2,1,0:T(8,128)(2,1)}), bf16[16,768,128]{2,1,0:T(8,128)(2,1)S(1)}, u32[]{:S(2)}, u32[]{:S(2)}) async-start(bf16[16,768,128]{2,1,0:T(8,128)(2,1)} %broadcast_in_dim.49), calls=%async_computation.1 | async-start | bytes 6291456 | tf_op jit(solution)/shard_map/all_to_all | solution.py:265
  94.7 12.7 %copy-start = (bf16[16,768,128]{2,1,0:T(8,128)(2,1)}, bf16[16,768,128]{2,1,0:T(8,128)(2,1)S(1)}, u32[]{:S(2)}) copy-start(bf16[16,768,128]{2,1,0:T(8,128)(2,1)S(1)} %all-to-all-done.1.rows_ref) | copy-start | bytes 9437188
  94.7 41.8 %all-to-all-start.2 = ((bf16[32,64,128]{2,1,0:T(8,128)(2,1)}), bf16[32,64,128]{2,1,0:T(8,128)(2,1)}, u32[]{:S(2)}, u32[]{:S(2)}) async-start(bf16[32,64,128]{2,1,0:T(8,128)(2,1)} %broadcast_select_fusion), calls=%async_computation.2 | async-start | bytes 1048576 | tf_op jit(solution)/shard_map/all_to_all | solution.py:265
  179.2 6.6 %copy-start.3 = (f32[64]{0:T(128)S(1)}, f32[64]{0:T(128)}, u32[]{:S(2)}) copy-start(f32[64]{0:T(128)} %param.18) | copy-start | bytes 772
  179.3 7.3 %copy-start.2 = (f32[256,2]{0,1:T(2,128)S(1)}, f32[256,2]{0,1:T(2,128)}, u32[]{:S(2)}) copy-start(f32[256,2]{0,1:T(2,128)} %param.22) | copy-start | bytes 6148
  180.4 24.4 %all-to-all-start.4 = ((bf16[32,24,128]{2,1,0:T(8,128)(2,1)}), bf16[32,24,128]{2,1,0:T(8,128)(2,1)S(1)}, u32[]{:S(2)}, u32[]{:S(2)}) async-start(bf16[32,24,128]{2,1,0:T(8,128)(2,1)} %bitcast.10), calls=%async_computation.4 | async-start | bytes 393216 | tf_op jit(solution)/shard_map/all_to_all | solution.py:265
where the time goes:
time: 206 us
  blocking collectives  78.1 us (38%)
  waiting for transfers between devices  63.5 us (31%)
  Pallas kernels  26 us (13%)
  starting transfers between devices  20.4 us (10%)
  local copies, waits for them, and re-layouts  10.7 us (5%)
  other arithmetic  5.01 us (2%)
    all_to_all x2, blocking collectives, spread(): return lax.all_to_all(array, axis, 0, 0, tiled=True)  78.1 us
    all_to_all x3, waiting for transfers between devices, spread(): return lax.all_to_all(array, axis, 0, 0, tiled=True)  63.5 us
    all_to_all x3, starting transfers between devices, spread(): return lax.all_to_all(array, axis, 0, 0, tiled=True)  20.4 us
    pallas_call x1, Pallas kernels, local_half(): pl.pallas_call(local_kernel, out_shape=(full(jnp.float32), jax.ShapeDtype...  15.3 us
    pallas_call x1, Pallas kernels, expert_rows(): pl.pallas_call(expert_kernel, grid=(total // tile,), in_specs=[block, fix...  6.91 us
    unnamed x11, local copies, waits for them, and re-layouts  5.44 us
  transfers between devices with their start and end apart: 3, of which 3 were waited for; matrix products, arithmetic and copies ran while one was open for 3% of the time, Pallas kernels for 13%

commit v1 on v0

--- a/solution.py
+++ b/solution.py
@@ -174,25 +174,46 @@
     )(query, key, value, erase, decay)
 
 
-def finish_kernel(me_ref, got_ref, oloc_ref, qp_ref, gain_ref, out_ref):
-    devices = got_ref.shape[0]
-    me = me_ref[0]
+def stacked(wide):
     left = lax.broadcasted_iota(jnp.int32, (2 * HEAD_DIM, 2 * HEAD_DIM), 1) < HEAD_DIM
-    entering = []
-    for way in (0, 1):
-        level = []
-        for place in range(devices):
-            source = place if way == 0 else devices - 1 - place
-            wanted = source < me if way == 0 else source > me
-            both = got_ref[source].astype(jnp.float32)
-            stacked = jnp.concatenate([pltpu.roll(both, HEAD_DIM, 1), both], axis=0)
-            level.append(jnp.where(left & wanted, stacked, 0.0))
-        while len(level) > 1:
-            level = [
-                first + mm(first, later) + later
-                for first, later in zip(level[::2], level[1::2])
-            ]
-        entering.append(level[0][HEAD_DIM:])
+    full = wide.astype(jnp.float32)
+    return jnp.where(left, jnp.concatenate([pltpu.roll(full, HEAD_DIM, 1), full], axis=0), 0.0)
+
+
+def widened(tall):
+    return tall[HEAD_DIM:] + pltpu.roll(tall[:HEAD_DIM], HEAD_DIM, 1)
+
+
+def composed(first, later):
+    return first + mm(first, later) + later
+
+
+def step_kernel(arrived_f_ref, arrived_b_ref, past_ref, own_ref, next_past_ref, through_ref):
+    for way, arrived in ((0, arrived_f_ref), (1, arrived_b_ref)):
+        past = composed(stacked(arrived[...]), stacked(past_ref[way]))
+        next_past_ref[way] = widened(past)
+        through_ref[way] = widened(composed(past, stacked(own_ref[way]))).astype(jnp.bfloat16)
+
+
+def scan_step(arrived, past, own):
+    return pl.pallas_call(
+        step_kernel,
+        out_shape=(
+            jax.ShapeDtypeStruct(past.shape, jnp.float32),
+            jax.ShapeDtypeStruct(past.shape, jnp.bfloat16),
+        ),
+        cost_estimate=pl.CostEstimate(
+            flops=8 * 128**3, bytes_accessed=6 * 2 * past.size, transcendentals=0
+        ),
+        name="scan_step",
+    )(*arrived, past, own)
+
+
+def finish_kernel(arrived_f_ref, arrived_b_ref, past_ref, oloc_ref, qp_ref, gain_ref, out_ref):
+    entering = [
+        composed(stacked(arrived[...]), stacked(past_ref[way]))[HEAD_DIM:]
+        for way, arrived in ((0, arrived_f_ref), (1, arrived_b_ref))
+    ]
     states = entering[0] + pltpu.roll(entering[1], HEAD_DIM, 1)
     summed = oloc_ref[...] + mm(states, qp_ref[...])
     center = jnp.mean(summed, axis=0, keepdims=True)
@@ -203,16 +224,22 @@
     ).astype(jnp.bfloat16)
 
 
-def finish_half(me, got, oloc, qp, gain):
+def finish_half(arrived, past, oloc, qp, gain):
     return pl.pallas_call(
         finish_kernel,
         out_shape=jax.ShapeDtypeStruct(oloc.shape, jnp.bfloat16),
-        in_specs=[pl.BlockSpec(memory_space=pltpu.SMEM)] + [pl.BlockSpec(memory_space=pltpu.VMEM)] * 4,
         cost_estimate=pl.CostEstimate(
-            flops=62 * 2 * 128 * 64 * 64 + 4 * 64 * 64 * 1024, bytes_accessed=2**20, transcendentals=1024
+            flops=4 * 128**3 + 16 * 128**3, bytes_accessed=2**20, transcendentals=1024
         ),
         name="mixer_finish",
-    )(me, got, oloc, qp, gain)
+    )(*arrived, past, oloc, qp, gain)
+
+
+def passed_on(through, distance):
+    count = lax.axis_size("ep")
+    ahead = [(i, i + distance) for i in range(count - distance)]
+    back = [(i + distance, i) for i in range(count - distance)]
+    return lax.ppermute(through[0], "ep", ahead), lax.ppermute(through[1], "ep", back)
 
 
 def expert_kernel(rows_ref, gate_ref, up_ref, down_ref, out_ref):
@@ -297,25 +324,29 @@
     arrived = spread(outgoing.reshape(experts_n, capacity, col_count), "ep").reshape(
         slot_total, col_count
     )
+    oloc, qp, own_maps = local_half(query_in, key_in, value_in, erase_pre, decay_pre)
+    arrived, own_maps = lax.optimization_barrier((arrived, own_maps))
     shared = spread(jnp.broadcast_to(arrived[None], (shares, *arrived.shape)), "tp")
 
-    oloc, qp, maps = local_half(query_in, key_in, value_in, erase_pre, decay_pre)
-    me = lax.axis_index("ep")
-    later = jnp.arange(experts_n) > me
-    outgoing = jnp.where(later[:, None, None], maps[:1], maps[1:])
-
-    shared, outgoing = lax.optimization_barrier((shared, outgoing))
+    past = jnp.zeros(own_maps.shape, jnp.float32)
+    through, distance = own_maps, 1
+    while distance < experts_n // 4:
+        past, through = scan_step(passed_on(through, distance), past, own_maps)
+        distance *= 2
+    shared, past, through = lax.optimization_barrier((shared, past, through))
     partial = expert_rows(shared, gate_weight[0], up_weight[0], down_weight[0])
-    got = spread(outgoing, "ep")
-    partial, got = lax.optimization_barrier((partial, got))
+    partial, past, through = lax.optimization_barrier((partial, past, through))
+    while distance < experts_n // 2:
+        past, through = scan_step(passed_on(through, distance), past, own_maps)
+        distance *= 2
+    crossing = passed_on(through, distance)
     pieces = spread(partial, "tp")
+    pieces, crossing = lax.optimization_barrier((pieces, crossing))
     summed = jnp.sum(pieces.astype(jnp.float32), axis=0).astype(jnp.bfloat16)
     returned = spread(summed.reshape(experts_n, capacity, col_count), "ep").reshape(
         slot_total, col_count
     )
-    mixer_out = finish_half(
-        me.reshape(1).astype(jnp.int32), got, oloc, qp, mix_gain[:, None]
-    )
+    mixer_out = finish_half(crossing, past, oloc, qp, mix_gain[:, None])
     matches = targets[:, :, None] == jnp.arange(slot_total, dtype=jnp.int32)[None, None, :]
     combine = jnp.sum(matches.astype(jnp.float32) * route_weight[:, :, None], axis=1)
     expert_out = jnp.dot(combine, returned.astype(jnp.float32)).astype(jnp.bfloat16)

time: 206 us -> 189 us (0.917)
  blocking collectives: 78.1 us -> 0 us
  starting transfers between devices: 20.4 us -> 77.9 us
  waiting for transfers between devices: 63.5 us -> 54.7 us
  Pallas kernels: 26 us -> 32.3 us
  local copies, waits for them, and re-layouts: 10.7 us -> 16.3 us
    all_to_all x2 -> x0, blocking collectives: 78.1 us -> none  [spread(): return lax.all_to_all(array, axis, 0, 0, tiled=True)]
    all_to_all x3 -> x4, waiting for transfers between devices: 63.5 us -> 28.9 us  [spread(): return lax.all_to_all(array, axis, 0, 0, tiled=True)]
    ppermute x0 -> x10, starting transfers between devices: none -> 32.2 us  [the longest x5 25.1 us: passed_on(): lax.ppermute(through[0], 'ep', ahead)]
    ppermute x0 -> x10, waiting for transfers between devices: none -> 25.8 us  [the longest x5 25.8 us: passed_on(): lax.ppermute(through[1], 'ep', back)]
    all_to_all x3 -> x4, starting transfers between devices: 20.4 us -> 45.7 us  [spread(): return lax.all_to_all(array, axis, 0, 0, tiled=True)]
    pallas_call x0 -> x4, Pallas kernels: none -> 7.76 us  [scan_step(): pl.pallas_call(step_kernel, out_shape=(jax.ShapeDtypeStruct(past.shape, j...]
    unnamed x11 -> x35, local copies, waits for them, and re-layouts: 5.44 us -> 8.95 us
    squeeze x0 -> x5, local copies, waits for them, and re-layouts: none -> 2.22 us  [passed_on(): through[1]]
  transfers between devices with their start and end apart: 3 -> 14, of which waited for: 3 -> 8; matrix products, arithmetic and copies ran while one was open for 3% -> 4% of each run, Pallas kernels for 13% -> 14%
where the time goes in v1:
time: 189 us; the launch traced here: 188 us
  starting transfers between devices  77.9 us (41%)
  waiting for transfers between devices  54.7 us (29%)
  Pallas kernels  32.3 us (17%)
  local copies, waits for them, and re-layouts  16.3 us (9%)
  other arithmetic  4.01 us (2%)
    all_to_all x4, starting transfers between devices, spread(): return lax.all_to_all(array, axis, 0, 0, tiled=True)  45.7 us
    all_to_all x4, waiting for transfers between devices, spread(): return lax.all_to_all(array, axis, 0, 0, tiled=True)  28.9 us
    ppermute x5, waiting for transfers between devices, passed_on(): lax.ppermute(through[1], 'ep', back)  25.8 us
    ppermute x5, starting transfers between devices, passed_on(): lax.ppermute(through[0], 'ep', ahead)  25.1 us
    pallas_call x1, Pallas kernels, local_half(): pl.pallas_call(local_kernel, out_shape=(full(jnp.float32), jax.ShapeDtype...  15.4 us
    unnamed x35, local copies, waits for them, and re-layouts  8.95 us
    pallas_call x4, Pallas kernels, scan_step(): pl.pallas_call(step_kernel, out_shape=(jax.ShapeDtypeStruct(past.shape, j...  7.76 us
    ppermute x5, starting transfers between devices, passed_on(): lax.ppermute(through[1], 'ep', back)  7.09 us
  transfers between devices with their start and end apart: 14, of which 8 were waited for; matrix products, arithmetic and copies ran while one was open for 4% of the time, Pallas kernels for 14%

profile of v1, /device:TPU:1, one launch (start us, length us, event | category | flops | bytes accessed | tf_op | source)
XLA Modules:
  0.0 188.1 jit_solution(2979495772242111033)
XLA Ops:
  0.6 0.9 copy.40
  1.5 0.1 eq.56
  1.7 0.1 eq.52
  1.9 1.2 reduce-window.6
  3.0 0.2 slice_reduce_fusion
  3.3 0.1 fusion.3
  3.4 0.1 reshape.51
  3.6 0.1 copy.43
  3.6 0.7 multiply_add_fusion
  4.3 0.3 convert_reduce_fusion
  4.7 0.3 multiply_reduce_fusion
  5.0 0.8 dynamic_slice.7
  5.7 1.0 convolution_convert_fusion
  6.7 16.7 %all-to-all-start = ((bf16[32,24,128]{2,1,0:T(8,128)(2,1)}), bf16[32,24,128]{2,1,0:T(8,128)(2,1)S(1)}, u32[]{:S(2)}, u32[]{:S(2)}) async-start(bf16[32,24,128]{2,1,0:T(8,128)(2,1)} %bitcast.1), calls=%async_computation | async-start | bytes 393216 | tf_op jit(solution)/shard_map/all_to_all | solution.py:292
  23.5 15.4 %mixer_local.1 = (f32[64,1024]{1,0:T(8,128)}, bf16[128,1024]{1,0:T(8,128)(2,1)}, bf16[2,64,128]{2,1,0:T(8,128)(2,1)}) custom-call(bf16[64,1024]{1,0:T(8,128)(2,1)} %q_ref.1, bf16[64,1024]{1,0:T(8,128)(2,1)} %k_ref.1, bf16[64,1024]{1,0:T(8,128)(2,1)} %v_ref.1, bf16[64,1024]{1,0:T(8,128)(2,1)} %e_ref.1, bf16[64,1024]{1,0:T(8,128)(2,1)} %d_ref.1), custom_call_target="tpu_custom_call" | custom-call | flops 1476395008 | bytes 1179648 | tf_op jit(solution)/shard_map/mixer_local/pallas_call | solution.py:153
  38.9 3.4 %all-to-all-done = bf16[32,24,128]{2,1,0:T(8,128)(2,1)S(1)} async-done(((bf16[32,24,128]{2,1,0:T(8,128)(2,1)}), bf16[32,24,128]{2,1,0:T(8,128)(2,1)S(1)}, u32[]{:S(2)}, u32[]{:S(2)}) %all-to-all-start) | async-done | bytes 196640 | tf_op jit(solution)/shard_map/all_to_all | solution.py:292
  42.3 2.3 %broadcast_in_dim.6 = bf16[16,768,128]{2,1,0:T(8,128)(2,1)} broadcast(bf16[768,128]{1,0:T(8,128)(2,1)S(1)} %bitcast.53), dimensions={1,2} | broadcast | bytes 3342336 | tf_op jit(solution)/shard_map/broadcast_in_dim | solution.py:329
  44.5 6.9 %all-to-all-start.1 = ((bf16[16,768,128]{2,1,0:T(8,128)(2,1)}), bf16[16,768,128]{2,1,0:T(8,128)(2,1)S(1)}, u32[]{:S(2)}, u32[]{:S(2)}) async-start(bf16[16,768,128]{2,1,0:T(8,128)(2,1)} %broadcast_in_dim.6), calls=%async_computation.1 | async-start | bytes 6291456 | tf_op jit(solution)/shard_map/all_to_all | solution.py:292
  51.4 3.3 %collective-permute-start = (bf16[64,128]{1,0:T(8,128)(2,1)S(1)}, bf16[64,128]{1,0:T(8,128)(2,1)S(1)}, u32[]{:S(2)}, u32[]{:S(2)}) collective-permute-start(bf16[64,128]{1,0:T(8,128)(2,1)S(1)} %get-tuple-element.55), channel_id=1, source_target_pairs={{0,16},{16,32},{32,48},{48,64},{64,80},{80,96},{96,112},{112,128},... | collective-permute-start | bytes 49160 | tf_op jit(solution)/shard_map/ppermute | solution.py:242
  54.8 1.9 %collective-permute-start.1 = (bf16[64,128]{1,0:T(8,128)(2,1)S(1)}, bf16[64,128]{1,0:T(8,128)(2,1)S(1)}, u32[]{:S(2)}, u32[]{:S(2)}) collective-permute-start(bf16[64,128]{1,0:T(8,128)(2,1)S(1)} %get-tuple-element.54), channel_id=1, source_target_pairs={{16,0},{32,16},{48,32},{64,48},{80,64},{96,80},{112,96},{128,112},... | collective-permute-start | bytes 49160 | tf_op jit(solution)/shard_map/ppermute | solution.py:242
  56.7 0.0 collective-permute-done.arrived_f_ref
  56.8 3.4 %collective-permute-done.1.arrived_b_ref = bf16[64,128]{1,0:T(8,128)(2,1)S(1)} collective-permute-done((bf16[64,128]{1,0:T(8,128)(2,1)S(1)}, bf16[64,128]{1,0:T(8,128)(2,1)S(1)}, u32[]{:S(2)}, u32[]{:S(2)}) %collective-permute-start.1) | collective-permute-done | bytes 16416 | tf_op jit(solution)/shard_map/ppermute | solution.py:242
  60.2 0.6 broadcast_in_dim.7.past_ref
  60.8 1.9 %scan_step.4 = (f32[2,64,128]{2,1,0:T(8,128)}, bf16[2,64,128]{2,1,0:T(8,128)(2,1)}) custom-call(bf16[64,128]{1,0:T(8,128)(2,1)} %copy-done.7, bf16[64,128]{1,0:T(8,128)(2,1)} %copy-done.11, f32[2,64,128]{2,1,0:T(8,128)} %broadcast_in_dim.7.past_ref, bf16[2,64,128]{2,1,0:T(8,128)(2,1)} %get-tuple-element.26.own_ref), custom_call_target="tpu_custom_call" | custom-call | flops 16777216 | bytes 196608 | tf_op jit(solution)/shard_map/scan_step/pallas_call | solution.py:199
  62.7 0.7 slice_bitcast_fusion.6
  63.5 1.7 collective-permute-start.2
  65.1 1.3 collective-permute-start.3
  66.4 0.0 collective-permute-done.2.arrived_f_ref
  66.5 3.5 %collective-permute-done.3.arrived_b_ref = bf16[64,128]{1,0:T(8,128)(2,1)S(1)} collective-permute-done((bf16[64,128]{1,0:T(8,128)(2,1)S(1)}, bf16[64,128]{1,0:T(8,128)(2,1)S(1)}, u32[]{:S(2)}, u32[]{:S(2)}) %collective-permute-start.3) | collective-permute-done | bytes 16416 | tf_op jit(solution)/shard_map/ppermute | solution.py:242
  69.9 0.6 copy-done.12
  70.5 1.9 %scan_step.5 = (f32[2,64,128]{2,1,0:T(8,128)}, bf16[2,64,128]{2,1,0:T(8,128)(2,1)}) custom-call(bf16[64,128]{1,0:T(8,128)(2,1)} %copy-done.8, bf16[64,128]{1,0:T(8,128)(2,1)} %copy-done.12, f32[2,64,128]{2,1,0:T(8,128)} %get-tuple-element.28.past_ref, bf16[2,64,128]{2,1,0:T(8,128)(2,1)} %get-tuple-element.26.own_ref), custom_call_target="tpu_custom_call" | custom-call | flops 16777216 | bytes 196608 | tf_op jit(solution)/shard_map/scan_step/pallas_call | solution.py:199
  72.5 0.7 slice_bitcast_fusion.4
  73.2 4.9 %collective-permute-start.4 = (bf16[64,128]{1,0:T(8,128)(2,1)S(1)}, bf16[64,128]{1,0:T(8,128)(2,1)S(1)}, u32[]{:S(2)}, u32[]{:S(2)}) collective-permute-start(bf16[64,128]{1,0:T(8,128)(2,1)S(1)} %get-tuple-element.51), channel_id=1, source_target_pairs={{0,64},{16,80},{32,96},{48,112},{64,128},{80,144},{96,160},{112,17... | collective-permute-start | bytes 49160 | tf_op jit(solution)/shard_map/ppermute | solution.py:242
  78.1 1.3 collective-permute-start.5
  79.4 2.3 %copy.45 = bf16[1,2048,224]{2,1,0:T(8,128)(2,1)} copy(bf16[1,2048,224]{1,2,0:T(8,128)(2,1)} %param.24) | data formatting | bytes 1835008 | tf_op args[11]
  81.7 2.2 %copy.44 = bf16[1,2048,224]{2,1,0:T(8,128)(2,1)} copy(bf16[1,2048,224]{1,2,0:T(8,128)(2,1)} %param.23) | data formatting | bytes 1835008 | tf_op args[10]
  84.0 0.0 collective-permute-done.4.arrived_f_ref
  84.0 0.6 copy-done.6
  84.6 0.0 copy-done.10
  84.6 1.9 %scan_step.6 = (f32[2,64,128]{2,1,0:T(8,128)}, bf16[2,64,128]{2,1,0:T(8,128)(2,1)}) custom-call(bf16[64,128]{1,0:T(8,128)(2,1)} %copy-done.6, bf16[64,128]{1,0:T(8,128)(2,1)} %copy-done.10, f32[2,64,128]{2,1,0:T(8,128)} %get-tuple-element.30.past_ref, bf16[2,64,128]{2,1,0:T(8,128)(2,1)} %get-tuple-element.26.own_ref), custom_call_target="tpu_custom_call" | custom-call | flops 16777216 | bytes 196608 | tf_op jit(solution)/shard_map/scan_step/pallas_call | solution.py:199
  86.5 9.2 %all-to-all-done.1.rows_ref = bf16[16,768,128]{2,1,0:T(8,128)(2,1)S(1)} async-done(((bf16[16,768,128]{2,1,0:T(8,128)(2,1)}), bf16[16,768,128]{2,1,0:T(8,128)(2,1)S(1)}, u32[]{:S(2)}, u32[]{:S(2)}) %all-to-all-start.1) | async-done | bytes 3145760 | tf_op jit(solution)/shard_map/all_to_all | solution.py:292
  95.7 1.7 copy-done
  97.4 6.9 %expert_rows.1 = bf16[16,768,128]{2,1,0:T(8,128)(2,1)} custom-call(bf16[16,768,128]{2,1,0:T(8,128)(2,1)} %copy-done, bf16[2048,224]{1,0:T(8,128)(2,1)} %bitcast.51, bf16[2048,224]{1,0:T(8,128)(2,1)} %bitcast.50, bf16[224,2048]{1,0:T(8,128)(2,1)} %bitcast.52), custom_call_target="tpu_custom_call" | custom-call | flops 2113929216 | bytes 9043968 | tf_op jit(solution)/shard_map/expert_rows/pallas_call | solution.py:261
  104.3 3.9 %all-to-all-start.2 = ((bf16[16,768,128]{2,1,0:T(8,128)(2,1)}), bf16[16,768,128]{2,1,0:T(8,128)(2,1)S(1)}, u32[]{:S(2)}, u32[]{:S(2)}) async-start(bf16[16,768,128]{2,1,0:T(8,128)(2,1)} %expert_rows.1), calls=%async_computation.2 | async-start | bytes 6291456 | tf_op jit(solution)/shard_map/all_to_all | solution.py:292
  108.2 7.4 %collective-permute-start.6 = (bf16[64,128]{1,0:T(8,128)(2,1)S(1)}, bf16[64,128]{1,0:T(8,128)(2,1)S(1)}, u32[]{:S(2)}, u32[]{:S(2)}) collective-permute-start(bf16[64,128]{1,0:T(8,128)(2,1)S(1)} %get-tuple-element.49), channel_id=1, source_target_pairs={{0,128},{16,144},{32,160},{48,176},{64,192},{80,208},{96,224},{112... | collective-permute-start | bytes 49160 | tf_op jit(solution)/shard_map/ppermute | solution.py:242
  115.6 1.3 collective-permute-start.7
  117.0 7.1 %collective-permute-done.7.arrived_b_ref = bf16[64,128]{1,0:T(8,128)(2,1)S(1)} collective-permute-done((bf16[64,128]{1,0:T(8,128)(2,1)S(1)}, bf16[64,128]{1,0:T(8,128)(2,1)S(1)}, u32[]{:S(2)}, u32[]{:S(2)}) %collective-permute-start.7) | collective-permute-done | bytes 16416 | tf_op jit(solution)/shard_map/ppermute | solution.py:242
  124.0 0.6 copy-done.13
  124.6 1.9 %scan_step.7 = (f32[2,64,128]{2,1,0:T(8,128)}, bf16[2,64,128]{2,1,0:T(8,128)(2,1)}) custom-call(bf16[64,128]{1,0:T(8,128)(2,1)} %copy-done.9, bf16[64,128]{1,0:T(8,128)(2,1)} %copy-done.13, f32[2,64,128]{2,1,0:T(8,128)} %get-tuple-element.38.past_ref, bf16[2,64,128]{2,1,0:T(8,128)(2,1)} %get-tuple-element.26.own_ref), custom_call_target="tpu_custom_call" | custom-call | flops 16777216 | bytes 196608 | tf_op jit(solution)/shard_map/scan_step/pallas_call | solution.py:199
  126.6 0.7 slice_bitcast_fusion
  127.3 7.7 %collective-permute-start.8 = (bf16[64,128]{1,0:T(8,128)(2,1)S(1)}, bf16[64,128]{1,0:T(8,128)(2,1)S(1)}, u32[]{:S(2)}, u32[]{:S(2)}) collective-permute-start(bf16[64,128]{1,0:T(8,128)(2,1)S(1)} %get-tuple-element.47), channel_id=1, source_target_pairs={{0,256},{16,272},{32,288},{48,304},{64,320},{80,336},{96,352},{112... | collective-permute-start | bytes 49160 | tf_op jit(solution)/shard_map/ppermute | solution.py:242
  135.0 0.0 copy-start.15
  135.1 0.0 copy-start.14
  135.1 1.3 collective-permute-start.9
  136.4 0.0 collective-permute-done.8.arrived_f_ref
  136.4 11.9 %collective-permute-done.9.arrived_b_ref = bf16[64,128]{1,0:T(8,128)(2,1)S(1)} collective-permute-done((bf16[64,128]{1,0:T(8,128)(2,1)S(1)}, bf16[64,128]{1,0:T(8,128)(2,1)S(1)}, u32[]{:S(2)}, u32[]{:S(2)}) %collective-permute-start.9) | collective-permute-done | bytes 16416 | tf_op jit(solution)/shard_map/ppermute | solution.py:242
  148.3 0.7 all-to-all-done.2
  149.0 1.1 reduce_sum.52
  150.2 18.2 %all-to-all-start.3 = ((bf16[32,24,128]{2,1,0:T(8,128)(2,1)}), bf16[32,24,128]{2,1,0:T(8,128)(2,1)S(1)}, u32[]{:S(2)}, u32[]{:S(2)}) async-start(bf16[32,24,128]{2,1,0:T(8,128)(2,1)} %bitcast.17), calls=%async_computation.3 | async-start | bytes 393216 | tf_op jit(solution)/shard_map/all_to_all | solution.py:292
  168.4 0.7 copy.46.gain_ref
  169.1 0.2 select_reduce_fusion
  169.3 2.3 %mixer_finish.1 = bf16[64,1024]{1,0:T(8,128)(2,1)} custom-call(bf16[64,128]{1,0:T(8,128)(2,1)} %copy-done.4, bf16[64,128]{1,0:T(8,128)(2,1)} %copy-done.5, f32[2,64,128]{2,1,0:T(8,128)} %get-tuple-element.42.past_ref, f32[64,1024]{1,0:T(8,128)} %get-tuple-element.43.oloc_ref, bf16[128,1024]{1,0:T(8,128)(2,1)} %get-tuple-element.44.qp_ref, f32[64,1]{1,0:T(8,128)} %copy.46.gain_ref), custom_call_target="tpu_custom_call" | custom-call | flops 41943040 | bytes 1048576 | tf_op jit(solution)/shard_map/mixer_finish/pallas_call | solution.py:228
  171.6 15.6 %all-to-all-done.3 = bf16[32,24,128]{2,1,0:T(8,128)(2,1)S(1)} async-done(((bf16[32,24,128]{2,1,0:T(8,128)(2,1)}), bf16[32,24,128]{2,1,0:T(8,128)(2,1)S(1)}, u32[]{:S(2)}, u32[]{:S(2)}) %all-to-all-start.3) | async-done | bytes 196640 | tf_op jit(solution)/shard_map/all_to_all | solution.py:292
  187.2 0.9 fusion.9
  (33 shorter events, 0.1 us)
Async XLA Ops:
  0.6 4.0 %copy-start.1 = (bf16[256,2048]{1,0:T(8,128)(2,1)S(1)}, bf16[256,2048]{1,0:T(8,128)(2,1)}, u32[]{:S(2)}) copy-start(bf16[256,2048]{1,0:T(8,128)(2,1)} %param.19) | copy-start | bytes 3145732
  6.7 35.5 %all-to-all-start = ((bf16[32,24,128]{2,1,0:T(8,128)(2,1)}), bf16[32,24,128]{2,1,0:T(8,128)(2,1)S(1)}, u32[]{:S(2)}, u32[]{:S(2)}) async-start(bf16[32,24,128]{2,1,0:T(8,128)(2,1)} %bitcast.1), calls=%async_computation | async-start | bytes 393216 | tf_op jit(solution)/shard_map/all_to_all | solution.py:292
  44.5 6.9 %copy-start.2 = (bf16[2,64,128]{2,1,0:T(8,128)(2,1)S(1)}, bf16[2,64,128]{2,1,0:T(8,128)(2,1)}, u32[]{:S(2)}) copy-start(bf16[2,64,128]{2,1,0:T(8,128)(2,1)} %get-tuple-element.26.own_ref) | copy-start | bytes 98308
  44.5 51.2 %all-to-all-start.1 = ((bf16[16,768,128]{2,1,0:T(8,128)(2,1)}), bf16[16,768,128]{2,1,0:T(8,128)(2,1)S(1)}, u32[]{:S(2)}, u32[]{:S(2)}) async-start(bf16[16,768,128]{2,1,0:T(8,128)(2,1)} %broadcast_in_dim.6), calls=%async_computation.1 | async-start | bytes 6291456 | tf_op jit(solution)/shard_map/all_to_all | solution.py:292
  51.4 5.3 %collective-permute-start = (bf16[64,128]{1,0:T(8,128)(2,1)S(1)}, bf16[64,128]{1,0:T(8,128)(2,1)S(1)}, u32[]{:S(2)}, u32[]{:S(2)}) collective-permute-start(bf16[64,128]{1,0:T(8,128)(2,1)S(1)} %get-tuple-element.55), channel_id=1, source_target_pairs={{0,16},{16,32},{32,48},{48,64},{64,80},{80,96},{96,112},{112,128},... | collective-permute-start | bytes 49160 | tf_op jit(solution)/shard_map/ppermute | solution.py:242
  54.8 5.4 %collective-permute-start.1 = (bf16[64,128]{1,0:T(8,128)(2,1)S(1)}, bf16[64,128]{1,0:T(8,128)(2,1)S(1)}, u32[]{:S(2)}, u32[]{:S(2)}) collective-permute-start(bf16[64,128]{1,0:T(8,128)(2,1)S(1)} %get-tuple-element.54), channel_id=1, source_target_pairs={{16,0},{32,16},{48,32},{64,48},{80,64},{96,80},{112,96},{128,112},... | collective-permute-start | bytes 49160 | tf_op jit(solution)/shard_map/ppermute | solution.py:242
  56.7 4.1 %copy-start.7 = (bf16[64,128]{1,0:T(8,128)(2,1)}, bf16[64,128]{1,0:T(8,128)(2,1)S(1)}, u32[]{:S(2)}) copy-start(bf16[64,128]{1,0:T(8,128)(2,1)S(1)} %collective-permute-done.arrived_f_ref) | copy-start | bytes 49156
  60.2 0.6 copy-start.11
  63.5 3.0 %collective-permute-start.2 = (bf16[64,128]{1,0:T(8,128)(2,1)S(1)}, bf16[64,128]{1,0:T(8,128)(2,1)S(1)}, u32[]{:S(2)}, u32[]{:S(2)}) collective-permute-start(bf16[64,128]{1,0:T(8,128)(2,1)S(1)} %get-tuple-element.53), channel_id=1, source_target_pairs={{0,32},{16,48},{32,64},{48,80},{64,96},{80,112},{96,128},{112,144}... | collective-permute-start | bytes 49160 | tf_op jit(solution)/shard_map/ppermute | solution.py:242
  65.1 4.8 %collective-permute-start.3 = (bf16[64,128]{1,0:T(8,128)(2,1)S(1)}, bf16[64,128]{1,0:T(8,128)(2,1)S(1)}, u32[]{:S(2)}, u32[]{:S(2)}) collective-permute-start(bf16[64,128]{1,0:T(8,128)(2,1)S(1)} %get-tuple-element.52), channel_id=1, source_target_pairs={{32,0},{48,16},{64,32},{80,48},{96,64},{112,80},{128,96},{144,112}... | collective-permute-start | bytes 49160 | tf_op jit(solution)/shard_map/ppermute | solution.py:242
  66.5 3.5 %copy-start.8 = (bf16[64,128]{1,0:T(8,128)(2,1)}, bf16[64,128]{1,0:T(8,128)(2,1)S(1)}, u32[]{:S(2)}) copy-start(bf16[64,128]{1,0:T(8,128)(2,1)S(1)} %collective-permute-done.2.arrived_f_ref) | copy-start | bytes 49156
  69.9 0.6 copy-start.12
  73.2 10.8 %collective-permute-start.4 = (bf16[64,128]{1,0:T(8,128)(2,1)S(1)}, bf16[64,128]{1,0:T(8,128)(2,1)S(1)}, u32[]{:S(2)}, u32[]{:S(2)}) collective-permute-start(bf16[64,128]{1,0:T(8,128)(2,1)S(1)} %get-tuple-element.51), channel_id=1, source_target_pairs={{0,64},{16,80},{32,96},{48,112},{64,128},{80,144},{96,160},{112,17... | collective-permute-start | bytes 49160 | tf_op jit(solution)/shard_map/ppermute | solution.py:242
  78.1 5.8 %collective-permute-start.5 = (bf16[64,128]{1,0:T(8,128)(2,1)S(1)}, bf16[64,128]{1,0:T(8,128)(2,1)S(1)}, u32[]{:S(2)}, u32[]{:S(2)}) collective-permute-start(bf16[64,128]{1,0:T(8,128)(2,1)S(1)} %get-tuple-element.50), channel_id=1, source_target_pairs={{64,0},{80,16},{96,32},{112,48},{128,64},{144,80},{160,96},{176,11... | collective-permute-start | bytes 49160 | tf_op jit(solution)/shard_map/ppermute | solution.py:242
  84.0 0.6 copy-start.6
  84.0 0.6 copy-start.10
  95.7 1.7 copy-start
  104.3 3.9 %copy-start.3 = (bf16[2,64,128]{2,1,0:T(8,128)(2,1)S(1)}, bf16[2,64,128]{2,1,0:T(8,128)(2,1)}, u32[]{:S(2)}) copy-start(bf16[2,64,128]{2,1,0:T(8,128)(2,1)} %get-tuple-element.37) | copy-start | bytes 98308
  104.3 44.7 %all-to-all-start.2 = ((bf16[16,768,128]{2,1,0:T(8,128)(2,1)}), bf16[16,768,128]{2,1,0:T(8,128)(2,1)S(1)}, u32[]{:S(2)}, u32[]{:S(2)}) async-start(bf16[16,768,128]{2,1,0:T(8,128)(2,1)} %expert_rows.1), calls=%async_computation.2 | async-start | bytes 6291456 | tf_op jit(solution)/shard_map/all_to_all | solution.py:292
  108.2 8.7 %collective-permute-start.6 = (bf16[64,128]{1,0:T(8,128)(2,1)S(1)}, bf16[64,128]{1,0:T(8,128)(2,1)S(1)}, u32[]{:S(2)}, u32[]{:S(2)}) collective-permute-start(bf16[64,128]{1,0:T(8,128)(2,1)S(1)} %get-tuple-element.49), channel_id=1, source_target_pairs={{0,128},{16,144},{32,160},{48,176},{64,192},{80,208},{96,224},{112... | collective-permute-start | bytes 49160 | tf_op jit(solution)/shard_map/ppermute | solution.py:242
  115.6 8.4 %collective-permute-start.7 = (bf16[64,128]{1,0:T(8,128)(2,1)S(1)}, bf16[64,128]{1,0:T(8,128)(2,1)S(1)}, u32[]{:S(2)}, u32[]{:S(2)}) collective-permute-start(bf16[64,128]{1,0:T(8,128)(2,1)S(1)} %get-tuple-element.48), channel_id=1, source_target_pairs={{128,0},{144,16},{160,32},{176,48},{192,64},{208,80},{224,96},{240... | collective-permute-start | bytes 49160 | tf_op jit(solution)/shard_map/ppermute | solution.py:242
  117.0 7.1 %copy-start.9 = (bf16[64,128]{1,0:T(8,128)(2,1)}, bf16[64,128]{1,0:T(8,128)(2,1)S(1)}, u32[]{:S(2)}) copy-start(bf16[64,128]{1,0:T(8,128)(2,1)S(1)} %collective-permute-done.6.arrived_f_ref) | copy-start | bytes 49156
  124.0 0.6 copy-start.13
  127.3 9.1 %collective-permute-start.8 = (bf16[64,128]{1,0:T(8,128)(2,1)S(1)}, bf16[64,128]{1,0:T(8,128)(2,1)S(1)}, u32[]{:S(2)}, u32[]{:S(2)}) collective-permute-start(bf16[64,128]{1,0:T(8,128)(2,1)S(1)} %get-tuple-element.47), channel_id=1, source_target_pairs={{0,256},{16,272},{32,288},{48,304},{64,320},{80,336},{96,352},{112... | collective-permute-start | bytes 49160 | tf_op jit(solution)/shard_map/ppermute | solution.py:242
  135.0 33.3 %copy-start.15 = (f32[64]{0:T(128)S(1)}, f32[64]{0:T(128)}, u32[]{:S(2)}) copy-start(f32[64]{0:T(128)} %param.18) | copy-start | bytes 772
  135.1 34.1 %copy-start.14 = (f32[256,2]{0,1:T(2,128)S(1)}, f32[256,2]{0,1:T(2,128)}, u32[]{:S(2)}) copy-start(f32[256,2]{0,1:T(2,128)} %param.22) | copy-start | bytes 6148
  135.1 13.2 %collective-permute-start.9 = (bf16[64,128]{1,0:T(8,128)(2,1)S(1)}, bf16[64,128]{1,0:T(8,128)(2,1)S(1)}, u32[]{:S(2)}, u32[]{:S(2)}) collective-permute-start(bf16[64,128]{1,0:T(8,128)(2,1)S(1)} %get-tuple-element.46), channel_id=1, source_target_pairs={{256,0},{272,16},{288,32},{304,48},{320,64},{336,80},{352,96},{368... | collective-permute-start | bytes 49160 | tf_op jit(solution)/shard_map/ppermute | solution.py:242
  136.4 13.8 %copy-start.4 = (bf16[64,128]{1,0:T(8,128)(2,1)}, bf16[64,128]{1,0:T(8,128)(2,1)S(1)}, u32[]{:S(2)}) copy-start(bf16[64,128]{1,0:T(8,128)(2,1)S(1)} %collective-permute-done.8.arrived_f_ref) | copy-start | bytes 49156
  148.3 1.9 %copy-start.5 = (bf16[64,128]{1,0:T(8,128)(2,1)}, bf16[64,128]{1,0:T(8,128)(2,1)S(1)}, u32[]{:S(2)}) copy-start(bf16[64,128]{1,0:T(8,128)(2,1)S(1)} %collective-permute-done.9.arrived_b_ref) | copy-start | bytes 49156
  150.2 37.0 %all-to-all-start.3 = ((bf16[32,24,128]{2,1,0:T(8,128)(2,1)}), bf16[32,24,128]{2,1,0:T(8,128)(2,1)S(1)}, u32[]{:S(2)}, u32[]{:S(2)}) async-start(bf16[32,24,128]{2,1,0:T(8,128)(2,1)} %bitcast.17), calls=%async_computation.3 | async-start | bytes 393216 | tf_op jit(solution)/shard_map/all_to_all | solution.py:292

commit v2 on v1

--- a/solution.py
+++ b/solution.py
@@ -170,6 +170,7 @@
         cost_estimate=pl.CostEstimate(
             flops=16 * 22 * 2 * 128**3, bytes_accessed=tokens * 64 * 18, transcendentals=tokens * 64 * 9
         ),
+        compiler_params=pltpu.CompilerParams(vmem_limit_bytes=16 * 2**20),
         name="mixer_local",
     )(query, key, value, erase, decay)
 
@@ -188,33 +189,52 @@
     return first + mm(first, later) + later
 
 
-def step_kernel(arrived_f_ref, arrived_b_ref, past_ref, own_ref, next_past_ref, through_ref):
-    for way, arrived in ((0, arrived_f_ref), (1, arrived_b_ref)):
-        past = composed(stacked(arrived[...]), stacked(past_ref[way]))
-        next_past_ref[way] = widened(past)
-        through_ref[way] = widened(composed(past, stacked(own_ref[way]))).astype(jnp.bfloat16)
-
-
-def scan_step(arrived, past, own):
+def step_kernel(upper_ref, arrived_ref, through_ref, past_ref, next_past_ref, next_through_ref):
+    upper = upper_ref[0] != 0
+    other = [stacked(arrived_ref[way]) for way in (0, 1)]
+    mine = [stacked(through_ref[way]) for way in (0, 1)]
+    near = jnp.where(upper, past_ref[0], past_ref[1])
+    met = widened(composed(jnp.where(upper, other[0], other[1]), stacked(near)))
+    next_past_ref[0] = jnp.where(upper, met, past_ref[0])
+    next_past_ref[1] = jnp.where(upper, past_ref[1], met)
+    for way in (0, 1):
+        other_first = upper if way == 0 else jnp.logical_not(upper)
+        first = jnp.where(other_first, other[way], mine[way])
+        later = jnp.where(other_first, mine[way], other[way])
+        next_through_ref[way] = widened(composed(first, later)).astype(jnp.bfloat16)
+
+
+def in_vmem(count, scalars):
+    return [pl.BlockSpec(memory_space=pltpu.SMEM)] * scalars + [
+        pl.BlockSpec(memory_space=pltpu.VMEM)
+    ] * count
+
+
+def scan_step(upper, arrived, through, past):
     return pl.pallas_call(
         step_kernel,
         out_shape=(
             jax.ShapeDtypeStruct(past.shape, jnp.float32),
             jax.ShapeDtypeStruct(past.shape, jnp.bfloat16),
         ),
+        in_specs=in_vmem(3, 1),
+        out_specs=tuple(in_vmem(2, 0)),
         cost_estimate=pl.CostEstimate(
-            flops=8 * 128**3, bytes_accessed=6 * 2 * past.size, transcendentals=0
-        ),
+            flops=6 * 128**3, bytes_accessed=6 * 2 * past.size, transcendentals=0
+        ),
+        compiler_params=pltpu.CompilerParams(vmem_limit_bytes=4 * 2**20),
         name="scan_step",
-    )(*arrived, past, own)
-
-
-def finish_kernel(arrived_f_ref, arrived_b_ref, past_ref, oloc_ref, qp_ref, gain_ref, out_ref):
-    entering = [
-        composed(stacked(arrived[...]), stacked(past_ref[way]))[HEAD_DIM:]
-        for way, arrived in ((0, arrived_f_ref), (1, arrived_b_ref))
-    ]
-    states = entering[0] + pltpu.roll(entering[1], HEAD_DIM, 1)
+    )(upper, arrived, through, past)
+
+
+def finish_kernel(upper_ref, arrived_ref, past_ref, oloc_ref, qp_ref, gain_ref, out_ref):
+    upper = upper_ref[0] != 0
+    other = jnp.where(upper, arrived_ref[0].astype(jnp.float32), arrived_ref[1].astype(jnp.float32))
+    near = jnp.where(upper, past_ref[0], past_ref[1])
+    met = composed(stacked(other), stacked(near))[HEAD_DIM:]
+    kept = stacked(jnp.where(upper, past_ref[1], past_ref[0]))[HEAD_DIM:]
+    ahead, behind = jnp.where(upper, met, kept), jnp.where(upper, kept, met)
+    states = ahead + pltpu.roll(behind, HEAD_DIM, 1)
     summed = oloc_ref[...] + mm(states, qp_ref[...])
     center = jnp.mean(summed, axis=0, keepdims=True)
     away = summed - center
@@ -224,22 +244,27 @@
     ).astype(jnp.bfloat16)
 
 
-def finish_half(arrived, past, oloc, qp, gain):
+def finish_half(upper, arrived, past, oloc, qp, gain):
     return pl.pallas_call(
         finish_kernel,
         out_shape=jax.ShapeDtypeStruct(oloc.shape, jnp.bfloat16),
+        in_specs=in_vmem(5, 1),
+        out_specs=in_vmem(1, 0)[0],
         cost_estimate=pl.CostEstimate(
             flops=4 * 128**3 + 16 * 128**3, bytes_accessed=2**20, transcendentals=1024
         ),
+        compiler_params=pltpu.CompilerParams(vmem_limit_bytes=8 * 2**20),
         name="mixer_finish",
-    )(*arrived, past, oloc, qp, gain)
-
-
-def passed_on(through, distance):
+    )(upper, arrived, past, oloc, qp, gain)
+
+
+def swapped(through, distance):
     count = lax.axis_size("ep")
-    ahead = [(i, i + distance) for i in range(count - distance)]
-    back = [(i + distance, i) for i in range(count - distance)]
-    return lax.ppermute(through[0], "ep", ahead), lax.ppermute(through[1], "ep", back)
+    return lax.ppermute(through, "ep", [(i, i ^ distance) for i in range(count)])
+
+
+def side(distance):
+    return (lax.axis_index("ep") & distance).reshape(1).astype(jnp.int32)
 
 
 def expert_kernel(rows_ref, gate_ref, up_ref, down_ref, out_ref):
@@ -269,6 +294,7 @@
             bytes_accessed=2 * (2 * rows.size + 3 * gate.size),
             transcendentals=total * gate.shape[1],
         ),
+        compiler_params=pltpu.CompilerParams(vmem_limit_bytes=63600000),
         name="expert_rows",
     )(rows, gate, up, down)
 
@@ -328,25 +354,24 @@
     arrived, own_maps = lax.optimization_barrier((arrived, own_maps))
     shared = spread(jnp.broadcast_to(arrived[None], (shares, *arrived.shape)), "tp")
 
-    past = jnp.zeros(own_maps.shape, jnp.float32)
-    through, distance = own_maps, 1
+    past, through, distance = jnp.zeros(own_maps.shape, jnp.float32), own_maps, 1
     while distance < experts_n // 4:
-        past, through = scan_step(passed_on(through, distance), past, own_maps)
+        past, through = scan_step(side(distance), swapped(through, distance), through, past)
         distance *= 2
     shared, past, through = lax.optimization_barrier((shared, past, through))
     partial = expert_rows(shared, gate_weight[0], up_weight[0], down_weight[0])
     partial, past, through = lax.optimization_barrier((partial, past, through))
     while distance < experts_n // 2:
-        past, through = scan_step(passed_on(through, distance), past, own_maps)
+        past, through = scan_step(side(distance), swapped(through, distance), through, past)
         distance *= 2
-    crossing = passed_on(through, distance)
+    crossing = swapped(through, distance)
     pieces = spread(partial, "tp")
     pieces, crossing = lax.optimization_barrier((pieces, crossing))
     summed = jnp.sum(pieces.astype(jnp.float32), axis=0).astype(jnp.bfloat16)
     returned = spread(summed.reshape(experts_n, capacity, col_count), "ep").reshape(
         slot_total, col_count
     )
-    mixer_out = finish_half(crossing, past, oloc, qp, mix_gain[:, None])
+    mixer_out = finish_half(side(distance), crossing, past, oloc, qp, mix_gain[:, None])
     matches = targets[:, :, None] == jnp.arange(slot_total, dtype=jnp.int32)[None, None, :]
     combine = jnp.sum(matches.astype(jnp.float32) * route_weight[:, :, None], axis=1)
     expert_out = jnp.dot(combine, returned.astype(jnp.float32)).astype(jnp.bfloat16)

time: 189 us -> 188 us (level)
  waiting for transfers between devices: 54.7 us -> 78 us
  Pallas kernels: 32.3 us -> 22.8 us
  local copies, waits for them, and re-layouts: 16.3 us -> 7.48 us
  starting transfers between devices: 77.9 us -> 70.5 us
  other arithmetic: 4.01 us -> 5.91 us
    all_to_all x4, waiting for transfers between devices: 28.9 us -> 66.7 us  [spread(): return lax.all_to_all(array, axis, 0, 0, tiled=True)]
    ppermute x10 -> x5, waiting for transfers between devices: 25.8 us -> 11.3 us  [swapped(): lax.ppermute(through, 'ep', [(i, i ^ distance) for i in range(count)])]
    ppermute x10 -> x5, starting transfers between devices: 32.2 us -> 25.6 us  [swapped(): lax.ppermute(through, 'ep', [(i, i ^ distance) for i in range(count)])]
    pallas_call x4, Pallas kernels: 7.76 us -> 1.29 us  [scan_step(): pl.pallas_call(step_kernel, out_shape=(jax.ShapeDtypeStruct(past.shape, j...]
    unnamed x35 -> x23, local copies, waits for them, and re-layouts: 8.95 us -> 3.6 us
    squeeze x5 -> x0, local copies, waits for them, and re-layouts: 2.22 us -> none  [passed_on(): through[1]]
    pallas_call x1, Pallas kernels: 15.4 us -> 13.4 us  [local_half(): pl.pallas_call(local_kernel, out_shape=(full(jnp.float32), jax.ShapeDtype...]
    reduce_sum x1, other arithmetic: 1.14 us -> 3.05 us  [on_device(): summed = jnp.sum(pieces.astype(jnp.float32), axis=0).astype(jnp.bfloat16)]
  transfers between devices with their start and end apart: 14 -> 9, of which waited for: 8 -> 9; matrix products, arithmetic and copies ran while one was open for 4% -> 2% of each run, Pallas kernels for 14% -> 8%
where the time goes in v2:
time: 188 us
  waiting for transfers between devices  78 us (41%)
  starting transfers between devices  70.5 us (38%)
  Pallas kernels  22.8 us (12%)
  local copies, waits for them, and re-layouts  7.48 us (4%)
  other arithmetic  5.91 us (3%)
    all_to_all x4, waiting for transfers between devices, spread(): return lax.all_to_all(array, axis, 0, 0, tiled=True)  66.7 us
    all_to_all x4, starting transfers between devices, spread(): return lax.all_to_all(array, axis, 0, 0, tiled=True)  44.9 us
    ppermute x5, starting transfers between devices, swapped(): lax.ppermute(through, 'ep', [(i, i ^ distance) for i in range(count)])  25.6 us
    pallas_call x1, Pallas kernels, local_half(): pl.pallas_call(local_kernel, out_shape=(full(jnp.float32), jax.ShapeDtype...  13.4 us
    ppermute x5, waiting for transfers between devices, swapped(): lax.ppermute(through, 'ep', [(i, i ^ distance) for i in range(count)])  11.3 us
    pallas_call x1, Pallas kernels, expert_rows(): pl.pallas_call(expert_kernel, grid=(total // tile,), in_specs=[block, fix...  6.93 us
  transfers between devices with their start and end apart: 9, of which 9 were waited for; matrix products, arithmetic and copies ran while one was open for 2% of the time, Pallas kernels for 8%

profile of v2, /device:TPU:1, one launch (start us, length us, event | category | flops | bytes accessed | tf_op | source)
XLA Modules:
  0.0 187.6 jit_solution(9987040145777066722)
XLA Ops:
  0.6 0.0 copy-start.5
  0.6 0.9 copy.40
  1.5 0.1 eq.56
  1.7 0.1 eq.52
  1.8 0.0 copy-start
  1.8 0.0 copy-start.1
  1.9 0.0 copy-start.2
  1.9 0.0 copy-start.3
  1.9 0.0 copy-start.4
  1.9 1.2 reduce-window.6
  3.1 0.2 slice_reduce_fusion
  3.4 0.1 fusion.3
  3.5 0.1 reshape.67
  3.6 0.1 copy.43
  3.7 0.7 multiply_add_fusion
  4.4 0.3 convert_reduce_fusion
  4.7 0.0 copy-done.5
  4.7 0.3 multiply_reduce_fusion
  5.0 0.8 dynamic_slice.7
  5.8 1.0 convolution_convert_fusion
  6.8 16.7 %all-to-all-start = ((bf16[32,24,128]{2,1,0:T(8,128)(2,1)}), bf16[32,24,128]{2,1,0:T(8,128)(2,1)S(1)}, u32[]{:S(2)}, u32[]{:S(2)}) async-start(bf16[32,24,128]{2,1,0:T(8,128)(2,1)} %bitcast.2), calls=%async_computation | async-start | bytes 393216 | tf_op jit(solution)/shard_map/all_to_all | solution.py:318
  23.5 0.0 copy-done
  23.6 0.0 copy-done.1
  23.6 0.0 copy-done.2
  23.6 0.0 copy-done.3
  23.6 0.0 copy-done.4
  23.6 13.4 %mixer_local.1 = (f32[64,1024]{1,0:T(8,128)S(1)}, bf16[128,1024]{1,0:T(8,128)(2,1)S(1)}, bf16[2,64,128]{2,1,0:T(8,128)(2,1)S(1)}) custom-call(bf16[64,1024]{1,0:T(8,128)(2,1)S(1)} %copy-done, bf16[64,1024]{1,0:T(8,128)(2,1)S(1)} %copy-done.1, bf16[64,1024]{1,0:T(8,128)(2,1)S(1)} %copy-done.2, bf16[64,1024]{1,0:T(8,128)(2,1)S(1)} %copy-done.3, ...), custom_call_target="tpu_custom_call" | custom-call | flops 1476395008 | bytes 1179648 | tf_op jit(solution)/shard_map/mixer_local/pallas_call | solution.py:153
  37.0 5.3 %all-to-all-done = bf16[32,24,128]{2,1,0:T(8,128)(2,1)S(1)} async-done(((bf16[32,24,128]{2,1,0:T(8,128)(2,1)}), bf16[32,24,128]{2,1,0:T(8,128)(2,1)S(1)}, u32[]{:S(2)}, u32[]{:S(2)}) %all-to-all-start) | async-done | bytes 196640 | tf_op jit(solution)/shard_map/all_to_all | solution.py:318
  42.3 2.3 %broadcast_in_dim.6 = bf16[16,768,128]{2,1,0:T(8,128)(2,1)} broadcast(bf16[768,128]{1,0:T(8,128)(2,1)S(1)} %bitcast.38), dimensions={1,2} | broadcast | bytes 3342336 | tf_op jit(solution)/shard_map/broadcast_in_dim | solution.py:355
  44.6 6.9 %all-to-all-start.1 = ((bf16[16,768,128]{2,1,0:T(8,128)(2,1)}), bf16[16,768,128]{2,1,0:T(8,128)(2,1)}, u32[]{:S(2)}, u32[]{:S(2)}) async-start(bf16[16,768,128]{2,1,0:T(8,128)(2,1)} %broadcast_in_dim.6), calls=%async_computation.1 | async-start | bytes 6291456 | tf_op jit(solution)/shard_map/all_to_all | solution.py:318
  51.6 0.0 copy-start.7
  51.6 3.8 %collective-permute-start = (bf16[2,64,128]{2,1,0:T(8,128)(2,1)S(1)}, bf16[2,64,128]{2,1,0:T(8,128)(2,1)S(1)}, u32[]{:S(2)}, u32[]{:S(2)}) collective-permute-start(bf16[2,64,128]{2,1,0:T(8,128)(2,1)S(1)} %get-tuple-element.25.through_ref), channel_id=1, source_target_pairs={{0,16},{16,0},{32,48},{48,32},{64,80},{80,64},{96,112},{112,96},{1... | collective-permute-start | bytes 98312 | tf_op jit(solution)/shard_map/ppermute | solution.py:263
  55.3 0.8 collective-permute-done.arrived_ref
  56.2 0.3 scan_step.4
  56.5 1.9 %collective-permute-start.1 = (bf16[2,64,128]{2,1,0:T(8,128)(2,1)S(1)}, bf16[2,64,128]{2,1,0:T(8,128)(2,1)S(1)}, u32[]{:S(2)}, u32[]{:S(2)}) collective-permute-start(bf16[2,64,128]{2,1,0:T(8,128)(2,1)S(1)} %get-tuple-element.26.through_ref), channel_id=1, source_target_pairs={{0,32},{16,48},{32,0},{48,16},{64,96},{80,112},{96,64},{112,80},{1... | collective-permute-start | bytes 98312 | tf_op jit(solution)/shard_map/ppermute | solution.py:263
  58.4 3.1 %collective-permute-done.1.arrived_ref = bf16[2,64,128]{2,1,0:T(8,128)(2,1)S(1)} collective-permute-done((bf16[2,64,128]{2,1,0:T(8,128)(2,1)S(1)}, bf16[2,64,128]{2,1,0:T(8,128)(2,1)S(1)}, u32[]{:S(2)}, u32[]{:S(2)}) %collective-permute-start.1) | collective-permute-done | bytes 32800 | tf_op jit(solution)/shard_map/ppermute | solution.py:263
  61.6 0.3 scan_step.5
  61.9 1.9 %collective-permute-start.2 = (bf16[2,64,128]{2,1,0:T(8,128)(2,1)S(1)}, bf16[2,64,128]{2,1,0:T(8,128)(2,1)S(1)}, u32[]{:S(2)}, u32[]{:S(2)}) collective-permute-start(bf16[2,64,128]{2,1,0:T(8,128)(2,1)S(1)} %get-tuple-element.28.through_ref), channel_id=1, source_target_pairs={{0,64},{16,80},{32,96},{48,112},{64,0},{80,16},{96,32},{112,48},{1... | collective-permute-start | bytes 98312 | tf_op jit(solution)/shard_map/ppermute | solution.py:263
  63.8 0.0 copy-done.6
  63.8 1.3 copy.44
  65.2 0.0 copy-done.7
  65.2 1.3 copy.45
  66.5 1.4 collective-permute-done.2.arrived_ref
  67.9 0.3 scan_step.6
  68.3 27.6 %all-to-all-done.1.rows_ref = bf16[16,768,128]{2,1,0:T(8,128)(2,1)} async-done(((bf16[16,768,128]{2,1,0:T(8,128)(2,1)}), bf16[16,768,128]{2,1,0:T(8,128)(2,1)}, u32[]{:S(2)}, u32[]{:S(2)}) %all-to-all-start.1) | async-done | bytes 3145760 | tf_op jit(solution)/shard_map/all_to_all | solution.py:318
  95.9 6.9 %expert_rows.1 = bf16[16,768,128]{2,1,0:T(8,128)(2,1)} custom-call(bf16[16,768,128]{2,1,0:T(8,128)(2,1)} %all-to-all-done.1.rows_ref, bf16[2048,224]{1,0:T(8,128)(2,1)} %bitcast.35, bf16[2048,224]{1,0:T(8,128)(2,1)} %bitcast.36, bf16[224,2048]{1,0:T(8,128)(2,1)} %bitcast.37), custom_call_target="tpu_custom_call" | custom-call | flops 2113929216 | bytes 9043968 | tf_op jit(solution)/shard_map/expert_rows/pallas_call | solution.py:286
  102.8 4.5 %all-to-all-start.2 = ((bf16[16,768,128]{2,1,0:T(8,128)(2,1)}), bf16[16,768,128]{2,1,0:T(8,128)(2,1)}, u32[]{:S(2)}, u32[]{:S(2)}) async-start(bf16[16,768,128]{2,1,0:T(8,128)(2,1)} %expert_rows.1), calls=%async_computation.2 | async-start | bytes 6291456 | tf_op jit(solution)/shard_map/all_to_all | solution.py:318
  107.3 8.4 %collective-permute-start.3 = (bf16[2,64,128]{2,1,0:T(8,128)(2,1)S(1)}, bf16[2,64,128]{2,1,0:T(8,128)(2,1)S(1)}, u32[]{:S(2)}, u32[]{:S(2)}) collective-permute-start(bf16[2,64,128]{2,1,0:T(8,128)(2,1)S(1)} %get-tuple-element.36.through_ref), channel_id=1, source_target_pairs={{0,128},{16,144},{32,160},{48,176},{64,192},{80,208},{96,224},{112... | collective-permute-start | bytes 98312 | tf_op jit(solution)/shard_map/ppermute | solution.py:263
  115.7 2.0 %collective-permute-done.3.arrived_ref = bf16[2,64,128]{2,1,0:T(8,128)(2,1)S(1)} collective-permute-done((bf16[2,64,128]{2,1,0:T(8,128)(2,1)S(1)}, bf16[2,64,128]{2,1,0:T(8,128)(2,1)S(1)}, u32[]{:S(2)}, u32[]{:S(2)}) %collective-permute-start.3) | collective-permute-done | bytes 32800 | tf_op jit(solution)/shard_map/ppermute | solution.py:263
  117.8 0.3 scan_step.7
  118.1 0.0 copy-start.9
  118.1 0.0 copy-start.8
  118.1 9.6 %collective-permute-start.4 = (bf16[2,64,128]{2,1,0:T(8,128)(2,1)S(1)}, bf16[2,64,128]{2,1,0:T(8,128)(2,1)S(1)}, u32[]{:S(2)}, u32[]{:S(2)}) collective-permute-start(bf16[2,64,128]{2,1,0:T(8,128)(2,1)S(1)} %get-tuple-element.38), channel_id=1, source_target_pairs={{0,256},{16,272},{32,288},{48,304},{64,320},{80,336},{96,352},{112... | collective-permute-start | bytes 98312 | tf_op jit(solution)/shard_map/ppermute | solution.py:263
  127.7 3.9 %collective-permute-done.4.arrived_ref = bf16[2,64,128]{2,1,0:T(8,128)(2,1)S(1)} collective-permute-done((bf16[2,64,128]{2,1,0:T(8,128)(2,1)S(1)}, bf16[2,64,128]{2,1,0:T(8,128)(2,1)S(1)}, u32[]{:S(2)}, u32[]{:S(2)}) %collective-permute-start.4) | collective-permute-done | bytes 32800 | tf_op jit(solution)/shard_map/ppermute | solution.py:263
  131.6 16.5 %all-to-all-done.2 = bf16[16,768,128]{2,1,0:T(8,128)(2,1)} async-done(((bf16[16,768,128]{2,1,0:T(8,128)(2,1)}), bf16[16,768,128]{2,1,0:T(8,128)(2,1)}, u32[]{:S(2)}, u32[]{:S(2)}) %all-to-all-start.2) | async-done | bytes 3145760 | tf_op jit(solution)/shard_map/all_to_all | solution.py:318
  148.1 3.0 %reduce_sum.52 = bf16[768,128]{1,0:T(8,128)(2,1)} reduce(bf16[16,768,128]{2,1,0:T(8,128)(2,1)} %all-to-all-done.2, bf16[]{:T(256)} %constant.41.clone.1), dimensions={0}, to_apply=%region_6.7 | reduce | flops 1474560 | bytes 3342338 | tf_op jit(solution)/shard_map/reduce_sum | solution.py:370
  151.1 16.8 %all-to-all-start.3 = ((bf16[32,24,128]{2,1,0:T(8,128)(2,1)}), bf16[32,24,128]{2,1,0:T(8,128)(2,1)S(1)}, u32[]{:S(2)}, u32[]{:S(2)}) async-start(bf16[32,24,128]{2,1,0:T(8,128)(2,1)} %bitcast.12), calls=%async_computation.3 | async-start | bytes 393216 | tf_op jit(solution)/shard_map/all_to_all | solution.py:318
  167.9 0.0 copy-done.9
  167.9 0.1 copy.46.gain_ref
  168.0 0.0 copy-done.8
  168.0 0.2 select_reduce_fusion
  168.3 1.2 mixer_finish.1
  169.4 17.3 %all-to-all-done.3 = bf16[32,24,128]{2,1,0:T(8,128)(2,1)S(1)} async-done(((bf16[32,24,128]{2,1,0:T(8,128)(2,1)}), bf16[32,24,128]{2,1,0:T(8,128)(2,1)S(1)}, u32[]{:S(2)}, u32[]{:S(2)}) %all-to-all-start.3) | async-done | bytes 196640 | tf_op jit(solution)/shard_map/all_to_all | solution.py:318
  186.7 0.9 fusion.9
  (6 shorter events, 0.1 us)
Async XLA Ops:
  0.6 4.1 %copy-start.5 = (bf16[256,2048]{1,0:T(8,128)(2,1)S(1)}, bf16[256,2048]{1,0:T(8,128)(2,1)}, u32[]{:S(2)}) copy-start(bf16[256,2048]{1,0:T(8,128)(2,1)} %param.19) | copy-start | bytes 3145732
  1.8 21.7 %copy-start = (bf16[64,1024]{1,0:T(8,128)(2,1)S(1)}, bf16[64,1024]{1,0:T(8,128)(2,1)}, u32[]{:S(2)}) copy-start(bf16[64,1024]{1,0:T(8,128)(2,1)} %q_ref.1) | copy-start | bytes 393220
  1.8 21.7 %copy-start.1 = (bf16[64,1024]{1,0:T(8,128)(2,1)S(1)}, bf16[64,1024]{1,0:T(8,128)(2,1)}, u32[]{:S(2)}) copy-start(bf16[64,1024]{1,0:T(8,128)(2,1)} %k_ref.1) | copy-start | bytes 393220
  1.9 21.7 %copy-start.2 = (bf16[64,1024]{1,0:T(8,128)(2,1)S(1)}, bf16[64,1024]{1,0:T(8,128)(2,1)}, u32[]{:S(2)}) copy-start(bf16[64,1024]{1,0:T(8,128)(2,1)} %v_ref.1) | copy-start | bytes 393220
  1.9 21.7 %copy-start.3 = (bf16[64,1024]{1,0:T(8,128)(2,1)S(1)}, bf16[64,1024]{1,0:T(8,128)(2,1)}, u32[]{:S(2)}) copy-start(bf16[64,1024]{1,0:T(8,128)(2,1)} %e_ref.1) | copy-start | bytes 393220
  1.9 21.7 %copy-start.4 = (bf16[64,1024]{1,0:T(8,128)(2,1)S(1)}, bf16[64,1024]{1,0:T(8,128)(2,1)}, u32[]{:S(2)}) copy-start(bf16[64,1024]{1,0:T(8,128)(2,1)} %d_ref.1) | copy-start | bytes 393220
  6.8 35.5 %all-to-all-start = ((bf16[32,24,128]{2,1,0:T(8,128)(2,1)}), bf16[32,24,128]{2,1,0:T(8,128)(2,1)S(1)}, u32[]{:S(2)}, u32[]{:S(2)}) async-start(bf16[32,24,128]{2,1,0:T(8,128)(2,1)} %bitcast.2), calls=%async_computation | async-start | bytes 393216 | tf_op jit(solution)/shard_map/all_to_all | solution.py:318
  44.6 19.2 %copy-start.6 = (bf16[1,2048,224]{1,2,0:T(8,128)(2,1)S(1)}, bf16[1,2048,224]{1,2,0:T(8,128)(2,1)}, u32[]{:S(2)}) copy-start(bf16[1,2048,224]{1,2,0:T(8,128)(2,1)} %param.23) | copy-start | bytes 2752516
  44.6 51.3 %all-to-all-start.1 = ((bf16[16,768,128]{2,1,0:T(8,128)(2,1)}), bf16[16,768,128]{2,1,0:T(8,128)(2,1)}, u32[]{:S(2)}, u32[]{:S(2)}) async-start(bf16[16,768,128]{2,1,0:T(8,128)(2,1)} %broadcast_in_dim.6), calls=%async_computation.1 | async-start | bytes 6291456 | tf_op jit(solution)/shard_map/all_to_all | solution.py:318
  51.6 13.6 %copy-start.7 = (bf16[1,2048,224]{1,2,0:T(8,128)(2,1)S(1)}, bf16[1,2048,224]{1,2,0:T(8,128)(2,1)}, u32[]{:S(2)}) copy-start(bf16[1,2048,224]{1,2,0:T(8,128)(2,1)} %param.24) | copy-start | bytes 2752516
  51.6 4.6 %collective-permute-start = (bf16[2,64,128]{2,1,0:T(8,128)(2,1)S(1)}, bf16[2,64,128]{2,1,0:T(8,128)(2,1)S(1)}, u32[]{:S(2)}, u32[]{:S(2)}) collective-permute-start(bf16[2,64,128]{2,1,0:T(8,128)(2,1)S(1)} %get-tuple-element.25.through_ref), channel_id=1, source_target_pairs={{0,16},{16,0},{32,48},{48,32},{64,80},{80,64},{96,112},{112,96},{1... | collective-permute-start | bytes 98312 | tf_op jit(solution)/shard_map/ppermute | solution.py:263
  56.5 5.1 %collective-permute-start.1 = (bf16[2,64,128]{2,1,0:T(8,128)(2,1)S(1)}, bf16[2,64,128]{2,1,0:T(8,128)(2,1)S(1)}, u32[]{:S(2)}, u32[]{:S(2)}) collective-permute-start(bf16[2,64,128]{2,1,0:T(8,128)(2,1)S(1)} %get-tuple-element.26.through_ref), channel_id=1, source_target_pairs={{0,32},{16,48},{32,0},{48,16},{64,96},{80,112},{96,64},{112,80},{1... | collective-permute-start | bytes 98312 | tf_op jit(solution)/shard_map/ppermute | solution.py:263
  61.9 6.0 %collective-permute-start.2 = (bf16[2,64,128]{2,1,0:T(8,128)(2,1)S(1)}, bf16[2,64,128]{2,1,0:T(8,128)(2,1)S(1)}, u32[]{:S(2)}, u32[]{:S(2)}) collective-permute-start(bf16[2,64,128]{2,1,0:T(8,128)(2,1)S(1)} %get-tuple-element.28.through_ref), channel_id=1, source_target_pairs={{0,64},{16,80},{32,96},{48,112},{64,0},{80,16},{96,32},{112,48},{1... | collective-permute-start | bytes 98312 | tf_op jit(solution)/shard_map/ppermute | solution.py:263
  102.8 45.3 %all-to-all-start.2 = ((bf16[16,768,128]{2,1,0:T(8,128)(2,1)}), bf16[16,768,128]{2,1,0:T(8,128)(2,1)}, u32[]{:S(2)}, u32[]{:S(2)}) async-start(bf16[16,768,128]{2,1,0:T(8,128)(2,1)} %expert_rows.1), calls=%async_computation.2 | async-start | bytes 6291456 | tf_op jit(solution)/shard_map/all_to_all | solution.py:318
  107.3 10.5 %collective-permute-start.3 = (bf16[2,64,128]{2,1,0:T(8,128)(2,1)S(1)}, bf16[2,64,128]{2,1,0:T(8,128)(2,1)S(1)}, u32[]{:S(2)}, u32[]{:S(2)}) collective-permute-start(bf16[2,64,128]{2,1,0:T(8,128)(2,1)S(1)} %get-tuple-element.36.through_ref), channel_id=1, source_target_pairs={{0,128},{16,144},{32,160},{48,176},{64,192},{80,208},{96,224},{112... | collective-permute-start | bytes 98312 | tf_op jit(solution)/shard_map/ppermute | solution.py:263
  118.1 49.8 %copy-start.9 = (f32[64]{0:T(128)S(1)}, f32[64]{0:T(128)}, u32[]{:S(2)}) copy-start(f32[64]{0:T(128)} %param.18) | copy-start | bytes 772
  118.1 49.9 %copy-start.8 = (f32[256,2]{0,1:T(2,128)S(1)}, f32[256,2]{0,1:T(2,128)}, u32[]{:S(2)}) copy-start(f32[256,2]{0,1:T(2,128)} %param.22) | copy-start | bytes 6148
  118.1 13.5 %collective-permute-start.4 = (bf16[2,64,128]{2,1,0:T(8,128)(2,1)S(1)}, bf16[2,64,128]{2,1,0:T(8,128)(2,1)S(1)}, u32[]{:S(2)}, u32[]{:S(2)}) collective-permute-start(bf16[2,64,128]{2,1,0:T(8,128)(2,1)S(1)} %get-tuple-element.38), channel_id=1, source_target_pairs={{0,256},{16,272},{32,288},{48,304},{64,320},{80,336},{96,352},{112... | collective-permute-start | bytes 98312 | tf_op jit(solution)/shard_map/ppermute | solution.py:263
  151.1 35.6 %all-to-all-start.3 = ((bf16[32,24,128]{2,1,0:T(8,128)(2,1)}), bf16[32,24,128]{2,1,0:T(8,128)(2,1)S(1)}, u32[]{:S(2)}, u32[]{:S(2)}) async-start(bf16[32,24,128]{2,1,0:T(8,128)(2,1)} %bitcast.12), calls=%async_computation.3 | async-start | bytes 393216 | tf_op jit(solution)/shard_map/all_to_all | solution.py:318

commit v3 on v2

--- a/solution.py
+++ b/solution.py
@@ -1,3 +1,5 @@
+import functools
+
 import jax
 import jax.numpy as jnp
 from jax import lax
@@ -280,7 +282,7 @@
 
 def expert_rows(rows, gate, up, down):
     parts, total, lanes = rows.shape
-    tile = 256 if total % 256 == 0 else total
+    tile = 128 if total % 128 == 0 else total
     block = pl.BlockSpec((parts, tile, lanes), lambda i: (0, i, 0))
     fixed = lambda array: pl.BlockSpec(array.shape, lambda i: (0, 0))
     return pl.pallas_call(
@@ -299,19 +301,75 @@
     )(rows, gate, up, down)
 
 
-def slot_targets(routes, experts_n, capacity):
-    onehot = (routes[:, :, None] == jnp.arange(experts_n, dtype=jnp.int32)[None, None, :]).astype(
-        jnp.int32
-    )
-    flat = onehot.reshape(-1, experts_n)
-    before = jnp.cumsum(flat, axis=0) - flat
-    slot_index = jnp.sum(before * flat, axis=-1).reshape(routes.shape)
-    return routes * capacity + slot_index
-
-
-def dispatch_matrix(targets, slot_total):
-    matches = targets[None, :, :] == jnp.arange(slot_total, dtype=jnp.int32)[:, None, None]
-    return jnp.sum(matches.astype(jnp.float32), axis=-1).astype(jnp.bfloat16)
+def route_kernel(
+    capacity, at_ref, rows_ref, gain_ref, routes_ref, weight_ref, outgoing_ref, combine_ref
+):
+    total, slots = combine_ref.shape
+    full = rows_ref[...].astype(jnp.float32)
+    scale = lax.rsqrt(jnp.mean(full * full, axis=1, keepdims=True) + 1e-06)
+    lanes = pl.ds(pl.multiple_of(at_ref[0], LANES), LANES)
+    normed = rows_ref[:, lanes].astype(jnp.float32) * scale * gain_ref[:, lanes]
+    expert = lax.broadcasted_iota(jnp.int32, (total, LANES), 1)
+    named = [
+        jnp.where(routes_ref[:, k : k + 1] == expert, 1.0, 0.0)
+        for k in range(routes_ref.shape[1])
+    ]
+    earlier = lax.broadcasted_iota(jnp.int32, (total, total), 0) > lax.broadcasted_iota(
+        jnp.int32, (total, total), 1
+    )
+    before = mm(jnp.where(earlier, 1.0, 0.0), sum(named))
+    slot = lax.broadcasted_iota(jnp.int32, (total, slots), 1)
+    chosen = jnp.zeros((total, slots), jnp.float32)
+    combine = jnp.zeros((total, slots), jnp.float32)
+    for k, one in enumerate(named):
+        place = jnp.sum(before * one, axis=1, keepdims=True).astype(jnp.int32)
+        hit = routes_ref[:, k : k + 1] * capacity + place == slot
+        chosen = jnp.where(hit, 1.0, chosen)
+        combine = jnp.where(hit, weight_ref[:, k : k + 1], combine)
+    outgoing_ref[...] = mm_tn(chosen, normed).astype(jnp.bfloat16)
+    combine_ref[...] = combine.astype(jnp.bfloat16)
+
+
+def routed(at, rows, gain, routes, weight, slots, capacity):
+    total = rows.shape[0]
+    return pl.pallas_call(
+        functools.partial(route_kernel, capacity),
+        out_shape=(
+            jax.ShapeDtypeStruct((slots, LANES), jnp.bfloat16),
+            jax.ShapeDtypeStruct((total, slots), jnp.bfloat16),
+        ),
+        in_specs=in_vmem(4, 1),
+        out_specs=tuple(in_vmem(2, 0)),
+        cost_estimate=pl.CostEstimate(
+            flops=4 * total * slots * LANES, bytes_accessed=2 * rows.size, transcendentals=total
+        ),
+        compiler_params=pltpu.CompilerParams(vmem_limit_bytes=24 * 2**20),
+        name="route_rows",
+    )(at, rows, gain, routes, weight)
+
+
+def sum_kernel(pieces_ref, out_ref):
+    total = pieces_ref[0].astype(jnp.float32)
+    for j in range(1, pieces_ref.shape[0]):
+        total += pieces_ref[j].astype(jnp.float32)
+    out_ref[...] = total.astype(jnp.bfloat16)
+
+
+def summed_pieces(pieces):
+    parts, total, lanes = pieces.shape
+    tile = 128 if total % 128 == 0 else total
+    return pl.pallas_call(
+        sum_kernel,
+        grid=(total // tile,),
+        in_specs=[pl.BlockSpec((parts, tile, lanes), lambda i: (0, i, 0))],
+        out_specs=pl.BlockSpec((tile, lanes), lambda i: (i, 0)),
+        out_shape=jax.ShapeDtypeStruct((total, lanes), jnp.bfloat16),
+        cost_estimate=pl.CostEstimate(
+            flops=pieces.size, bytes_accessed=2 * pieces.size, transcendentals=0
+        ),
+        compiler_params=pltpu.CompilerParams(vmem_limit_bytes=63600000),
+        name="sum_pieces",
+    )(pieces)
 
 
 def spread(array, axis):
@@ -339,19 +397,20 @@
     slot_total = experts_n * capacity
     col_count = features // shares
     at = lax.axis_index("tp") * col_count
-    input_f = expert_in.astype(jnp.float32)
-    scale = lax.rsqrt(jnp.mean(input_f * input_f, axis=-1, keepdims=True) + 1e-06)
-    own = lax.dynamic_slice_in_dim(expert_in, at, col_count, 1).astype(jnp.float32)
-    normed = (own * scale * lax.dynamic_slice_in_dim(expert_gain, at, col_count, 0)).astype(
-        jnp.bfloat16
-    )
-    targets = slot_targets(routes, experts_n, capacity)
-    outgoing = mm(dispatch_matrix(targets, slot_total), normed).astype(jnp.bfloat16)
+    outgoing, combine = routed(
+        at.reshape(1).astype(jnp.int32),
+        expert_in,
+        expert_gain[None],
+        routes,
+        route_weight,
+        slot_total,
+        capacity,
+    )
     arrived = spread(outgoing.reshape(experts_n, capacity, col_count), "ep").reshape(
         slot_total, col_count
     )
+    arrived, query_in = lax.optimization_barrier((arrived, query_in))
     oloc, qp, own_maps = local_half(query_in, key_in, value_in, erase_pre, decay_pre)
-    arrived, own_maps = lax.optimization_barrier((arrived, own_maps))
     shared = spread(jnp.broadcast_to(arrived[None], (shares, *arrived.shape)), "tp")
 
     past, through, distance = jnp.zeros(own_maps.shape, jnp.float32), own_maps, 1
@@ -367,14 +426,12 @@
     crossing = swapped(through, distance)
     pieces = spread(partial, "tp")
     pieces, crossing = lax.optimization_barrier((pieces, crossing))
-    summed = jnp.sum(pieces.astype(jnp.float32), axis=0).astype(jnp.bfloat16)
+    summed = summed_pieces(pieces)
     returned = spread(summed.reshape(experts_n, capacity, col_count), "ep").reshape(
         slot_total, col_count
     )
     mixer_out = finish_half(side(distance), crossing, past, oloc, qp, mix_gain[:, None])
-    matches = targets[:, :, None] == jnp.arange(slot_total, dtype=jnp.int32)[None, None, :]
-    combine = jnp.sum(matches.astype(jnp.float32) * route_weight[:, :, None], axis=1)
-    expert_out = jnp.dot(combine, returned.astype(jnp.float32)).astype(jnp.bfloat16)
+    expert_out = mm(combine, returned).astype(jnp.bfloat16)
     return (mixer_out, expert_out)
 
 

time: 188 us -> 189 us (level)
  blocking collectives: 0 us -> 35.3 us
  starting transfers between devices: 70.5 us -> 48.7 us
  waiting for transfers between devices: 78 us -> 63.6 us
  Pallas kernels: 22.8 us -> 30 us
  other arithmetic: 5.91 us -> 0 us
    all_to_all x0 -> x1, blocking collectives: none -> 35.3 us  [spread(): return lax.all_to_all(array, axis, 0, 0, tiled=True)]
    all_to_all x4 -> x3, starting transfers between devices: 44.9 us -> 27.3 us  [spread(): return lax.all_to_all(array, axis, 0, 0, tiled=True)]
    all_to_all x4 -> x3, waiting for transfers between devices: 66.7 us -> 49.9 us  [spread(): return lax.all_to_all(array, axis, 0, 0, tiled=True)]
    pallas_call x0 -> x2, Pallas kernels: none -> 5.83 us  [the longest x1 4.66 us: summed_pieces(): pl.pallas_call(sum_kernel, grid=(total // tile,), in_specs=[pl.BlockSpec(...]
    ppermute x5, starting transfers between devices: 25.6 us -> 21.5 us  [swapped(): lax.ppermute(through, 'ep', [(i, i ^ distance) for i in range(count)])]
    reduce_sum x5 -> x0, other arithmetic: 4 us -> none  [the longest x1 3.05 us: on_device(): summed = jnp.sum(pieces.astype(jnp.float32), axis=0).astype(jnp.bfloat16)]
    unnamed x23 -> x24, local copies, waits for them, and re-layouts: 3.6 us -> 6.25 us
    ppermute x5, waiting for transfers between devices: 11.3 us -> 13.7 us  [swapped(): lax.ppermute(through, 'ep', [(i, i ^ distance) for i in range(count)])]
  transfers between devices with their start and end apart: 9 -> 8, of which waited for: 9 -> 8; matrix products, arithmetic and copies ran while one was open for 2% -> 1% of each run, Pallas kernels for 8% -> 8%
where the time goes in v3:
time: 189 us; the launch traced here: 188 us
  waiting for transfers between devices  63.6 us (34%)
  starting transfers between devices  48.7 us (26%)
  blocking collectives  35.3 us (19%)
  Pallas kernels  30 us (16%)
  local copies, waits for them, and re-layouts  8.63 us (5%)
    all_to_all x3, waiting for transfers between devices, spread(): return lax.all_to_all(array, axis, 0, 0, tiled=True)  49.9 us
    all_to_all x1, blocking collectives, spread(): return lax.all_to_all(array, axis, 0, 0, tiled=True)  35.3 us
    all_to_all x3, starting transfers between devices, spread(): return lax.all_to_all(array, axis, 0, 0, tiled=True)  27.3 us
    ppermute x5, starting transfers between devices, swapped(): lax.ppermute(through, 'ep', [(i, i ^ distance) for i in range(count)])  21.5 us
    ppermute x5, waiting for transfers between devices, swapped(): lax.ppermute(through, 'ep', [(i, i ^ distance) for i in range(count)])  13.7 us
    pallas_call x1, Pallas kernels, local_half(): pl.pallas_call(local_kernel, out_shape=(full(jnp.float32), jax.ShapeDtype...  13.4 us
    pallas_call x1, Pallas kernels, expert_rows(): pl.pallas_call(expert_kernel, grid=(total // tile,), in_specs=[block, fix...  8.26 us
    unnamed x24, local copies, waits for them, and re-layouts  6.25 us
  transfers between devices with their start and end apart: 8, of which 8 were waited for; matrix products, arithmetic and copies ran while one was open for 1% of the time, Pallas kernels for 8%

profile of v3, /device:TPU:1, one launch (start us, length us, event | category | flops | bytes accessed | tf_op | source)
XLA Modules:
  0.0 188.0 jit_solution(3639572385922461225)
XLA Ops:
  0.6 0.8 copy.15.routes_ref
  1.4 0.8 copy.16.weight_ref
  2.3 0.0 copy-start
  2.3 1.2 copy-done
  3.5 0.0 copy-start.1
  3.5 0.7 copy-done.1
  4.2 1.2 route_rows.1
  5.4 35.3 %all_to_all.20 = bf16[32,24,128]{2,1,0:T(8,128)(2,1)S(1)} all-to-all(bf16[32,24,128]{2,1,0:T(8,128)(2,1)S(1)} %bitcast.17), channel_id=1, replica_groups=mesh['ep'=32,'tp'=16] {'ep'}, dimensions={0} | all-to-all | bytes 393216 | tf_op jit(solution)/shard_map/all_to_all | solution.py:376
  40.7 2.3 %broadcast_in_dim.16 = bf16[16,768,128]{2,1,0:T(8,128)(2,1)} broadcast(bf16[768,128]{1,0:T(8,128)(2,1)S(1)} %bitcast.23), dimensions={1,2} | broadcast | bytes 3342336 | tf_op jit(solution)/shard_map/broadcast_in_dim | solution.py:414
  43.0 0.0 copy-start.2
  43.0 0.0 copy-start.3
  43.0 0.0 copy-start.4
  43.0 0.0 copy-start.5
  43.0 0.0 copy-start.6
  43.0 6.9 %all-to-all-start.1 = ((bf16[16,768,128]{2,1,0:T(8,128)(2,1)}), bf16[16,768,128]{2,1,0:T(8,128)(2,1)}, u32[]{:S(2)}, u32[]{:S(2)}) async-start(bf16[16,768,128]{2,1,0:T(8,128)(2,1)} %broadcast_in_dim.16), calls=%async_computation.1 | async-start | bytes 6291456 | tf_op jit(solution)/shard_map/all_to_all | solution.py:376
  50.0 0.0 copy-done.2
  50.0 0.0 copy-done.3
  50.0 0.0 copy-done.4
  50.0 0.0 copy-done.5
  50.0 0.0 copy-done.6
  50.0 0.0 copy-start.7
  50.0 0.0 copy-start.8
  50.0 13.4 %mixer_local.1 = (f32[64,1024]{1,0:T(8,128)S(1)}, bf16[128,1024]{1,0:T(8,128)(2,1)S(1)}, bf16[2,64,128]{2,1,0:T(8,128)(2,1)S(1)}) custom-call(bf16[64,1024]{1,0:T(8,128)(2,1)S(1)} %copy-done.2, bf16[64,1024]{1,0:T(8,128)(2,1)S(1)} %copy-done.3, bf16[64,1024]{1,0:T(8,128)(2,1)S(1)} %copy-done.4, bf16[64,1024]{1,0:T(8,128)(2,1)S(1)} %copy-done.5, ...), custom_call_target="tpu_custom_call" | custom-call | flops 1476395008 | bytes 1179648 | tf_op jit(solution)/shard_map/mixer_local/pallas_call | solution.py:155
  63.5 3.6 %collective-permute-start = (bf16[2,64,128]{2,1,0:T(8,128)(2,1)S(1)}, bf16[2,64,128]{2,1,0:T(8,128)(2,1)S(1)}, u32[]{:S(2)}, u32[]{:S(2)}) collective-permute-start(bf16[2,64,128]{2,1,0:T(8,128)(2,1)S(1)} %get-tuple-element.28.through_ref), channel_id=1, source_target_pairs={{0,16},{16,0},{32,48},{48,32},{64,80},{80,64},{96,112},{112,96},{1... | collective-permute-start | bytes 98312 | tf_op jit(solution)/shard_map/ppermute | solution.py:265
  67.1 0.8 collective-permute-done.arrived_ref
  68.0 0.3 scan_step.4
  68.3 1.9 %collective-permute-start.1 = (bf16[2,64,128]{2,1,0:T(8,128)(2,1)S(1)}, bf16[2,64,128]{2,1,0:T(8,128)(2,1)S(1)}, u32[]{:S(2)}, u32[]{:S(2)}) collective-permute-start(bf16[2,64,128]{2,1,0:T(8,128)(2,1)S(1)} %get-tuple-element.29.through_ref), channel_id=1, source_target_pairs={{0,32},{16,48},{32,0},{48,16},{64,96},{80,112},{96,64},{112,80},{1... | collective-permute-start | bytes 98312 | tf_op jit(solution)/shard_map/ppermute | solution.py:265
  70.2 3.1 %collective-permute-done.1.arrived_ref = bf16[2,64,128]{2,1,0:T(8,128)(2,1)S(1)} collective-permute-done((bf16[2,64,128]{2,1,0:T(8,128)(2,1)S(1)}, bf16[2,64,128]{2,1,0:T(8,128)(2,1)S(1)}, u32[]{:S(2)}, u32[]{:S(2)}) %collective-permute-start.1) | collective-permute-done | bytes 32800 | tf_op jit(solution)/shard_map/ppermute | solution.py:265
  73.3 0.3 scan_step.5
  73.7 1.9 %collective-permute-start.2 = (bf16[2,64,128]{2,1,0:T(8,128)(2,1)S(1)}, bf16[2,64,128]{2,1,0:T(8,128)(2,1)S(1)}, u32[]{:S(2)}, u32[]{:S(2)}) collective-permute-start(bf16[2,64,128]{2,1,0:T(8,128)(2,1)S(1)} %get-tuple-element.31.through_ref), channel_id=1, source_target_pairs={{0,64},{16,80},{32,96},{48,112},{64,0},{80,16},{96,32},{112,48},{1... | collective-permute-start | bytes 98312 | tf_op jit(solution)/shard_map/ppermute | solution.py:265
  75.6 0.0 copy-done.7
  75.6 1.3 copy.17
  76.9 0.0 copy-done.8
  76.9 1.4 copy.18
  78.3 1.4 collective-permute-done.2.arrived_ref
  79.7 0.3 scan_step.6
  80.0 14.3 %all-to-all-done.1.rows_ref = bf16[16,768,128]{2,1,0:T(8,128)(2,1)} async-done(((bf16[16,768,128]{2,1,0:T(8,128)(2,1)}), bf16[16,768,128]{2,1,0:T(8,128)(2,1)}, u32[]{:S(2)}, u32[]{:S(2)}) %all-to-all-start.1) | async-done | bytes 3145760 | tf_op jit(solution)/shard_map/all_to_all | solution.py:376
  94.3 8.3 %expert_rows.1 = bf16[16,768,128]{2,1,0:T(8,128)(2,1)} custom-call(bf16[16,768,128]{2,1,0:T(8,128)(2,1)} %all-to-all-done.1.rows_ref, bf16[2048,224]{1,0:T(8,128)(2,1)} %bitcast.19, bf16[2048,224]{1,0:T(8,128)(2,1)} %bitcast.20, bf16[224,2048]{1,0:T(8,128)(2,1)} %bitcast.21), custom_call_target="tpu_custom_call" | custom-call | flops 2113929216 | bytes 9043968 | tf_op jit(solution)/shard_map/expert_rows/pallas_call | solution.py:288
  102.6 4.5 %all-to-all-start.2 = ((bf16[16,768,128]{2,1,0:T(8,128)(2,1)}), bf16[16,768,128]{2,1,0:T(8,128)(2,1)}, u32[]{:S(2)}, u32[]{:S(2)}) async-start(bf16[16,768,128]{2,1,0:T(8,128)(2,1)} %expert_rows.1), calls=%async_computation.2 | async-start | bytes 6291456 | tf_op jit(solution)/shard_map/all_to_all | solution.py:376
  107.1 0.0 copy-start.9
  107.1 7.7 %collective-permute-start.3 = (bf16[2,64,128]{2,1,0:T(8,128)(2,1)S(1)}, bf16[2,64,128]{2,1,0:T(8,128)(2,1)S(1)}, u32[]{:S(2)}, u32[]{:S(2)}) collective-permute-start(bf16[2,64,128]{2,1,0:T(8,128)(2,1)S(1)} %get-tuple-element.39.through_ref), channel_id=1, source_target_pairs={{0,128},{16,144},{32,160},{48,176},{64,192},{80,208},{96,224},{112... | collective-permute-start | bytes 98312 | tf_op jit(solution)/shard_map/ppermute | solution.py:265
  114.8 1.3 collective-permute-done.3.arrived_ref
  116.0 0.3 scan_step.7
  116.4 6.3 %collective-permute-start.4 = (bf16[2,64,128]{2,1,0:T(8,128)(2,1)S(1)}, bf16[2,64,128]{2,1,0:T(8,128)(2,1)S(1)}, u32[]{:S(2)}, u32[]{:S(2)}) collective-permute-start(bf16[2,64,128]{2,1,0:T(8,128)(2,1)S(1)} %get-tuple-element.41), channel_id=1, source_target_pairs={{0,256},{16,272},{32,288},{48,304},{64,320},{80,336},{96,352},{112... | collective-permute-start | bytes 98312 | tf_op jit(solution)/shard_map/ppermute | solution.py:265
  122.7 7.0 %collective-permute-done.4.arrived_ref = bf16[2,64,128]{2,1,0:T(8,128)(2,1)S(1)} collective-permute-done((bf16[2,64,128]{2,1,0:T(8,128)(2,1)S(1)}, bf16[2,64,128]{2,1,0:T(8,128)(2,1)S(1)}, u32[]{:S(2)}, u32[]{:S(2)}) %collective-permute-start.4) | collective-permute-done | bytes 32800 | tf_op jit(solution)/shard_map/ppermute | solution.py:265
  129.8 18.1 %all-to-all-done.2.pieces_ref = bf16[16,768,128]{2,1,0:T(8,128)(2,1)} async-done(((bf16[16,768,128]{2,1,0:T(8,128)(2,1)}), bf16[16,768,128]{2,1,0:T(8,128)(2,1)}, u32[]{:S(2)}, u32[]{:S(2)}) %all-to-all-start.2) | async-done | bytes 3145760 | tf_op jit(solution)/shard_map/all_to_all | solution.py:376
  147.8 4.7 %sum_pieces.1 = bf16[768,128]{1,0:T(8,128)(2,1)} custom-call(bf16[16,768,128]{2,1,0:T(8,128)(2,1)} %all-to-all-done.2.pieces_ref), custom_call_target="tpu_custom_call" | custom-call | flops 1572864 | bytes 3145728 | tf_op jit(solution)/shard_map/sum_pieces/pallas_call | solution.py:361
  152.5 15.8 %all-to-all-start.3 = ((bf16[32,24,128]{2,1,0:T(8,128)(2,1)}), bf16[32,24,128]{2,1,0:T(8,128)(2,1)S(1)}, u32[]{:S(2)}, u32[]{:S(2)}) async-start(bf16[32,24,128]{2,1,0:T(8,128)(2,1)} %bitcast.22), calls=%async_computation.3 | async-start | bytes 393216 | tf_op jit(solution)/shard_map/all_to_all | solution.py:376
  168.3 0.0 copy-done.9
  168.4 0.1 copy.19.gain_ref
  168.4 1.2 mixer_finish.1
  169.6 17.5 %all-to-all-done.3 = bf16[32,24,128]{2,1,0:T(8,128)(2,1)S(1)} async-done(((bf16[32,24,128]{2,1,0:T(8,128)(2,1)}), bf16[32,24,128]{2,1,0:T(8,128)(2,1)S(1)}, u32[]{:S(2)}, u32[]{:S(2)}) %all-to-all-start.3) | async-done | bytes 196640 | tf_op jit(solution)/shard_map/all_to_all | solution.py:376
  187.1 0.9 convolution_convert_fusion
  (1 shorter events, 0.0 us)
Async XLA Ops:
  2.3 1.2 copy-start
  3.5 0.7 copy-start.1
  43.0 7.0 %copy-start.2 = (bf16[64,1024]{1,0:T(8,128)(2,1)S(1)}, bf16[64,1024]{1,0:T(8,128)(2,1)}, u32[]{:S(2)}) copy-start(bf16[64,1024]{1,0:T(8,128)(2,1)} %q_ref) | copy-start | bytes 393220
  43.0 7.0 %copy-start.3 = (bf16[64,1024]{1,0:T(8,128)(2,1)S(1)}, bf16[64,1024]{1,0:T(8,128)(2,1)}, u32[]{:S(2)}) copy-start(bf16[64,1024]{1,0:T(8,128)(2,1)} %k_ref.1) | copy-start | bytes 393220
  43.0 7.0 %copy-start.4 = (bf16[64,1024]{1,0:T(8,128)(2,1)S(1)}, bf16[64,1024]{1,0:T(8,128)(2,1)}, u32[]{:S(2)}) copy-start(bf16[64,1024]{1,0:T(8,128)(2,1)} %v_ref.1) | copy-start | bytes 393220
  43.0 7.0 %copy-start.5 = (bf16[64,1024]{1,0:T(8,128)(2,1)S(1)}, bf16[64,1024]{1,0:T(8,128)(2,1)}, u32[]{:S(2)}) copy-start(bf16[64,1024]{1,0:T(8,128)(2,1)} %e_ref.1) | copy-start | bytes 393220
  43.0 7.0 %copy-start.6 = (bf16[64,1024]{1,0:T(8,128)(2,1)S(1)}, bf16[64,1024]{1,0:T(8,128)(2,1)}, u32[]{:S(2)}) copy-start(bf16[64,1024]{1,0:T(8,128)(2,1)} %d_ref.1) | copy-start | bytes 393220
  43.0 51.3 %all-to-all-start.1 = ((bf16[16,768,128]{2,1,0:T(8,128)(2,1)}), bf16[16,768,128]{2,1,0:T(8,128)(2,1)}, u32[]{:S(2)}, u32[]{:S(2)}) async-start(bf16[16,768,128]{2,1,0:T(8,128)(2,1)} %broadcast_in_dim.16), calls=%async_computation.1 | async-start | bytes 6291456 | tf_op jit(solution)/shard_map/all_to_all | solution.py:376
  50.0 25.6 %copy-start.7 = (bf16[1,2048,224]{1,2,0:T(8,128)(2,1)S(1)}, bf16[1,2048,224]{1,2,0:T(8,128)(2,1)}, u32[]{:S(2)}) copy-start(bf16[1,2048,224]{1,2,0:T(8,128)(2,1)} %param.23) | copy-start | bytes 2752516
  50.0 26.9 %copy-start.8 = (bf16[1,2048,224]{1,2,0:T(8,128)(2,1)S(1)}, bf16[1,2048,224]{1,2,0:T(8,128)(2,1)}, u32[]{:S(2)}) copy-start(bf16[1,2048,224]{1,2,0:T(8,128)(2,1)} %param.24) | copy-start | bytes 2752516
  63.5 4.5 %collective-permute-start = (bf16[2,64,128]{2,1,0:T(8,128)(2,1)S(1)}, bf16[2,64,128]{2,1,0:T(8,128)(2,1)S(1)}, u32[]{:S(2)}, u32[]{:S(2)}) collective-permute-start(bf16[2,64,128]{2,1,0:T(8,128)(2,1)S(1)} %get-tuple-element.28.through_ref), channel_id=1, source_target_pairs={{0,16},{16,0},{32,48},{48,32},{64,80},{80,64},{96,112},{112,96},{1... | collective-permute-start | bytes 98312 | tf_op jit(solution)/shard_map/ppermute | solution.py:265
  68.3 5.1 %collective-permute-start.1 = (bf16[2,64,128]{2,1,0:T(8,128)(2,1)S(1)}, bf16[2,64,128]{2,1,0:T(8,128)(2,1)S(1)}, u32[]{:S(2)}, u32[]{:S(2)}) collective-permute-start(bf16[2,64,128]{2,1,0:T(8,128)(2,1)S(1)} %get-tuple-element.29.through_ref), channel_id=1, source_target_pairs={{0,32},{16,48},{32,0},{48,16},{64,96},{80,112},{96,64},{112,80},{1... | collective-permute-start | bytes 98312 | tf_op jit(solution)/shard_map/ppermute | solution.py:265
  73.7 6.0 %collective-permute-start.2 = (bf16[2,64,128]{2,1,0:T(8,128)(2,1)S(1)}, bf16[2,64,128]{2,1,0:T(8,128)(2,1)S(1)}, u32[]{:S(2)}, u32[]{:S(2)}) collective-permute-start(bf16[2,64,128]{2,1,0:T(8,128)(2,1)S(1)} %get-tuple-element.31.through_ref), channel_id=1, source_target_pairs={{0,64},{16,80},{32,96},{48,112},{64,0},{80,16},{96,32},{112,48},{1... | collective-permute-start | bytes 98312 | tf_op jit(solution)/shard_map/ppermute | solution.py:265
  102.6 45.3 %all-to-all-start.2 = ((bf16[16,768,128]{2,1,0:T(8,128)(2,1)}), bf16[16,768,128]{2,1,0:T(8,128)(2,1)}, u32[]{:S(2)}, u32[]{:S(2)}) async-start(bf16[16,768,128]{2,1,0:T(8,128)(2,1)} %expert_rows.1), calls=%async_computation.2 | async-start | bytes 6291456 | tf_op jit(solution)/shard_map/all_to_all | solution.py:376
  107.1 61.3 %copy-start.9 = (f32[64]{0:T(128)S(1)}, f32[64]{0:T(128)}, u32[]{:S(2)}) copy-start(f32[64]{0:T(128)} %param.18) | copy-start | bytes 772
  107.1 9.0 %collective-permute-start.3 = (bf16[2,64,128]{2,1,0:T(8,128)(2,1)S(1)}, bf16[2,64,128]{2,1,0:T(8,128)(2,1)S(1)}, u32[]{:S(2)}, u32[]{:S(2)}) collective-permute-start(bf16[2,64,128]{2,1,0:T(8,128)(2,1)S(1)} %get-tuple-element.39.through_ref), channel_id=1, source_target_pairs={{0,128},{16,144},{32,160},{48,176},{64,192},{80,208},{96,224},{112... | collective-permute-start | bytes 98312 | tf_op jit(solution)/shard_map/ppermute | solution.py:265
  116.4 13.4 %collective-permute-start.4 = (bf16[2,64,128]{2,1,0:T(8,128)(2,1)S(1)}, bf16[2,64,128]{2,1,0:T(8,128)(2,1)S(1)}, u32[]{:S(2)}, u32[]{:S(2)}) collective-permute-start(bf16[2,64,128]{2,1,0:T(8,128)(2,1)S(1)} %get-tuple-element.41), channel_id=1, source_target_pairs={{0,256},{16,272},{32,288},{48,304},{64,320},{80,336},{96,352},{112... | collective-permute-start | bytes 98312 | tf_op jit(solution)/shard_map/ppermute | solution.py:265
  152.5 34.6 %all-to-all-start.3 = ((bf16[32,24,128]{2,1,0:T(8,128)(2,1)}), bf16[32,24,128]{2,1,0:T(8,128)(2,1)S(1)}, u32[]{:S(2)}, u32[]{:S(2)}) async-start(bf16[32,24,128]{2,1,0:T(8,128)(2,1)} %bitcast.22), calls=%async_computation.3 | async-start | bytes 393216 | tf_op jit(solution)/shard_map/all_to_all | solution.py:376

commit v4 on v3

--- a/solution.py
+++ b/solution.py
@@ -172,7 +172,7 @@
         cost_estimate=pl.CostEstimate(
             flops=16 * 22 * 2 * 128**3, bytes_accessed=tokens * 64 * 18, transcendentals=tokens * 64 * 9
         ),
-        compiler_params=pltpu.CompilerParams(vmem_limit_bytes=16 * 2**20),
+        compiler_params=pltpu.CompilerParams(vmem_limit_bytes=66000000),
         name="mixer_local",
     )(query, key, value, erase, decay)
 
@@ -296,7 +296,7 @@
             bytes_accessed=2 * (2 * rows.size + 3 * gate.size),
             transcendentals=total * gate.shape[1],
         ),
-        compiler_params=pltpu.CompilerParams(vmem_limit_bytes=63600000),
+        compiler_params=pltpu.CompilerParams(vmem_limit_bytes=66000000),
         name="expert_rows",
     )(rows, gate, up, down)
 
@@ -304,72 +304,52 @@
 def route_kernel(
     capacity, at_ref, rows_ref, gain_ref, routes_ref, weight_ref, outgoing_ref, combine_ref
 ):
-    total, slots = combine_ref.shape
+    slots, total = combine_ref.shape
     full = rows_ref[...].astype(jnp.float32)
     scale = lax.rsqrt(jnp.mean(full * full, axis=1, keepdims=True) + 1e-06)
     lanes = pl.ds(pl.multiple_of(at_ref[0], LANES), LANES)
     normed = rows_ref[:, lanes].astype(jnp.float32) * scale * gain_ref[:, lanes]
-    expert = lax.broadcasted_iota(jnp.int32, (total, LANES), 1)
+    expert = lax.broadcasted_iota(jnp.int32, (LANES, total), 0)
     named = [
-        jnp.where(routes_ref[:, k : k + 1] == expert, 1.0, 0.0)
-        for k in range(routes_ref.shape[1])
+        jnp.where(routes_ref[k : k + 1, :] == expert, 1.0, 0.0)
+        for k in range(routes_ref.shape[0])
     ]
-    earlier = lax.broadcasted_iota(jnp.int32, (total, total), 0) > lax.broadcasted_iota(
+    earlier = lax.broadcasted_iota(jnp.int32, (total, total), 0) < lax.broadcasted_iota(
         jnp.int32, (total, total), 1
     )
-    before = mm(jnp.where(earlier, 1.0, 0.0), sum(named))
-    slot = lax.broadcasted_iota(jnp.int32, (total, slots), 1)
-    chosen = jnp.zeros((total, slots), jnp.float32)
-    combine = jnp.zeros((total, slots), jnp.float32)
+    before = mm(sum(named), jnp.where(earlier, 1.0, 0.0))
+    slot = lax.broadcasted_iota(jnp.int32, (slots, total), 0)
+    chosen = jnp.zeros((slots, total), jnp.float32)
+    combine = jnp.zeros((slots, total), jnp.float32)
     for k, one in enumerate(named):
-        place = jnp.sum(before * one, axis=1, keepdims=True).astype(jnp.int32)
-        hit = routes_ref[:, k : k + 1] * capacity + place == slot
+        place = jnp.sum(before * one, axis=0, keepdims=True).astype(jnp.int32)
+        hit = routes_ref[k : k + 1, :] * capacity + place == slot
         chosen = jnp.where(hit, 1.0, chosen)
-        combine = jnp.where(hit, weight_ref[:, k : k + 1], combine)
-    outgoing_ref[...] = mm_tn(chosen, normed).astype(jnp.bfloat16)
+        combine = jnp.where(hit, weight_ref[k : k + 1, :], combine)
+    outgoing_ref[...] = mm(chosen, normed).astype(jnp.bfloat16)
     combine_ref[...] = combine.astype(jnp.bfloat16)
 
 
 def routed(at, rows, gain, routes, weight, slots, capacity):
     total = rows.shape[0]
+    whole = lambda array: pl.BlockSpec(array.shape, lambda: (0, 0))
     return pl.pallas_call(
         functools.partial(route_kernel, capacity),
         out_shape=(
             jax.ShapeDtypeStruct((slots, LANES), jnp.bfloat16),
-            jax.ShapeDtypeStruct((total, slots), jnp.bfloat16),
-        ),
-        in_specs=in_vmem(4, 1),
-        out_specs=tuple(in_vmem(2, 0)),
+            jax.ShapeDtypeStruct((slots, total), jnp.bfloat16),
+        ),
+        in_specs=in_vmem(0, 1) + [whole(v) for v in (rows, gain, routes, weight)],
         cost_estimate=pl.CostEstimate(
             flops=4 * total * slots * LANES, bytes_accessed=2 * rows.size, transcendentals=total
         ),
-        compiler_params=pltpu.CompilerParams(vmem_limit_bytes=24 * 2**20),
+        compiler_params=pltpu.CompilerParams(vmem_limit_bytes=63600000),
         name="route_rows",
     )(at, rows, gain, routes, weight)
 
 
-def sum_kernel(pieces_ref, out_ref):
-    total = pieces_ref[0].astype(jnp.float32)
-    for j in range(1, pieces_ref.shape[0]):
-        total += pieces_ref[j].astype(jnp.float32)
-    out_ref[...] = total.astype(jnp.bfloat16)
-
-
 def summed_pieces(pieces):
-    parts, total, lanes = pieces.shape
-    tile = 128 if total % 128 == 0 else total
-    return pl.pallas_call(
-        sum_kernel,
-        grid=(total // tile,),
-        in_specs=[pl.BlockSpec((parts, tile, lanes), lambda i: (0, i, 0))],
-        out_specs=pl.BlockSpec((tile, lanes), lambda i: (i, 0)),
-        out_shape=jax.ShapeDtypeStruct((total, lanes), jnp.bfloat16),
-        cost_estimate=pl.CostEstimate(
-            flops=pieces.size, bytes_accessed=2 * pieces.size, transcendentals=0
-        ),
-        compiler_params=pltpu.CompilerParams(vmem_limit_bytes=63600000),
-        name="sum_pieces",
-    )(pieces)
+    return jnp.sum(pieces.astype(jnp.float32), axis=0).astype(jnp.bfloat16)
 
 
 def spread(array, axis):
@@ -401,37 +381,59 @@
         at.reshape(1).astype(jnp.int32),
         expert_in,
         expert_gain[None],
-        routes,
-        route_weight,
+        routes.T,
+        route_weight.T,
         slot_total,
         capacity,
     )
     arrived = spread(outgoing.reshape(experts_n, capacity, col_count), "ep").reshape(
         slot_total, col_count
     )
-    arrived, query_in = lax.optimization_barrier((arrived, query_in))
+    middle = slot_total // 2
+    copies = [
+        jnp.broadcast_to(part[None], (shares, *part.shape))
+        for part in (arrived[:middle], arrived[middle:])
+    ]
+    copies[0], query_in = lax.optimization_barrier((copies[0], query_in))
+    shared_a = spread(copies[0], "tp")
     oloc, qp, own_maps = local_half(query_in, key_in, value_in, erase_pre, decay_pre)
-    shared = spread(jnp.broadcast_to(arrived[None], (shares, *arrived.shape)), "tp")
-
-    past, through, distance = jnp.zeros(own_maps.shape, jnp.float32), own_maps, 1
-    while distance < experts_n // 4:
-        past, through = scan_step(side(distance), swapped(through, distance), through, past)
-        distance *= 2
-    shared, past, through = lax.optimization_barrier((shared, past, through))
-    partial = expert_rows(shared, gate_weight[0], up_weight[0], down_weight[0])
-    partial, past, through = lax.optimization_barrier((partial, past, through))
-    while distance < experts_n // 2:
-        past, through = scan_step(side(distance), swapped(through, distance), through, past)
-        distance *= 2
-    crossing = swapped(through, distance)
-    pieces = spread(partial, "tp")
-    pieces, crossing = lax.optimization_barrier((pieces, crossing))
-    summed = summed_pieces(pieces)
+    past, through = jnp.zeros(own_maps.shape, jnp.float32), own_maps
+    weights = [gate_weight[0], up_weight[0], down_weight[0]]
+    shared_a, copies[1], past, through = lax.optimization_barrier(
+        (shared_a, copies[1], past, through)
+    )
+
+    def scanned(steps, past, through):
+        for step in steps:
+            past, through = scan_step(side(step), swapped(through, step), through, past)
+        return past, through
+
+    shared_b = spread(copies[1], "tp")
+    partial_a = expert_rows(shared_a, *weights)
+    past, through = scanned((1, 2), past, through)
+    shared_b, partial_a, past, through = lax.optimization_barrier(
+        (shared_b, partial_a, past, through)
+    )
+    pieces_a = spread(partial_a, "tp")
+    partial_b = expert_rows(shared_b, *weights)
+    past, through = scanned((4,), past, through)
+    pieces_a, partial_b, past, through = lax.optimization_barrier(
+        (pieces_a, partial_b, past, through)
+    )
+    pieces_b = spread(partial_b, "tp")
+    summed_a = summed_pieces(pieces_a)
+    past, through = scanned((8,), past, through)
+    pieces_b, summed_a, past, through = lax.optimization_barrier(
+        (pieces_b, summed_a, past, through)
+    )
+    summed = jnp.concatenate([summed_a, summed_pieces(pieces_b)], axis=0)
     returned = spread(summed.reshape(experts_n, capacity, col_count), "ep").reshape(
         slot_total, col_count
     )
+    distance = experts_n // 2
+    crossing = swapped(through, distance)
     mixer_out = finish_half(side(distance), crossing, past, oloc, qp, mix_gain[:, None])
-    expert_out = mm(combine, returned).astype(jnp.bfloat16)
+    expert_out = mm_tn(combine, returned).astype(jnp.bfloat16)
     return (mixer_out, expert_out)
 
 

time: 189 us -> 190 us (level)
  starting transfers between devices: 48.7 us -> 77 us
  waiting for transfers between devices: 63.6 us -> 35.4 us
  local copies, waits for them, and re-layouts: 8.63 us -> 5.72 us
  other arithmetic: 0 us -> 2.53 us
    all_to_all x3 -> x5, waiting for transfers between devices: 49.9 us -> 25.3 us  [spread(): return lax.all_to_all(array, axis, 0, 0, tiled=True)]
    ppermute x5, starting transfers between devices: 21.5 us -> 36.3 us  [swapped(): lax.ppermute(through, 'ep', [(i, i ^ distance) for i in range(count)])]
    all_to_all x3 -> x5, starting transfers between devices: 27.3 us -> 40.7 us  [spread(): return lax.all_to_all(array, axis, 0, 0, tiled=True)]
    pallas_call x1 -> x0, Pallas kernels: 4.66 us -> none  [summed_pieces(): pl.pallas_call(sum_kernel, grid=(total // tile,), in_specs=[pl.BlockSpec(...]
    ppermute x5, waiting for transfers between devices: 13.7 us -> 10.1 us  [swapped(): lax.ppermute(through, 'ep', [(i, i ^ distance) for i in range(count)])]
    unnamed x24 -> x16, local copies, waits for them, and re-layouts: 6.25 us -> 2.68 us
    pallas_call x1 -> x2, Pallas kernels: 8.26 us -> 11 us  [expert_rows(): pl.pallas_call(expert_kernel, grid=(total // tile,), in_specs=[block, fix...]
    pallas_call x1, Pallas kernels: 13.4 us -> 15.3 us  [local_half(): pl.pallas_call(local_kernel, out_shape=(full(jnp.float32), jax.ShapeDtype...]
  transfers between devices with their start and end apart: 8 -> 10, of which waited for: 8 -> 6; matrix products, arithmetic and copies ran while one was open for 1% -> 2% of each run, Pallas kernels for 8% -> 15%
where the time goes in v4:
time: 190 us; the launch traced here: 189 us
  starting transfers between devices  77 us (41%)
  blocking collectives  35.5 us (19%)
  waiting for transfers between devices  35.4 us (19%)
  Pallas kernels  31.4 us (17%)
  local copies, waits for them, and re-layouts  5.72 us (3%)
  other arithmetic  2.53 us (1%)
    all_to_all x5, starting transfers between devices, spread(): return lax.all_to_all(array, axis, 0, 0, tiled=True)  40.7 us
    ppermute x5, starting transfers between devices, swapped(): lax.ppermute(through, 'ep', [(i, i ^ distance) for i in range(count)])  36.3 us
    all_to_all x1, blocking collectives, spread(): return lax.all_to_all(array, axis, 0, 0, tiled=True)  35.5 us
    all_to_all x5, waiting for transfers between devices, spread(): return lax.all_to_all(array, axis, 0, 0, tiled=True)  25.3 us
    pallas_call x1, Pallas kernels, local_half(): pl.pallas_call(local_kernel, out_shape=(full(jnp.float32), jax.ShapeDtype...  15.3 us
    pallas_call x2, Pallas kernels, expert_rows(): pl.pallas_call(expert_kernel, grid=(total // tile,), in_specs=[block, fix...  11 us
    ppermute x5, waiting for transfers between devices, swapped(): lax.ppermute(through, 'ep', [(i, i ^ distance) for i in range(count)])  10.1 us
  transfers between devices with their start and end apart: 10, of which 6 were waited for; matrix products, arithmetic and copies ran while one was open for 2% of the time, Pallas kernels for 15%

profile of v4, /device:TPU:1, one launch (start us, length us, event | category | flops | bytes accessed | tf_op | source)
XLA Modules:
  0.0 189.3 jit_solution(17183273919896856474)
XLA Ops:
  0.6 2.6 %route_rows.1 = (bf16[768,128]{1,0:T(8,128)(2,1)}, bf16[768,256]{1,0:T(8,128)(2,1)}) custom-call(s32[1]{0:T(128)} %bitcast.1.at_ref, bf16[256,2048]{1,0:T(8,128)(2,1)} %rows_ref.1, f32[1,2048]{1,0:T(1,128)} %bitcast.30, s32[2,256]{1,0:T(2,128)} %bitcast.31, f32[2,256]{1,0:T(2,128)} %bitcast.32), custom_call_target="tpu_custom_call" | custom-call | flops 100663296 | bytes 1048576 | tf_op jit(solution)/shard_map/route_rows/pallas_call | solution.py:336
  3.2 35.5 %all_to_all.30 = bf16[32,24,128]{2,1,0:T(8,128)(2,1)S(1)} all-to-all(bf16[32,24,128]{2,1,0:T(8,128)(2,1)} %bitcast.29), channel_id=1, replica_groups=mesh['ep'=32,'tp'=16] {'ep'}, dimensions={0} | all-to-all | bytes 393216 | tf_op jit(solution)/shard_map/all_to_all | solution.py:356
  38.8 1.4 broadcast_in_dim.27
  40.2 6.8 %all-to-all-start.1 = ((bf16[16,384,128]{2,1,0:T(8,128)(2,1)}), bf16[16,384,128]{2,1,0:T(8,128)(2,1)}, u32[]{:S(2)}, u32[]{:S(2)}) async-start(bf16[16,384,128]{2,1,0:T(8,128)(2,1)} %broadcast_in_dim.27), calls=%async_computation.1 | async-start | bytes 3145728 | tf_op jit(solution)/shard_map/all_to_all | solution.py:356
  47.0 15.3 %mixer_local.1 = (f32[64,1024]{1,0:T(8,128)}, bf16[128,1024]{1,0:T(8,128)(2,1)}, bf16[2,64,128]{2,1,0:T(8,128)(2,1)}) custom-call(bf16[64,1024]{1,0:T(8,128)(2,1)} %q_ref, bf16[64,1024]{1,0:T(8,128)(2,1)} %k_ref.1, bf16[64,1024]{1,0:T(8,128)(2,1)} %v_ref.1, bf16[64,1024]{1,0:T(8,128)(2,1)} %e_ref.1, bf16[64,1024]{1,0:T(8,128)(2,1)} %d_ref.1), custom_call_target="tpu_custom_call" | custom-call | flops 1476395008 | bytes 1179648 | tf_op jit(solution)/shard_map/mixer_local/pallas_call | solution.py:155
  62.4 5.6 %all-to-all-done.1.rows_ref = bf16[16,384,128]{2,1,0:T(8,128)(2,1)} async-done(((bf16[16,384,128]{2,1,0:T(8,128)(2,1)}), bf16[16,384,128]{2,1,0:T(8,128)(2,1)}, u32[]{:S(2)}, u32[]{:S(2)}) %all-to-all-start.1) | async-done | bytes 1572896 | tf_op jit(solution)/shard_map/all_to_all | solution.py:356
  68.0 1.5 broadcast_in_dim.29
  69.5 0.0 copy-start.2
  69.5 0.0 copy-start.3
  69.5 6.4 %all-to-all-start.2 = ((bf16[16,384,128]{2,1,0:T(8,128)(2,1)}), bf16[16,384,128]{2,1,0:T(8,128)(2,1)}, u32[]{:S(2)}, u32[]{:S(2)}) async-start(bf16[16,384,128]{2,1,0:T(8,128)(2,1)} %broadcast_in_dim.29), calls=%async_computation.2 | async-start | bytes 3145728 | tf_op jit(solution)/shard_map/all_to_all | solution.py:356
  75.8 0.0 copy-done.2
  75.8 0.0 copy-start.4
  75.8 4.1 %collective-permute-start = (bf16[2,64,128]{2,1,0:T(8,128)(2,1)S(1)}, bf16[2,64,128]{2,1,0:T(8,128)(2,1)S(1)}, u32[]{:S(2)}, u32[]{:S(2)}) collective-permute-start(bf16[2,64,128]{2,1,0:T(8,128)(2,1)S(1)} %copy-done.2), channel_id=1, source_target_pairs={{0,16},{16,0},{32,48},{48,32},{64,80},{80,64},{96,112},{112,96},{1... | collective-permute-start | bytes 98312 | tf_op jit(solution)/shard_map/ppermute | solution.py:265
  80.0 0.0 copy-done.3
  80.0 1.3 copy.15
  81.3 0.0 copy-done.4
  81.3 1.3 copy.16
  82.6 0.0 collective-permute-done.arrived_ref
  82.6 0.3 scan_step.4
  83.0 2.3 %collective-permute-start.1 = (bf16[2,64,128]{2,1,0:T(8,128)(2,1)S(1)}, bf16[2,64,128]{2,1,0:T(8,128)(2,1)S(1)}, u32[]{:S(2)}, u32[]{:S(2)}) collective-permute-start(bf16[2,64,128]{2,1,0:T(8,128)(2,1)S(1)} %get-tuple-element.41.through_ref), channel_id=1, source_target_pairs={{0,32},{16,48},{32,0},{48,16},{64,96},{80,112},{96,64},{112,80},{1... | collective-permute-start | bytes 98312 | tf_op jit(solution)/shard_map/ppermute | solution.py:265
  85.3 5.5 %expert_rows.2 = bf16[16,384,128]{2,1,0:T(8,128)(2,1)} custom-call(bf16[16,384,128]{2,1,0:T(8,128)(2,1)} %all-to-all-done.1.rows_ref, bf16[2048,224]{1,0:T(8,128)(2,1)} %bitcast.20, bf16[2048,224]{1,0:T(8,128)(2,1)} %bitcast.22, bf16[224,2048]{1,0:T(8,128)(2,1)} %bitcast.24), custom_call_target="tpu_custom_call" | custom-call | flops 1056964608 | bytes 5898240 | tf_op jit(solution)/shard_map/expert_rows/pallas_call | solution.py:288
  90.8 0.0 collective-permute-done.1.arrived_ref
  90.8 0.3 scan_step.5
  91.1 5.4 %all-to-all-done.2.rows_ref = bf16[16,384,128]{2,1,0:T(8,128)(2,1)} async-done(((bf16[16,384,128]{2,1,0:T(8,128)(2,1)}), bf16[16,384,128]{2,1,0:T(8,128)(2,1)}, u32[]{:S(2)}, u32[]{:S(2)}) %all-to-all-start.2) | async-done | bytes 1572896 | tf_op jit(solution)/shard_map/all_to_all | solution.py:356
  96.5 5.7 %all-to-all-start.3 = ((bf16[16,384,128]{2,1,0:T(8,128)(2,1)}), bf16[16,384,128]{2,1,0:T(8,128)(2,1)}, u32[]{:S(2)}, u32[]{:S(2)}) async-start(bf16[16,384,128]{2,1,0:T(8,128)(2,1)} %expert_rows.2), calls=%async_computation.3 | async-start | bytes 3145728 | tf_op jit(solution)/shard_map/all_to_all | solution.py:356
  102.2 6.2 %collective-permute-start.2 = (bf16[2,64,128]{2,1,0:T(8,128)(2,1)S(1)}, bf16[2,64,128]{2,1,0:T(8,128)(2,1)S(1)}, u32[]{:S(2)}, u32[]{:S(2)}) collective-permute-start(bf16[2,64,128]{2,1,0:T(8,128)(2,1)S(1)} %get-tuple-element.47.through_ref), channel_id=1, source_target_pairs={{0,64},{16,80},{32,96},{48,112},{64,0},{80,16},{96,32},{112,48},{1... | collective-permute-start | bytes 98312 | tf_op jit(solution)/shard_map/ppermute | solution.py:265
  108.5 5.5 %expert_rows.3 = bf16[16,384,128]{2,1,0:T(8,128)(2,1)} custom-call(bf16[16,384,128]{2,1,0:T(8,128)(2,1)} %all-to-all-done.2.rows_ref, bf16[2048,224]{1,0:T(8,128)(2,1)} %bitcast.21, bf16[2048,224]{1,0:T(8,128)(2,1)} %bitcast.23, bf16[224,2048]{1,0:T(8,128)(2,1)} %bitcast.25), custom_call_target="tpu_custom_call" | custom-call | flops 1056964608 | bytes 5898240 | tf_op jit(solution)/shard_map/expert_rows/pallas_call | solution.py:288
  113.9 0.0 collective-permute-done.2.arrived_ref
  113.9 0.3 scan_step.6
  114.3 8.1 %all-to-all-done.3 = bf16[16,384,128]{2,1,0:T(8,128)(2,1)} async-done(((bf16[16,384,128]{2,1,0:T(8,128)(2,1)}), bf16[16,384,128]{2,1,0:T(8,128)(2,1)}, u32[]{:S(2)}, u32[]{:S(2)}) %all-to-all-start.3) | async-done | bytes 1572896 | tf_op jit(solution)/shard_map/all_to_all | solution.py:356
  122.4 5.4 %all-to-all-start.4 = ((bf16[16,384,128]{2,1,0:T(8,128)(2,1)}), bf16[16,384,128]{2,1,0:T(8,128)(2,1)S(1)}, u32[]{:S(2)}, u32[]{:S(2)}) async-start(bf16[16,384,128]{2,1,0:T(8,128)(2,1)} %expert_rows.3), calls=%async_computation.4 | async-start | bytes 3145728 | tf_op jit(solution)/shard_map/all_to_all | solution.py:356
  127.8 11.7 %collective-permute-start.3 = (bf16[2,64,128]{2,1,0:T(8,128)(2,1)S(1)}, bf16[2,64,128]{2,1,0:T(8,128)(2,1)S(1)}, u32[]{:S(2)}, u32[]{:S(2)}) collective-permute-start(bf16[2,64,128]{2,1,0:T(8,128)(2,1)S(1)} %get-tuple-element.53.through_ref), channel_id=1, source_target_pairs={{0,128},{16,144},{32,160},{48,176},{64,192},{80,208},{96,224},{112... | collective-permute-start | bytes 98312 | tf_op jit(solution)/shard_map/ppermute | solution.py:265
  139.5 1.6 reduce_sum.24
  141.1 0.0 copy-start.6
  141.1 0.0 copy-start
  141.1 0.0 copy-start.1
  141.1 0.1 collective-permute-done.3.arrived_ref
  141.2 0.3 scan_step.7
  141.6 6.2 %all-to-all-done.4 = bf16[16,384,128]{2,1,0:T(8,128)(2,1)S(1)} async-done(((bf16[16,384,128]{2,1,0:T(8,128)(2,1)}), bf16[16,384,128]{2,1,0:T(8,128)(2,1)S(1)}, u32[]{:S(2)}, u32[]{:S(2)}) %all-to-all-start.4) | async-done | bytes 1572896 | tf_op jit(solution)/shard_map/all_to_all | solution.py:356
  147.7 0.0 copy-start.5
  147.7 0.2 reduce_sum.25
  148.0 0.7 pad_maximum_fusion
  148.6 16.5 %all-to-all-start.5 = ((bf16[32,24,128]{2,1,0:T(8,128)(2,1)}), bf16[32,24,128]{2,1,0:T(8,128)(2,1)S(1)}, u32[]{:S(2)}, u32[]{:S(2)}) async-start(bf16[32,24,128]{2,1,0:T(8,128)(2,1)} %bitcast.16), calls=%async_computation.5 | async-start | bytes 393216 | tf_op jit(solution)/shard_map/all_to_all | solution.py:356
  165.1 12.0 %collective-permute-start.4 = (bf16[2,64,128]{2,1,0:T(8,128)(2,1)S(1)}, bf16[2,64,128]{2,1,0:T(8,128)(2,1)S(1)}, u32[]{:S(2)}, u32[]{:S(2)}) collective-permute-start(bf16[2,64,128]{2,1,0:T(8,128)(2,1)S(1)} %get-tuple-element.57), channel_id=1, source_target_pairs={{0,256},{16,272},{32,288},{48,304},{64,320},{80,336},{96,352},{112... | collective-permute-start | bytes 98312 | tf_op jit(solution)/shard_map/ppermute | solution.py:265
  177.1 0.0 copy-done.6
  177.1 0.1 copy.17.gain_ref
  177.2 10.0 %collective-permute-done.4.arrived_ref = bf16[2,64,128]{2,1,0:T(8,128)(2,1)S(1)} collective-permute-done((bf16[2,64,128]{2,1,0:T(8,128)(2,1)S(1)}, bf16[2,64,128]{2,1,0:T(8,128)(2,1)S(1)}, u32[]{:S(2)}, u32[]{:S(2)}) %collective-permute-start.4) | collective-permute-done | bytes 32800 | tf_op jit(solution)/shard_map/ppermute | solution.py:265
  187.2 0.0 copy-done
  187.2 0.0 copy-done.1
  187.2 1.2 mixer_finish.1
  188.4 0.0 all-to-all-done.5
  188.4 0.0 copy-done.5
  188.4 0.9 convolution_convert_fusion
  (2 shorter events, 0.0 us)
Async XLA Ops:
  40.2 27.8 %all-to-all-start.1 = ((bf16[16,384,128]{2,1,0:T(8,128)(2,1)}), bf16[16,384,128]{2,1,0:T(8,128)(2,1)}, u32[]{:S(2)}, u32[]{:S(2)}) async-start(bf16[16,384,128]{2,1,0:T(8,128)(2,1)} %broadcast_in_dim.27), calls=%async_computation.1 | async-start | bytes 3145728 | tf_op jit(solution)/shard_map/all_to_all | solution.py:356
  69.5 6.4 %copy-start.2 = (bf16[2,64,128]{2,1,0:T(8,128)(2,1)S(1)}, bf16[2,64,128]{2,1,0:T(8,128)(2,1)}, u32[]{:S(2)}) copy-start(bf16[2,64,128]{2,1,0:T(8,128)(2,1)} %get-tuple-element.39.through_ref) | copy-start | bytes 98308
  69.5 10.5 %copy-start.3 = (bf16[1,2048,224]{1,2,0:T(8,128)(2,1)S(1)}, bf16[1,2048,224]{1,2,0:T(8,128)(2,1)}, u32[]{:S(2)}) copy-start(bf16[1,2048,224]{1,2,0:T(8,128)(2,1)} %param.23) | copy-start | bytes 2752516
  69.5 27.0 %all-to-all-start.2 = ((bf16[16,384,128]{2,1,0:T(8,128)(2,1)}), bf16[16,384,128]{2,1,0:T(8,128)(2,1)}, u32[]{:S(2)}, u32[]{:S(2)}) async-start(bf16[16,384,128]{2,1,0:T(8,128)(2,1)} %broadcast_in_dim.29), calls=%async_computation.2 | async-start | bytes 3145728 | tf_op jit(solution)/shard_map/all_to_all | solution.py:356
  75.8 5.4 %copy-start.4 = (bf16[1,2048,224]{1,2,0:T(8,128)(2,1)S(1)}, bf16[1,2048,224]{1,2,0:T(8,128)(2,1)}, u32[]{:S(2)}) copy-start(bf16[1,2048,224]{1,2,0:T(8,128)(2,1)} %param.24) | copy-start | bytes 2752516
  75.8 6.8 %collective-permute-start = (bf16[2,64,128]{2,1,0:T(8,128)(2,1)S(1)}, bf16[2,64,128]{2,1,0:T(8,128)(2,1)S(1)}, u32[]{:S(2)}, u32[]{:S(2)}) collective-permute-start(bf16[2,64,128]{2,1,0:T(8,128)(2,1)S(1)} %copy-done.2), channel_id=1, source_target_pairs={{0,16},{16,0},{32,48},{48,32},{64,80},{80,64},{96,112},{112,96},{1... | collective-permute-start | bytes 98312 | tf_op jit(solution)/shard_map/ppermute | solution.py:265
  83.0 7.8 %collective-permute-start.1 = (bf16[2,64,128]{2,1,0:T(8,128)(2,1)S(1)}, bf16[2,64,128]{2,1,0:T(8,128)(2,1)S(1)}, u32[]{:S(2)}, u32[]{:S(2)}) collective-permute-start(bf16[2,64,128]{2,1,0:T(8,128)(2,1)S(1)} %get-tuple-element.41.through_ref), channel_id=1, source_target_pairs={{0,32},{16,48},{32,0},{48,16},{64,96},{80,112},{96,64},{112,80},{1... | collective-permute-start | bytes 98312 | tf_op jit(solution)/shard_map/ppermute | solution.py:265
  96.5 25.9 %all-to-all-start.3 = ((bf16[16,384,128]{2,1,0:T(8,128)(2,1)}), bf16[16,384,128]{2,1,0:T(8,128)(2,1)}, u32[]{:S(2)}, u32[]{:S(2)}) async-start(bf16[16,384,128]{2,1,0:T(8,128)(2,1)} %expert_rows.2), calls=%async_computation.3 | async-start | bytes 3145728 | tf_op jit(solution)/shard_map/all_to_all | solution.py:356
  102.2 11.7 %collective-permute-start.2 = (bf16[2,64,128]{2,1,0:T(8,128)(2,1)S(1)}, bf16[2,64,128]{2,1,0:T(8,128)(2,1)S(1)}, u32[]{:S(2)}, u32[]{:S(2)}) collective-permute-start(bf16[2,64,128]{2,1,0:T(8,128)(2,1)S(1)} %get-tuple-element.47.through_ref), channel_id=1, source_target_pairs={{0,64},{16,80},{32,96},{48,112},{64,0},{80,16},{96,32},{112,48},{1... | collective-permute-start | bytes 98312 | tf_op jit(solution)/shard_map/ppermute | solution.py:265
  122.4 25.3 %all-to-all-start.4 = ((bf16[16,384,128]{2,1,0:T(8,128)(2,1)}), bf16[16,384,128]{2,1,0:T(8,128)(2,1)S(1)}, u32[]{:S(2)}, u32[]{:S(2)}) async-start(bf16[16,384,128]{2,1,0:T(8,128)(2,1)} %expert_rows.3), calls=%async_computation.4 | async-start | bytes 3145728 | tf_op jit(solution)/shard_map/all_to_all | solution.py:356
  127.8 13.5 %collective-permute-start.3 = (bf16[2,64,128]{2,1,0:T(8,128)(2,1)S(1)}, bf16[2,64,128]{2,1,0:T(8,128)(2,1)S(1)}, u32[]{:S(2)}, u32[]{:S(2)}) collective-permute-start(bf16[2,64,128]{2,1,0:T(8,128)(2,1)S(1)} %get-tuple-element.53.through_ref), channel_id=1, source_target_pairs={{0,128},{16,144},{32,160},{48,176},{64,192},{80,208},{96,224},{112... | collective-permute-start | bytes 98312 | tf_op jit(solution)/shard_map/ppermute | solution.py:265
  141.1 36.0 %copy-start.6 = (f32[64]{0:T(128)S(1)}, f32[64]{0:T(128)}, u32[]{:S(2)}) copy-start(f32[64]{0:T(128)} %param.18) | copy-start | bytes 772
  141.1 46.1 %copy-start = (f32[64,1024]{1,0:T(8,128)S(1)}, f32[64,1024]{1,0:T(8,128)}, u32[]{:S(2)}) copy-start(f32[64,1024]{1,0:T(8,128)} %get-tuple-element.59.oloc_ref) | copy-start | bytes 786436
  141.1 46.1 %copy-start.1 = (bf16[128,1024]{1,0:T(8,128)(2,1)S(1)}, bf16[128,1024]{1,0:T(8,128)(2,1)}, u32[]{:S(2)}) copy-start(bf16[128,1024]{1,0:T(8,128)(2,1)} %get-tuple-element.60.qp_ref) | copy-start | bytes 786436
  147.7 40.7 %copy-start.5 = (bf16[768,256]{1,0:T(8,128)(2,1)S(1)}, bf16[768,256]{1,0:T(8,128)(2,1)}, u32[]{:S(2)}) copy-start(bf16[768,256]{1,0:T(8,128)(2,1)} %get-tuple-element.61) | copy-start | bytes 1179652
  148.6 39.8 %all-to-all-start.5 = ((bf16[32,24,128]{2,1,0:T(8,128)(2,1)}), bf16[32,24,128]{2,1,0:T(8,128)(2,1)S(1)}, u32[]{:S(2)}, u32[]{:S(2)}) async-start(bf16[32,24,128]{2,1,0:T(8,128)(2,1)} %bitcast.16), calls=%async_computation.5 | async-start | bytes 393216 | tf_op jit(solution)/shard_map/all_to_all | solution.py:356
  165.1 22.1 %collective-permute-start.4 = (bf16[2,64,128]{2,1,0:T(8,128)(2,1)S(1)}, bf16[2,64,128]{2,1,0:T(8,128)(2,1)S(1)}, u32[]{:S(2)}, u32[]{:S(2)}) collective-permute-start(bf16[2,64,128]{2,1,0:T(8,128)(2,1)S(1)} %get-tuple-element.57), channel_id=1, source_target_pairs={{0,256},{16,272},{32,288},{48,304},{64,320},{80,336},{96,352},{112... | collective-permute-start | bytes 98312 | tf_op jit(solution)/shard_map/ppermute | solution.py:265

commit v5 on v4

--- a/solution.py
+++ b/solution.py
@@ -224,7 +224,7 @@
         cost_estimate=pl.CostEstimate(
             flops=6 * 128**3, bytes_accessed=6 * 2 * past.size, transcendentals=0
         ),
-        compiler_params=pltpu.CompilerParams(vmem_limit_bytes=4 * 2**20),
+        compiler_params=pltpu.CompilerParams(vmem_limit_bytes=66000000),
         name="scan_step",
     )(upper, arrived, through, past)
 
@@ -389,49 +389,50 @@
     arrived = spread(outgoing.reshape(experts_n, capacity, col_count), "ep").reshape(
         slot_total, col_count
     )
+    oloc, qp, own_maps = local_half(query_in, key_in, value_in, erase_pre, decay_pre)
+    arrived, own_maps = lax.optimization_barrier((arrived, own_maps))
     middle = slot_total // 2
     copies = [
         jnp.broadcast_to(part[None], (shares, *part.shape))
         for part in (arrived[:middle], arrived[middle:])
     ]
-    copies[0], query_in = lax.optimization_barrier((copies[0], query_in))
+    copies[0], own_maps = lax.optimization_barrier((copies[0], own_maps))
     shared_a = spread(copies[0], "tp")
-    oloc, qp, own_maps = local_half(query_in, key_in, value_in, erase_pre, decay_pre)
     past, through = jnp.zeros(own_maps.shape, jnp.float32), own_maps
     weights = [gate_weight[0], up_weight[0], down_weight[0]]
-    shared_a, copies[1], past, through = lax.optimization_barrier(
-        (shared_a, copies[1], past, through)
-    )
 
     def scanned(steps, past, through):
         for step in steps:
             past, through = scan_step(side(step), swapped(through, step), through, past)
         return past, through
 
+    past, through = scanned((1,), past, through)
+    copies[1], past, through = lax.optimization_barrier((copies[1], past, through))
+    past, through = scanned((2,), past, through)
+    shared_a, copies[1], past, through = lax.optimization_barrier(
+        (shared_a, copies[1], past, through)
+    )
     shared_b = spread(copies[1], "tp")
     partial_a = expert_rows(shared_a, *weights)
-    past, through = scanned((1, 2), past, through)
+    past, through = scanned((4,), past, through)
     shared_b, partial_a, past, through = lax.optimization_barrier(
         (shared_b, partial_a, past, through)
     )
     pieces_a = spread(partial_a, "tp")
     partial_b = expert_rows(shared_b, *weights)
-    past, through = scanned((4,), past, through)
+    past, through = scanned((8,), past, through)
     pieces_a, partial_b, past, through = lax.optimization_barrier(
         (pieces_a, partial_b, past, through)
     )
     pieces_b = spread(partial_b, "tp")
     summed_a = summed_pieces(pieces_a)
-    past, through = scanned((8,), past, through)
-    pieces_b, summed_a, past, through = lax.optimization_barrier(
-        (pieces_b, summed_a, past, through)
-    )
+    distance = experts_n // 2
+    crossing = swapped(through, distance)
+    pieces_b, summed_a, crossing = lax.optimization_barrier((pieces_b, summed_a, crossing))
     summed = jnp.concatenate([summed_a, summed_pieces(pieces_b)], axis=0)
     returned = spread(summed.reshape(experts_n, capacity, col_count), "ep").reshape(
         slot_total, col_count
     )
-    distance = experts_n // 2
-    crossing = swapped(through, distance)
     mixer_out = finish_half(side(distance), crossing, past, oloc, qp, mix_gain[:, None])
     expert_out = mm_tn(combine, returned).astype(jnp.bfloat16)
     return (mixer_out, expert_out)

time: 190 us -> 184 us (0.968)
  blocking collectives: 35.5 us -> 0 us
  waiting for transfers between devices: 35.4 us -> 48.8 us
  starting transfers between devices: 77 us -> 83.6 us
  Pallas kernels: 31.4 us -> 37.5 us
  local copies, waits for them, and re-layouts: 5.72 us -> 8.22 us
    all_to_all x1 -> x0, blocking collectives: 35.5 us -> none  [spread(): return lax.all_to_all(array, axis, 0, 0, tiled=True)]
    all_to_all x5 -> x6, waiting for transfers between devices: 25.3 us -> 44 us  [spread(): return lax.all_to_all(array, axis, 0, 0, tiled=True)]
    all_to_all x5 -> x6, starting transfers between devices: 40.7 us -> 56.6 us  [spread(): return lax.all_to_all(array, axis, 0, 0, tiled=True)]
    ppermute x5, starting transfers between devices: 36.3 us -> 27.1 us  [swapped(): lax.ppermute(through, 'ep', [(i, i ^ distance) for i in range(count)])]
    pallas_call x4, Pallas kernels: 1.29 us -> 7.35 us  [scan_step(): pl.pallas_call(step_kernel, out_shape=(jax.ShapeDtypeStruct(past.shape, j...]
    ppermute x5, waiting for transfers between devices: 10.1 us -> 4.79 us  [swapped(): lax.ppermute(through, 'ep', [(i, i ^ distance) for i in range(count)])]
    unnamed x16 -> x34, local copies, waits for them, and re-layouts: 2.68 us -> 4.55 us
  transfers between devices with their start and end apart: 10 -> 11, of which waited for: 6 -> 9; matrix products, arithmetic and copies ran while one was open for 2% -> 4% of each run, Pallas kernels for 15% -> 19%
where the time goes in v5:
time: 184 us; the launch traced here: 182 us
  starting transfers between devices  83.6 us (45%)
  waiting for transfers between devices  48.8 us (27%)
  Pallas kernels  37.5 us (20%)
  local copies, waits for them, and re-layouts  8.22 us (4%)
  other arithmetic  2.54 us (1%)
    all_to_all x6, starting transfers between devices, spread(): return lax.all_to_all(array, axis, 0, 0, tiled=True)  56.6 us
    all_to_all x6, waiting for transfers between devices, spread(): return lax.all_to_all(array, axis, 0, 0, tiled=True)  44 us
    ppermute x5, starting transfers between devices, swapped(): lax.ppermute(through, 'ep', [(i, i ^ distance) for i in range(count)])  27.1 us
    pallas_call x1, Pallas kernels, local_half(): pl.pallas_call(local_kernel, out_shape=(full(jnp.float32), jax.ShapeDtype...  15.3 us
    pallas_call x2, Pallas kernels, expert_rows(): pl.pallas_call(expert_kernel, grid=(total // tile,), in_specs=[block, fix...  11 us
    pallas_call x4, Pallas kernels, scan_step(): pl.pallas_call(step_kernel, out_shape=(jax.ShapeDtypeStruct(past.shape, j...  7.35 us
    ppermute x5, waiting for transfers between devices, swapped(): lax.ppermute(through, 'ep', [(i, i ^ distance) for i in range(count)])  4.79 us
    unnamed x34, local copies, waits for them, and re-layouts  4.55 us
  transfers between devices with their start and end apart: 11, of which 9 were waited for; matrix products, arithmetic and copies ran while one was open for 4% of the time, Pallas kernels for 19%

profile of v5, /device:TPU:1, one launch (start us, length us, event | category | flops | bytes accessed | tf_op | source)
XLA Modules:
  0.0 182.5 jit_solution(15635904931281267251)
XLA Ops:
  0.6 2.6 %route_rows.1 = (bf16[768,128]{1,0:T(8,128)(2,1)}, bf16[768,256]{1,0:T(8,128)(2,1)}) custom-call(s32[1]{0:T(128)} %bitcast.1.at_ref, bf16[256,2048]{1,0:T(8,128)(2,1)} %rows_ref.1, f32[1,2048]{1,0:T(1,128)} %bitcast.28, s32[2,256]{1,0:T(2,128)} %bitcast.29, f32[2,256]{1,0:T(2,128)} %bitcast.30), custom_call_target="tpu_custom_call" | custom-call | flops 100663296 | bytes 1048576 | tf_op jit(solution)/shard_map/route_rows/pallas_call | solution.py:336
  3.2 16.7 %all-to-all-start = ((bf16[32,24,128]{2,1,0:T(8,128)(2,1)}), bf16[32,24,128]{2,1,0:T(8,128)(2,1)S(1)}, u32[]{:S(2)}, u32[]{:S(2)}) async-start(bf16[32,24,128]{2,1,0:T(8,128)(2,1)} %bitcast.27), calls=%async_computation | async-start | bytes 393216 | tf_op jit(solution)/shard_map/all_to_all | solution.py:356
  20.0 15.3 %mixer_local.1 = (f32[64,1024]{1,0:T(8,128)}, bf16[128,1024]{1,0:T(8,128)(2,1)}, bf16[2,64,128]{2,1,0:T(8,128)(2,1)}) custom-call(bf16[64,1024]{1,0:T(8,128)(2,1)} %q_ref.1, bf16[64,1024]{1,0:T(8,128)(2,1)} %k_ref.1, bf16[64,1024]{1,0:T(8,128)(2,1)} %v_ref.1, bf16[64,1024]{1,0:T(8,128)(2,1)} %e_ref.1, bf16[64,1024]{1,0:T(8,128)(2,1)} %d_ref.1), custom_call_target="tpu_custom_call" | custom-call | flops 1476395008 | bytes 1179648 | tf_op jit(solution)/shard_map/mixer_local/pallas_call | solution.py:155
  35.3 3.4 %all-to-all-done = bf16[32,24,128]{2,1,0:T(8,128)(2,1)S(1)} async-done(((bf16[32,24,128]{2,1,0:T(8,128)(2,1)}), bf16[32,24,128]{2,1,0:T(8,128)(2,1)S(1)}, u32[]{:S(2)}, u32[]{:S(2)}) %all-to-all-start) | async-done | bytes 196640 | tf_op jit(solution)/shard_map/all_to_all | solution.py:356
  38.8 1.5 broadcast_in_dim.22
  40.2 6.9 %all-to-all-start.1 = ((bf16[16,384,128]{2,1,0:T(8,128)(2,1)}), bf16[16,384,128]{2,1,0:T(8,128)(2,1)}, u32[]{:S(2)}, u32[]{:S(2)}) async-start(bf16[16,384,128]{2,1,0:T(8,128)(2,1)} %broadcast_in_dim.22), calls=%async_computation.1 | async-start | bytes 3145728 | tf_op jit(solution)/shard_map/all_to_all | solution.py:356
  47.2 0.0 copy-done.6
  47.2 3.6 %collective-permute-start = (bf16[2,64,128]{2,1,0:T(8,128)(2,1)S(1)}, bf16[2,64,128]{2,1,0:T(8,128)(2,1)S(1)}, u32[]{:S(2)}, u32[]{:S(2)}) collective-permute-start(bf16[2,64,128]{2,1,0:T(8,128)(2,1)S(1)} %copy-done.6), channel_id=1, source_target_pairs={{0,16},{16,0},{32,48},{48,32},{64,80},{80,64},{96,112},{112,96},{1... | collective-permute-start | bytes 98312 | tf_op jit(solution)/shard_map/ppermute | solution.py:265
  50.8 0.8 collective-permute-done.arrived_ref
  51.7 0.6 broadcast_in_dim.24.past_ref
  52.3 0.0 copy-done.10
  52.3 1.8 %scan_step.4 = (f32[2,64,128]{2,1,0:T(8,128)}, bf16[2,64,128]{2,1,0:T(8,128)(2,1)}) custom-call(s32[1]{0:T(128)} %bitcast.7.upper_ref, bf16[2,64,128]{2,1,0:T(8,128)(2,1)} %copy-done.10, bf16[2,64,128]{2,1,0:T(8,128)(2,1)} %get-tuple-element.42.through_ref, f32[2,64,128]{2,1,0:T(8,128)} %broadcast_in_dim.24.past_ref), custom_call_target="tpu_custom_call" | custom-call | flops 12582912 | bytes 196608 | tf_op jit(solution)/shard_map/scan_step/pallas_call | solution.py:216
  54.2 1.5 broadcast_in_dim.23
  55.6 0.0 copy-done.9
  55.6 1.9 %collective-permute-start.1 = (bf16[2,64,128]{2,1,0:T(8,128)(2,1)S(1)}, bf16[2,64,128]{2,1,0:T(8,128)(2,1)S(1)}, u32[]{:S(2)}, u32[]{:S(2)}) collective-permute-start(bf16[2,64,128]{2,1,0:T(8,128)(2,1)S(1)} %copy-done.9), channel_id=1, source_target_pairs={{0,32},{16,48},{32,0},{48,16},{64,96},{80,112},{96,64},{112,80},{1... | collective-permute-start | bytes 98312 | tf_op jit(solution)/shard_map/ppermute | solution.py:265
  57.5 3.1 %collective-permute-done.1.arrived_ref = bf16[2,64,128]{2,1,0:T(8,128)(2,1)S(1)} collective-permute-done((bf16[2,64,128]{2,1,0:T(8,128)(2,1)S(1)}, bf16[2,64,128]{2,1,0:T(8,128)(2,1)S(1)}, u32[]{:S(2)}, u32[]{:S(2)}) %collective-permute-start.1) | collective-permute-done | bytes 32800 | tf_op jit(solution)/shard_map/ppermute | solution.py:265
  60.7 0.6 copy-done.13
  61.3 1.8 %scan_step.5 = (f32[2,64,128]{2,1,0:T(8,128)}, bf16[2,64,128]{2,1,0:T(8,128)(2,1)}) custom-call(s32[1]{0:T(128)} %bitcast.8.upper_ref, bf16[2,64,128]{2,1,0:T(8,128)(2,1)} %copy-done.13, bf16[2,64,128]{2,1,0:T(8,128)(2,1)} %get-tuple-element.46.through_ref, f32[2,64,128]{2,1,0:T(8,128)} %get-tuple-element.47.past_ref), custom_call_target="tpu_custom_call" | custom-call | flops 12582912 | bytes 196608 | tf_op jit(solution)/shard_map/scan_step/pallas_call | solution.py:216
  63.1 5.0 %all-to-all-done.1.rows_ref = bf16[16,384,128]{2,1,0:T(8,128)(2,1)} async-done(((bf16[16,384,128]{2,1,0:T(8,128)(2,1)}), bf16[16,384,128]{2,1,0:T(8,128)(2,1)}, u32[]{:S(2)}, u32[]{:S(2)}) %all-to-all-start.1) | async-done | bytes 1572896 | tf_op jit(solution)/shard_map/all_to_all | solution.py:356
  68.1 6.4 %all-to-all-start.2 = ((bf16[16,384,128]{2,1,0:T(8,128)(2,1)}), bf16[16,384,128]{2,1,0:T(8,128)(2,1)}, u32[]{:S(2)}, u32[]{:S(2)}) async-start(bf16[16,384,128]{2,1,0:T(8,128)(2,1)} %broadcast_in_dim.23), calls=%async_computation.2 | async-start | bytes 3145728 | tf_op jit(solution)/shard_map/all_to_all | solution.py:356
  74.5 0.0 copy-start.4
  74.5 0.0 copy-done.3
  74.5 0.0 copy-start.7
  74.5 1.4 copy.16
  75.9 0.0 copy-done.4
  75.9 1.3 copy.15
  77.2 0.0 copy-done.7
  77.2 5.1 %collective-permute-start.2 = (bf16[2,64,128]{2,1,0:T(8,128)(2,1)S(1)}, bf16[2,64,128]{2,1,0:T(8,128)(2,1)S(1)}, u32[]{:S(2)}, u32[]{:S(2)}) collective-permute-start(bf16[2,64,128]{2,1,0:T(8,128)(2,1)S(1)} %copy-done.7), channel_id=1, source_target_pairs={{0,64},{16,80},{32,96},{48,112},{64,0},{80,16},{96,32},{112,48},{1... | collective-permute-start | bytes 98312 | tf_op jit(solution)/shard_map/ppermute | solution.py:265
  82.3 5.5 %expert_rows.2 = bf16[16,384,128]{2,1,0:T(8,128)(2,1)} custom-call(bf16[16,384,128]{2,1,0:T(8,128)(2,1)} %all-to-all-done.1.rows_ref, bf16[2048,224]{1,0:T(8,128)(2,1)} %bitcast.21, bf16[2048,224]{1,0:T(8,128)(2,1)} %bitcast.19, bf16[224,2048]{1,0:T(8,128)(2,1)} %bitcast.23), custom_call_target="tpu_custom_call" | custom-call | flops 1056964608 | bytes 5898240 | tf_op jit(solution)/shard_map/expert_rows/pallas_call | solution.py:288
  87.8 0.0 collective-permute-done.2.arrived_ref
  87.8 0.6 copy-done.12
  88.5 1.8 %scan_step.6 = (f32[2,64,128]{2,1,0:T(8,128)}, bf16[2,64,128]{2,1,0:T(8,128)(2,1)}) custom-call(s32[1]{0:T(128)} %bitcast.12.upper_ref, bf16[2,64,128]{2,1,0:T(8,128)(2,1)} %copy-done.12, bf16[2,64,128]{2,1,0:T(8,128)(2,1)} %get-tuple-element.52.through_ref, f32[2,64,128]{2,1,0:T(8,128)} %get-tuple-element.53.past_ref), custom_call_target="tpu_custom_call" | custom-call | flops 12582912 | bytes 196608 | tf_op jit(solution)/shard_map/scan_step/pallas_call | solution.py:216
  90.3 4.9 %all-to-all-done.2.rows_ref = bf16[16,384,128]{2,1,0:T(8,128)(2,1)} async-done(((bf16[16,384,128]{2,1,0:T(8,128)(2,1)}), bf16[16,384,128]{2,1,0:T(8,128)(2,1)}, u32[]{:S(2)}, u32[]{:S(2)}) %all-to-all-start.2) | async-done | bytes 1572896 | tf_op jit(solution)/shard_map/all_to_all | solution.py:356
  95.2 5.9 %all-to-all-start.3 = ((bf16[16,384,128]{2,1,0:T(8,128)(2,1)}), bf16[16,384,128]{2,1,0:T(8,128)(2,1)}, u32[]{:S(2)}, u32[]{:S(2)}) async-start(bf16[16,384,128]{2,1,0:T(8,128)(2,1)} %expert_rows.2), calls=%async_computation.3 | async-start | bytes 3145728 | tf_op jit(solution)/shard_map/all_to_all | solution.py:356
  101.1 0.0 copy-done.8
  101.1 5.5 %collective-permute-start.3 = (bf16[2,64,128]{2,1,0:T(8,128)(2,1)S(1)}, bf16[2,64,128]{2,1,0:T(8,128)(2,1)S(1)}, u32[]{:S(2)}, u32[]{:S(2)}) collective-permute-start(bf16[2,64,128]{2,1,0:T(8,128)(2,1)S(1)} %copy-done.8), channel_id=1, source_target_pairs={{0,128},{16,144},{32,160},{48,176},{64,192},{80,208},{96,224},{112... | collective-permute-start | bytes 98312 | tf_op jit(solution)/shard_map/ppermute | solution.py:265
  106.6 5.5 %expert_rows.3 = bf16[16,384,128]{2,1,0:T(8,128)(2,1)} custom-call(bf16[16,384,128]{2,1,0:T(8,128)(2,1)} %all-to-all-done.2.rows_ref, bf16[2048,224]{1,0:T(8,128)(2,1)} %bitcast.22, bf16[2048,224]{1,0:T(8,128)(2,1)} %bitcast.20, bf16[224,2048]{1,0:T(8,128)(2,1)} %bitcast.24), custom_call_target="tpu_custom_call" | custom-call | flops 1056964608 | bytes 5898240 | tf_op jit(solution)/shard_map/expert_rows/pallas_call | solution.py:288
  112.1 0.0 collective-permute-done.3.arrived_ref
  112.1 0.6 copy-done.11
  112.7 1.8 %scan_step.7 = (f32[2,64,128]{2,1,0:T(8,128)}, bf16[2,64,128]{2,1,0:T(8,128)(2,1)}) custom-call(s32[1]{0:T(128)} %bitcast.13.upper_ref, bf16[2,64,128]{2,1,0:T(8,128)(2,1)} %copy-done.11, bf16[2,64,128]{2,1,0:T(8,128)(2,1)} %get-tuple-element.58.through_ref, f32[2,64,128]{2,1,0:T(8,128)} %get-tuple-element.59.past_ref), custom_call_target="tpu_custom_call" | custom-call | flops 12582912 | bytes 196608 | tf_op jit(solution)/shard_map/scan_step/pallas_call | solution.py:216
  114.6 6.6 %all-to-all-done.3 = bf16[16,384,128]{2,1,0:T(8,128)(2,1)} async-done(((bf16[16,384,128]{2,1,0:T(8,128)(2,1)}), bf16[16,384,128]{2,1,0:T(8,128)(2,1)}, u32[]{:S(2)}, u32[]{:S(2)}) %all-to-all-start.3) | async-done | bytes 1572896 | tf_op jit(solution)/shard_map/all_to_all | solution.py:356
  121.2 5.5 %all-to-all-start.4 = ((bf16[16,384,128]{2,1,0:T(8,128)(2,1)}), bf16[16,384,128]{2,1,0:T(8,128)(2,1)S(1)}, u32[]{:S(2)}, u32[]{:S(2)}) async-start(bf16[16,384,128]{2,1,0:T(8,128)(2,1)} %expert_rows.3), calls=%async_computation.4 | async-start | bytes 3145728 | tf_op jit(solution)/shard_map/all_to_all | solution.py:356
  126.7 0.0 copy-done.15
  126.7 10.9 %collective-permute-start.4 = (bf16[2,64,128]{2,1,0:T(8,128)(2,1)S(1)}, bf16[2,64,128]{2,1,0:T(8,128)(2,1)S(1)}, u32[]{:S(2)}, u32[]{:S(2)}) collective-permute-start(bf16[2,64,128]{2,1,0:T(8,128)(2,1)S(1)} %copy-done.15), channel_id=1, source_target_pairs={{0,256},{16,272},{32,288},{48,304},{64,320},{80,336},{96,352},{112... | collective-permute-start | bytes 98312 | tf_op jit(solution)/shard_map/ppermute | solution.py:265
  137.6 1.6 reduce_sum.24
  139.2 0.0 copy-start.14
  139.2 0.0 copy-start
  139.2 0.0 copy-start.1
  139.3 0.0 copy-start.2
  139.3 0.0 copy-start.5
  139.3 0.8 collective-permute-done.4.arrived_ref
  140.1 6.6 %all-to-all-done.4 = bf16[16,384,128]{2,1,0:T(8,128)(2,1)S(1)} async-done(((bf16[16,384,128]{2,1,0:T(8,128)(2,1)}), bf16[16,384,128]{2,1,0:T(8,128)(2,1)S(1)}, u32[]{:S(2)}, u32[]{:S(2)}) %all-to-all-start.4) | async-done | bytes 1572896 | tf_op jit(solution)/shard_map/all_to_all | solution.py:356
  146.7 0.2 reduce_sum.25
  146.9 0.7 pad_maximum_fusion
  147.6 15.2 %all-to-all-start.5 = ((bf16[32,24,128]{2,1,0:T(8,128)(2,1)}), bf16[32,24,128]{2,1,0:T(8,128)(2,1)S(1)}, u32[]{:S(2)}, u32[]{:S(2)}) async-start(bf16[32,24,128]{2,1,0:T(8,128)(2,1)} %bitcast.15), calls=%async_computation.5 | async-start | bytes 393216 | tf_op jit(solution)/shard_map/all_to_all | solution.py:356
  162.8 0.0 copy-done.14
  162.8 0.1 copy.17.gain_ref
  162.9 0.0 copy-done
  162.9 0.0 copy-done.1
  162.9 0.0 copy-done.2
  162.9 1.2 mixer_finish.1
  164.1 17.5 %all-to-all-done.5 = bf16[32,24,128]{2,1,0:T(8,128)(2,1)S(1)} async-done(((bf16[32,24,128]{2,1,0:T(8,128)(2,1)}), bf16[32,24,128]{2,1,0:T(8,128)(2,1)S(1)}, u32[]{:S(2)}, u32[]{:S(2)}) %all-to-all-start.5) | async-done | bytes 196640 | tf_op jit(solution)/shard_map/all_to_all | solution.py:356
  181.6 0.0 copy-done.5
  181.6 0.9 convolution_convert_fusion
  (10 shorter events, 0.0 us)
Async XLA Ops:
  3.2 35.5 %all-to-all-start = ((bf16[32,24,128]{2,1,0:T(8,128)(2,1)}), bf16[32,24,128]{2,1,0:T(8,128)(2,1)S(1)}, u32[]{:S(2)}, u32[]{:S(2)}) async-start(bf16[32,24,128]{2,1,0:T(8,128)(2,1)} %bitcast.27), calls=%async_computation | async-start | bytes 393216 | tf_op jit(solution)/shard_map/all_to_all | solution.py:356
  40.2 6.9 %copy-start.6 = (bf16[2,64,128]{2,1,0:T(8,128)(2,1)S(1)}, bf16[2,64,128]{2,1,0:T(8,128)(2,1)}, u32[]{:S(2)}) copy-start(bf16[2,64,128]{2,1,0:T(8,128)(2,1)} %get-tuple-element.42.through_ref) | copy-start | bytes 98308
  40.2 27.9 %all-to-all-start.1 = ((bf16[16,384,128]{2,1,0:T(8,128)(2,1)}), bf16[16,384,128]{2,1,0:T(8,128)(2,1)}, u32[]{:S(2)}, u32[]{:S(2)}) async-start(bf16[16,384,128]{2,1,0:T(8,128)(2,1)} %broadcast_in_dim.22), calls=%async_computation.1 | async-start | bytes 3145728 | tf_op jit(solution)/shard_map/all_to_all | solution.py:356
  47.2 4.5 %collective-permute-start = (bf16[2,64,128]{2,1,0:T(8,128)(2,1)S(1)}, bf16[2,64,128]{2,1,0:T(8,128)(2,1)S(1)}, u32[]{:S(2)}, u32[]{:S(2)}) collective-permute-start(bf16[2,64,128]{2,1,0:T(8,128)(2,1)S(1)} %copy-done.6), channel_id=1, source_target_pairs={{0,16},{16,0},{32,48},{48,32},{64,80},{80,64},{96,112},{112,96},{1... | collective-permute-start | bytes 98312 | tf_op jit(solution)/shard_map/ppermute | solution.py:265
  51.7 0.6 copy-start.10
  54.2 1.5 copy-start.9
  55.6 5.0 %collective-permute-start.1 = (bf16[2,64,128]{2,1,0:T(8,128)(2,1)S(1)}, bf16[2,64,128]{2,1,0:T(8,128)(2,1)S(1)}, u32[]{:S(2)}, u32[]{:S(2)}) collective-permute-start(bf16[2,64,128]{2,1,0:T(8,128)(2,1)S(1)} %copy-done.9), channel_id=1, source_target_pairs={{0,32},{16,48},{32,0},{48,16},{64,96},{80,112},{96,64},{112,80},{1... | collective-permute-start | bytes 98312 | tf_op jit(solution)/shard_map/ppermute | solution.py:265
  60.7 0.6 copy-start.13
  68.1 6.4 %copy-start.3 = (bf16[1,2048,224]{1,2,0:T(8,128)(2,1)S(1)}, bf16[1,2048,224]{1,2,0:T(8,128)(2,1)}, u32[]{:S(2)}) copy-start(bf16[1,2048,224]{1,2,0:T(8,128)(2,1)} %param.24) | copy-start | bytes 2752516
  68.1 27.0 %all-to-all-start.2 = ((bf16[16,384,128]{2,1,0:T(8,128)(2,1)}), bf16[16,384,128]{2,1,0:T(8,128)(2,1)}, u32[]{:S(2)}, u32[]{:S(2)}) async-start(bf16[16,384,128]{2,1,0:T(8,128)(2,1)} %broadcast_in_dim.23), calls=%async_computation.2 | async-start | bytes 3145728 | tf_op jit(solution)/shard_map/all_to_all | solution.py:356
  74.5 1.4 copy-start.4
  74.5 2.7 %copy-start.7 = (bf16[2,64,128]{2,1,0:T(8,128)(2,1)S(1)}, bf16[2,64,128]{2,1,0:T(8,128)(2,1)}, u32[]{:S(2)}) copy-start(bf16[2,64,128]{2,1,0:T(8,128)(2,1)} %get-tuple-element.52.through_ref) | copy-start | bytes 98308
  77.2 10.6 %collective-permute-start.2 = (bf16[2,64,128]{2,1,0:T(8,128)(2,1)S(1)}, bf16[2,64,128]{2,1,0:T(8,128)(2,1)S(1)}, u32[]{:S(2)}, u32[]{:S(2)}) collective-permute-start(bf16[2,64,128]{2,1,0:T(8,128)(2,1)S(1)} %copy-done.7), channel_id=1, source_target_pairs={{0,64},{16,80},{32,96},{48,112},{64,0},{80,16},{96,32},{112,48},{1... | collective-permute-start | bytes 98312 | tf_op jit(solution)/shard_map/ppermute | solution.py:265
  87.8 0.6 copy-start.12
  95.2 5.9 %copy-start.8 = (bf16[2,64,128]{2,1,0:T(8,128)(2,1)S(1)}, bf16[2,64,128]{2,1,0:T(8,128)(2,1)}, u32[]{:S(2)}) copy-start(bf16[2,64,128]{2,1,0:T(8,128)(2,1)} %get-tuple-element.58.through_ref) | copy-start | bytes 98308
  95.2 26.0 %all-to-all-start.3 = ((bf16[16,384,128]{2,1,0:T(8,128)(2,1)}), bf16[16,384,128]{2,1,0:T(8,128)(2,1)}, u32[]{:S(2)}, u32[]{:S(2)}) async-start(bf16[16,384,128]{2,1,0:T(8,128)(2,1)} %expert_rows.2), calls=%async_computation.3 | async-start | bytes 3145728 | tf_op jit(solution)/shard_map/all_to_all | solution.py:356
  101.1 11.1 %collective-permute-start.3 = (bf16[2,64,128]{2,1,0:T(8,128)(2,1)S(1)}, bf16[2,64,128]{2,1,0:T(8,128)(2,1)S(1)}, u32[]{:S(2)}, u32[]{:S(2)}) collective-permute-start(bf16[2,64,128]{2,1,0:T(8,128)(2,1)S(1)} %copy-done.8), channel_id=1, source_target_pairs={{0,128},{16,144},{32,160},{48,176},{64,192},{80,208},{96,224},{112... | collective-permute-start | bytes 98312 | tf_op jit(solution)/shard_map/ppermute | solution.py:265
  112.1 0.6 copy-start.11
  121.2 5.5 %copy-start.15 = (bf16[2,64,128]{2,1,0:T(8,128)(2,1)S(1)}, bf16[2,64,128]{2,1,0:T(8,128)(2,1)}, u32[]{:S(2)}) copy-start(bf16[2,64,128]{2,1,0:T(8,128)(2,1)} %get-tuple-element.64) | copy-start | bytes 98308
  121.2 25.5 %all-to-all-start.4 = ((bf16[16,384,128]{2,1,0:T(8,128)(2,1)}), bf16[16,384,128]{2,1,0:T(8,128)(2,1)S(1)}, u32[]{:S(2)}, u32[]{:S(2)}) async-start(bf16[16,384,128]{2,1,0:T(8,128)(2,1)} %expert_rows.3), calls=%async_computation.4 | async-start | bytes 3145728 | tf_op jit(solution)/shard_map/all_to_all | solution.py:356
  126.7 13.4 %collective-permute-start.4 = (bf16[2,64,128]{2,1,0:T(8,128)(2,1)S(1)}, bf16[2,64,128]{2,1,0:T(8,128)(2,1)S(1)}, u32[]{:S(2)}, u32[]{:S(2)}) collective-permute-start(bf16[2,64,128]{2,1,0:T(8,128)(2,1)S(1)} %copy-done.15), channel_id=1, source_target_pairs={{0,256},{16,272},{32,288},{48,304},{64,320},{80,336},{96,352},{112... | collective-permute-start | bytes 98312 | tf_op jit(solution)/shard_map/ppermute | solution.py:265
  139.2 23.5 %copy-start.14 = (f32[64]{0:T(128)S(1)}, f32[64]{0:T(128)}, u32[]{:S(2)}) copy-start(f32[64]{0:T(128)} %param.18) | copy-start | bytes 772
  139.2 23.6 %copy-start = (f32[64,1024]{1,0:T(8,128)S(1)}, f32[64,1024]{1,0:T(8,128)}, u32[]{:S(2)}) copy-start(f32[64,1024]{1,0:T(8,128)} %get-tuple-element.67.oloc_ref) | copy-start | bytes 786436
  139.2 23.6 %copy-start.1 = (bf16[128,1024]{1,0:T(8,128)(2,1)S(1)}, bf16[128,1024]{1,0:T(8,128)(2,1)}, u32[]{:S(2)}) copy-start(bf16[128,1024]{1,0:T(8,128)(2,1)} %get-tuple-element.68.qp_ref) | copy-start | bytes 786436
  139.3 23.6 %copy-start.2 = (f32[2,64,128]{2,1,0:T(8,128)S(1)}, f32[2,64,128]{2,1,0:T(8,128)}, u32[]{:S(2)}) copy-start(f32[2,64,128]{2,1,0:T(8,128)} %get-tuple-element.66.past_ref) | copy-start | bytes 196612
  139.3 42.3 %copy-start.5 = (bf16[768,256]{1,0:T(8,128)(2,1)S(1)}, bf16[768,256]{1,0:T(8,128)(2,1)}, u32[]{:S(2)}) copy-start(bf16[768,256]{1,0:T(8,128)(2,1)} %get-tuple-element.69) | copy-start | bytes 1179652
  147.6 33.9 %all-to-all-start.5 = ((bf16[32,24,128]{2,1,0:T(8,128)(2,1)}), bf16[32,24,128]{2,1,0:T(8,128)(2,1)S(1)}, u32[]{:S(2)}, u32[]{:S(2)}) async-start(bf16[32,24,128]{2,1,0:T(8,128)(2,1)} %bitcast.15), calls=%async_computation.5 | async-start | bytes 393216 | tf_op jit(solution)/shard_map/all_to_all | solution.py:356

commit v6 on v5

--- a/solution.py
+++ b/solution.py
@@ -272,8 +272,8 @@
 def expert_kernel(rows_ref, gate_ref, up_ref, down_ref, out_ref):
     parts = rows_ref.shape[0]
     rows = jnp.concatenate([rows_ref[j] for j in range(parts)], axis=1)
-    gate = mm(rows, gate_ref[...])
-    up = mm(rows, up_ref[...])
+    gate = mm_nt(rows, gate_ref[...])
+    up = mm_nt(rows, up_ref[...])
     hidden = (gate / (1.0 + jnp.exp(-gate)) * up).astype(jnp.bfloat16)
     result = mm(hidden, down_ref[...]).astype(jnp.bfloat16)
     for j in range(parts):
@@ -294,7 +294,7 @@
         cost_estimate=pl.CostEstimate(
             flops=6 * total * gate.size,
             bytes_accessed=2 * (2 * rows.size + 3 * gate.size),
-            transcendentals=total * gate.shape[1],
+            transcendentals=total * gate.shape[0],
         ),
         compiler_params=pltpu.CompilerParams(vmem_limit_bytes=66000000),
         name="expert_rows",
@@ -396,31 +396,26 @@
         jnp.broadcast_to(part[None], (shares, *part.shape))
         for part in (arrived[:middle], arrived[middle:])
     ]
-    copies[0], own_maps = lax.optimization_barrier((copies[0], own_maps))
+    copies, own_maps = lax.optimization_barrier((copies, own_maps))
     shared_a = spread(copies[0], "tp")
+    weights = [gate_weight[0].T, up_weight[0].T, down_weight[0]]
+    shared_a, copies, own_maps = lax.optimization_barrier((shared_a, copies, own_maps))
     past, through = jnp.zeros(own_maps.shape, jnp.float32), own_maps
-    weights = [gate_weight[0], up_weight[0], down_weight[0]]
 
     def scanned(steps, past, through):
         for step in steps:
             past, through = scan_step(side(step), swapped(through, step), through, past)
         return past, through
 
-    past, through = scanned((1,), past, through)
-    copies[1], past, through = lax.optimization_barrier((copies[1], past, through))
-    past, through = scanned((2,), past, through)
-    shared_a, copies[1], past, through = lax.optimization_barrier(
-        (shared_a, copies[1], past, through)
-    )
     shared_b = spread(copies[1], "tp")
     partial_a = expert_rows(shared_a, *weights)
-    past, through = scanned((4,), past, through)
+    past, through = scanned((1, 2), past, through)
     shared_b, partial_a, past, through = lax.optimization_barrier(
         (shared_b, partial_a, past, through)
     )
     pieces_a = spread(partial_a, "tp")
     partial_b = expert_rows(shared_b, *weights)
-    past, through = scanned((8,), past, through)
+    past, through = scanned((4, 8), past, through)
     pieces_a, partial_b, past, through = lax.optimization_barrier(
         (pieces_a, partial_b, past, through)
     )

time: 184 us -> 184 us (level)
  blocking collectives: 0 us -> 28 us
  waiting for transfers between devices: 48.8 us -> 34.3 us
  starting transfers between devices: 83.6 us -> 72.8 us
  local copies, waits for them, and re-layouts: 8.22 us -> 4.4 us
    all_to_all x0 -> x1, blocking collectives: none -> 28 us  [spread(): return lax.all_to_all(array, axis, 0, 0, tiled=True)]
    all_to_all x6 -> x5, waiting for transfers between devices: 44 us -> 29.1 us  [spread(): return lax.all_to_all(array, axis, 0, 0, tiled=True)]
    all_to_all x6 -> x5, starting transfers between devices: 56.6 us -> 48 us  [spread(): return lax.all_to_all(array, axis, 0, 0, tiled=True)]
    unnamed x34 -> x24, local copies, waits for them, and re-layouts: 4.55 us -> 1.87 us
    ppermute x5, starting transfers between devices: 27.1 us -> 24.8 us  [swapped(): lax.ppermute(through, 'ep', [(i, i ^ distance) for i in range(count)])]
  transfers between devices with their start and end apart: 11 -> 10, of which waited for: 9 -> 7; matrix products, arithmetic and copies ran while one was open for 4% -> 1% of each run, Pallas kernels for 19% -> 20%
where the time goes in v6:
time: 184 us; the launch traced here: 182 us
  starting transfers between devices  72.8 us (40%)
  Pallas kernels  38.6 us (21%)
  waiting for transfers between devices  34.3 us (19%)
  blocking collectives  28 us (15%)
  local copies, waits for them, and re-layouts  4.4 us (2%)
  other arithmetic  2.56 us (1%)
    all_to_all x5, starting transfers between devices, spread(): return lax.all_to_all(array, axis, 0, 0, tiled=True)  48 us
    all_to_all x5, waiting for transfers between devices, spread(): return lax.all_to_all(array, axis, 0, 0, tiled=True)  29.1 us
    all_to_all x1, blocking collectives, spread(): return lax.all_to_all(array, axis, 0, 0, tiled=True)  28 us
    ppermute x5, starting transfers between devices, swapped(): lax.ppermute(through, 'ep', [(i, i ^ distance) for i in range(count)])  24.8 us
    pallas_call x1, Pallas kernels, local_half(): pl.pallas_call(local_kernel, out_shape=(full(jnp.float32), jax.ShapeDtype...  15.4 us
    pallas_call x2, Pallas kernels, expert_rows(): pl.pallas_call(expert_kernel, grid=(total // tile,), in_specs=[block, fix...  12.1 us
    pallas_call x4, Pallas kernels, scan_step(): pl.pallas_call(step_kernel, out_shape=(jax.ShapeDtypeStruct(past.shape, j...  7.35 us
    ppermute x5, waiting for transfers between devices, swapped(): lax.ppermute(through, 'ep', [(i, i ^ distance) for i in range(count)])  5.2 us
  transfers between devices with their start and end apart: 10, of which 7 were waited for; matrix products, arithmetic and copies ran while one was open for 1% of the time, Pallas kernels for 20%

profile of v6, /device:TPU:1, one launch (start us, length us, event | category | flops | bytes accessed | tf_op | source)
XLA Modules:
  0.0 182.4 jit_solution(5540432655190569728)
XLA Ops:
  0.6 2.6 %route_rows.1 = (bf16[768,128]{1,0:T(8,128)(2,1)}, bf16[768,256]{1,0:T(8,128)(2,1)}) custom-call(s32[1]{0:T(128)} %bitcast.1.at_ref, bf16[256,2048]{1,0:T(8,128)(2,1)} %rows_ref.1, f32[1,2048]{1,0:T(1,128)} %bitcast.32, s32[2,256]{1,0:T(2,128)} %bitcast.33, f32[2,256]{1,0:T(2,128)} %bitcast.34), custom_call_target="tpu_custom_call" | custom-call | flops 100663296 | bytes 1048576 | tf_op jit(solution)/shard_map/route_rows/pallas_call | solution.py:336
  3.2 16.7 %all-to-all-start = ((bf16[32,24,128]{2,1,0:T(8,128)(2,1)}), bf16[32,24,128]{2,1,0:T(8,128)(2,1)S(1)}, u32[]{:S(2)}, u32[]{:S(2)}) async-start(bf16[32,24,128]{2,1,0:T(8,128)(2,1)} %bitcast.31), calls=%async_computation | async-start | bytes 393216 | tf_op jit(solution)/shard_map/all_to_all | solution.py:356
  20.0 15.4 %mixer_local.1 = (f32[64,1024]{1,0:T(8,128)}, bf16[128,1024]{1,0:T(8,128)(2,1)}, bf16[2,64,128]{2,1,0:T(8,128)(2,1)}) custom-call(bf16[64,1024]{1,0:T(8,128)(2,1)} %q_ref.1, bf16[64,1024]{1,0:T(8,128)(2,1)} %k_ref.1, bf16[64,1024]{1,0:T(8,128)(2,1)} %v_ref.1, bf16[64,1024]{1,0:T(8,128)(2,1)} %e_ref.1, bf16[64,1024]{1,0:T(8,128)(2,1)} %d_ref.1), custom_call_target="tpu_custom_call" | custom-call | flops 1476395008 | bytes 1179648 | tf_op jit(solution)/shard_map/mixer_local/pallas_call | solution.py:155
  35.3 3.4 %all-to-all-done = bf16[32,24,128]{2,1,0:T(8,128)(2,1)S(1)} async-done(((bf16[32,24,128]{2,1,0:T(8,128)(2,1)}), bf16[32,24,128]{2,1,0:T(8,128)(2,1)S(1)}, u32[]{:S(2)}, u32[]{:S(2)}) %all-to-all-start) | async-done | bytes 196640 | tf_op jit(solution)/shard_map/all_to_all | solution.py:356
  38.8 0.3 broadcast_in_dim.22
  39.1 1.5 broadcast_in_dim.23
  40.6 28.0 %all_to_all.30.rows_ref = bf16[16,384,128]{2,1,0:T(8,128)(2,1)} all-to-all(bf16[16,384,128]{2,1,0:T(8,128)(2,1)S(1)} %broadcast_in_dim.22), channel_id=1, replica_groups=mesh['ep'=32,'tp'=16] {'tp'}, dimensions={0} | all-to-all | bytes 3145728 | tf_op jit(solution)/shard_map/all_to_all | solution.py:356
  68.6 0.0 copy-start.4
  68.6 4.5 %all-to-all-start.2 = ((bf16[16,384,128]{2,1,0:T(8,128)(2,1)}), bf16[16,384,128]{2,1,0:T(8,128)(2,1)}, u32[]{:S(2)}, u32[]{:S(2)}) async-start(bf16[16,384,128]{2,1,0:T(8,128)(2,1)} %broadcast_in_dim.23), calls=%async_computation.2 | async-start | bytes 3145728 | tf_op jit(solution)/shard_map/all_to_all | solution.py:356
  73.2 0.0 copy-done.4
  73.2 4.4 %collective-permute-start = (bf16[2,64,128]{2,1,0:T(8,128)(2,1)S(1)}, bf16[2,64,128]{2,1,0:T(8,128)(2,1)S(1)}, u32[]{:S(2)}, u32[]{:S(2)}) collective-permute-start(bf16[2,64,128]{2,1,0:T(8,128)(2,1)S(1)} %copy-done.4), channel_id=1, source_target_pairs={{0,16},{16,0},{32,48},{48,32},{64,80},{80,64},{96,112},{112,96},{1... | collective-permute-start | bytes 98312 | tf_op jit(solution)/shard_map/ppermute | solution.py:265
  77.5 0.8 collective-permute-done.arrived_ref
  78.4 0.0 copy-start.6
  78.4 0.6 broadcast_in_dim.24.past_ref
  79.0 0.0 copy-done.6
  79.0 1.8 %scan_step.4 = (f32[2,64,128]{2,1,0:T(8,128)}, bf16[2,64,128]{2,1,0:T(8,128)(2,1)}) custom-call(s32[1]{0:T(128)} %bitcast.13.upper_ref, bf16[2,64,128]{2,1,0:T(8,128)(2,1)} %copy-done.6, bf16[2,64,128]{2,1,0:T(8,128)(2,1)} %get-tuple-element.43.through_ref, f32[2,64,128]{2,1,0:T(8,128)} %broadcast_in_dim.24.past_ref), custom_call_target="tpu_custom_call" | custom-call | flops 12582912 | bytes 196608 | tf_op jit(solution)/shard_map/scan_step/pallas_call | solution.py:216
  80.8 1.9 %collective-permute-start.1 = (bf16[2,64,128]{2,1,0:T(8,128)(2,1)}, bf16[2,64,128]{2,1,0:T(8,128)(2,1)S(1)}, u32[]{:S(2)}, u32[]{:S(2)}) collective-permute-start(bf16[2,64,128]{2,1,0:T(8,128)(2,1)} %get-tuple-element.44.through_ref), channel_id=1, source_target_pairs={{0,32},{16,48},{32,0},{48,16},{64,96},{80,112},{96,64},{112,80},{1... | collective-permute-start | bytes 98312 | tf_op jit(solution)/shard_map/ppermute | solution.py:265
  82.8 6.1 %expert_rows.2 = bf16[16,384,128]{2,1,0:T(8,128)(2,1)} custom-call(bf16[16,384,128]{2,1,0:T(8,128)(2,1)} %all_to_all.30.rows_ref, bf16[224,2048]{1,0:T(8,128)(2,1)} %bitcast.23, bf16[224,2048]{1,0:T(8,128)(2,1)} %bitcast.25, bf16[224,2048]{1,0:T(8,128)(2,1)} %bitcast.27), custom_call_target="tpu_custom_call" | custom-call | flops 1056964608 | bytes 5898240 | tf_op jit(solution)/shard_map/expert_rows/pallas_call | solution.py:288
  88.8 0.0 collective-permute-done.1.arrived_ref
  88.8 0.0 copy-start.7
  88.8 0.6 copy-done.7
  89.4 1.8 %scan_step.5 = (f32[2,64,128]{2,1,0:T(8,128)}, bf16[2,64,128]{2,1,0:T(8,128)(2,1)}) custom-call(s32[1]{0:T(128)} %bitcast.12.upper_ref, bf16[2,64,128]{2,1,0:T(8,128)(2,1)} %copy-done.7, bf16[2,64,128]{2,1,0:T(8,128)(2,1)} %get-tuple-element.44.through_ref, f32[2,64,128]{2,1,0:T(8,128)} %get-tuple-element.45.past_ref), custom_call_target="tpu_custom_call" | custom-call | flops 12582912 | bytes 196608 | tf_op jit(solution)/shard_map/scan_step/pallas_call | solution.py:216
  91.3 2.1 %all-to-all-done.2.rows_ref = bf16[16,384,128]{2,1,0:T(8,128)(2,1)} async-done(((bf16[16,384,128]{2,1,0:T(8,128)(2,1)}), bf16[16,384,128]{2,1,0:T(8,128)(2,1)}, u32[]{:S(2)}, u32[]{:S(2)}) %all-to-all-start.2) | async-done | bytes 1572896 | tf_op jit(solution)/shard_map/all_to_all | solution.py:356
  93.3 0.0 copy-start.5
  93.3 5.5 %all-to-all-start.3 = ((bf16[16,384,128]{2,1,0:T(8,128)(2,1)}), bf16[16,384,128]{2,1,0:T(8,128)(2,1)}, u32[]{:S(2)}, u32[]{:S(2)}) async-start(bf16[16,384,128]{2,1,0:T(8,128)(2,1)} %expert_rows.2), calls=%async_computation.3 | async-start | bytes 3145728 | tf_op jit(solution)/shard_map/all_to_all | solution.py:356
  98.9 0.0 copy-done.5
  98.9 5.4 %collective-permute-start.2 = (bf16[2,64,128]{2,1,0:T(8,128)(2,1)S(1)}, bf16[2,64,128]{2,1,0:T(8,128)(2,1)S(1)}, u32[]{:S(2)}, u32[]{:S(2)}) collective-permute-start(bf16[2,64,128]{2,1,0:T(8,128)(2,1)S(1)} %copy-done.5), channel_id=1, source_target_pairs={{0,64},{16,80},{32,96},{48,112},{64,0},{80,16},{96,32},{112,48},{1... | collective-permute-start | bytes 98312 | tf_op jit(solution)/shard_map/ppermute | solution.py:265
  104.3 1.3 collective-permute-done.2.arrived_ref
  105.6 0.0 copy-start.8
  105.6 0.6 copy-done.8
  106.2 1.8 %scan_step.6 = (f32[2,64,128]{2,1,0:T(8,128)}, bf16[2,64,128]{2,1,0:T(8,128)(2,1)}) custom-call(s32[1]{0:T(128)} %bitcast.17.upper_ref, bf16[2,64,128]{2,1,0:T(8,128)(2,1)} %copy-done.8, bf16[2,64,128]{2,1,0:T(8,128)(2,1)} %get-tuple-element.50.through_ref, f32[2,64,128]{2,1,0:T(8,128)} %get-tuple-element.51.past_ref), custom_call_target="tpu_custom_call" | custom-call | flops 12582912 | bytes 196608 | tf_op jit(solution)/shard_map/scan_step/pallas_call | solution.py:216
  108.1 4.5 %collective-permute-start.3 = (bf16[2,64,128]{2,1,0:T(8,128)(2,1)}, bf16[2,64,128]{2,1,0:T(8,128)(2,1)S(1)}, u32[]{:S(2)}, u32[]{:S(2)}) collective-permute-start(bf16[2,64,128]{2,1,0:T(8,128)(2,1)} %get-tuple-element.52.through_ref), channel_id=1, source_target_pairs={{0,128},{16,144},{32,160},{48,176},{64,192},{80,208},{96,224},{112... | collective-permute-start | bytes 98312 | tf_op jit(solution)/shard_map/ppermute | solution.py:265
  112.6 6.0 %expert_rows.3 = bf16[16,384,128]{2,1,0:T(8,128)(2,1)} custom-call(bf16[16,384,128]{2,1,0:T(8,128)(2,1)} %all-to-all-done.2.rows_ref, bf16[224,2048]{1,0:T(8,128)(2,1)} %bitcast.24, bf16[224,2048]{1,0:T(8,128)(2,1)} %bitcast.26, bf16[224,2048]{1,0:T(8,128)(2,1)} %bitcast.28), custom_call_target="tpu_custom_call" | custom-call | flops 1056964608 | bytes 5898240 | tf_op jit(solution)/shard_map/expert_rows/pallas_call | solution.py:288
  118.6 0.0 collective-permute-done.3.arrived_ref
  118.6 0.0 copy-start.9
  118.6 0.6 copy-done.9
  119.2 1.8 %scan_step.7 = (f32[2,64,128]{2,1,0:T(8,128)}, bf16[2,64,128]{2,1,0:T(8,128)(2,1)}) custom-call(s32[1]{0:T(128)} %bitcast.16.upper_ref, bf16[2,64,128]{2,1,0:T(8,128)(2,1)} %copy-done.9, bf16[2,64,128]{2,1,0:T(8,128)(2,1)} %get-tuple-element.52.through_ref, f32[2,64,128]{2,1,0:T(8,128)} %get-tuple-element.53.past_ref), custom_call_target="tpu_custom_call" | custom-call | flops 12582912 | bytes 196608 | tf_op jit(solution)/shard_map/scan_step/pallas_call | solution.py:216
  121.0 0.0 all-to-all-done.3
  121.0 0.0 copy-start.11
  121.0 7.1 %all-to-all-start.4 = ((bf16[16,384,128]{2,1,0:T(8,128)(2,1)}), bf16[16,384,128]{2,1,0:T(8,128)(2,1)S(1)}, u32[]{:S(2)}, u32[]{:S(2)}) async-start(bf16[16,384,128]{2,1,0:T(8,128)(2,1)} %expert_rows.3), calls=%async_computation.4 | async-start | bytes 3145728 | tf_op jit(solution)/shard_map/all_to_all | solution.py:356
  128.2 0.0 copy-done.11
  128.2 8.6 %collective-permute-start.4 = (bf16[2,64,128]{2,1,0:T(8,128)(2,1)S(1)}, bf16[2,64,128]{2,1,0:T(8,128)(2,1)S(1)}, u32[]{:S(2)}, u32[]{:S(2)}) collective-permute-start(bf16[2,64,128]{2,1,0:T(8,128)(2,1)S(1)} %copy-done.11), channel_id=1, source_target_pairs={{0,256},{16,272},{32,288},{48,304},{64,320},{80,336},{96,352},{112... | collective-permute-start | bytes 98312 | tf_op jit(solution)/shard_map/ppermute | solution.py:265
  136.8 1.6 reduce_sum.24
  138.5 0.0 copy-start.10
  138.5 0.0 copy-start
  138.5 0.0 copy-start.1
  138.5 0.0 copy-start.2
  138.5 0.0 copy-start.3
  138.5 3.1 %collective-permute-done.4.arrived_ref = bf16[2,64,128]{2,1,0:T(8,128)(2,1)S(1)} collective-permute-done((bf16[2,64,128]{2,1,0:T(8,128)(2,1)S(1)}, bf16[2,64,128]{2,1,0:T(8,128)(2,1)S(1)}, u32[]{:S(2)}, u32[]{:S(2)}) %collective-permute-start.4) | collective-permute-done | bytes 32800 | tf_op jit(solution)/shard_map/ppermute | solution.py:265
  141.6 6.2 %all-to-all-done.4 = bf16[16,384,128]{2,1,0:T(8,128)(2,1)S(1)} async-done(((bf16[16,384,128]{2,1,0:T(8,128)(2,1)}), bf16[16,384,128]{2,1,0:T(8,128)(2,1)S(1)}, u32[]{:S(2)}, u32[]{:S(2)}) %all-to-all-start.4) | async-done | bytes 1572896 | tf_op jit(solution)/shard_map/all_to_all | solution.py:356
  147.8 0.2 reduce_sum.25
  148.0 0.7 pad_maximum_fusion
  148.7 14.0 %all-to-all-start.5 = ((bf16[32,24,128]{2,1,0:T(8,128)(2,1)}), bf16[32,24,128]{2,1,0:T(8,128)(2,1)S(1)}, u32[]{:S(2)}, u32[]{:S(2)}) async-start(bf16[32,24,128]{2,1,0:T(8,128)(2,1)} %bitcast.19), calls=%async_computation.5 | async-start | bytes 393216 | tf_op jit(solution)/shard_map/all_to_all | solution.py:356
  162.7 0.0 copy-done.10
  162.7 0.1 copy.15.gain_ref
  162.8 0.0 copy-done
  162.8 0.0 copy-done.1
  162.8 0.0 copy-done.2
  162.8 1.2 mixer_finish.1
  164.0 17.5 %all-to-all-done.5 = bf16[32,24,128]{2,1,0:T(8,128)(2,1)S(1)} async-done(((bf16[32,24,128]{2,1,0:T(8,128)(2,1)}), bf16[32,24,128]{2,1,0:T(8,128)(2,1)S(1)}, u32[]{:S(2)}, u32[]{:S(2)}) %all-to-all-start.5) | async-done | bytes 196640 | tf_op jit(solution)/shard_map/all_to_all | solution.py:356
  181.5 0.0 copy-done.3
  181.5 0.9 convolution_convert_fusion
  (1 shorter events, 0.0 us)
Async XLA Ops:
  3.2 35.5 %all-to-all-start = ((bf16[32,24,128]{2,1,0:T(8,128)(2,1)}), bf16[32,24,128]{2,1,0:T(8,128)(2,1)S(1)}, u32[]{:S(2)}, u32[]{:S(2)}) async-start(bf16[32,24,128]{2,1,0:T(8,128)(2,1)} %bitcast.31), calls=%async_computation | async-start | bytes 393216 | tf_op jit(solution)/shard_map/all_to_all | solution.py:356
  68.6 4.6 %copy-start.4 = (bf16[2,64,128]{2,1,0:T(8,128)(2,1)S(1)}, bf16[2,64,128]{2,1,0:T(8,128)(2,1)}, u32[]{:S(2)}) copy-start(bf16[2,64,128]{2,1,0:T(8,128)(2,1)} %get-tuple-element.43.through_ref) | copy-start | bytes 98308
  68.6 24.7 %all-to-all-start.2 = ((bf16[16,384,128]{2,1,0:T(8,128)(2,1)}), bf16[16,384,128]{2,1,0:T(8,128)(2,1)}, u32[]{:S(2)}, u32[]{:S(2)}) async-start(bf16[16,384,128]{2,1,0:T(8,128)(2,1)} %broadcast_in_dim.23), calls=%async_computation.2 | async-start | bytes 3145728 | tf_op jit(solution)/shard_map/all_to_all | solution.py:356
  73.2 5.2 %collective-permute-start = (bf16[2,64,128]{2,1,0:T(8,128)(2,1)S(1)}, bf16[2,64,128]{2,1,0:T(8,128)(2,1)S(1)}, u32[]{:S(2)}, u32[]{:S(2)}) collective-permute-start(bf16[2,64,128]{2,1,0:T(8,128)(2,1)S(1)} %copy-done.4), channel_id=1, source_target_pairs={{0,16},{16,0},{32,48},{48,32},{64,80},{80,64},{96,112},{112,96},{1... | collective-permute-start | bytes 98312 | tf_op jit(solution)/shard_map/ppermute | solution.py:265
  78.4 0.6 copy-start.6
  80.8 8.0 %collective-permute-start.1 = (bf16[2,64,128]{2,1,0:T(8,128)(2,1)}, bf16[2,64,128]{2,1,0:T(8,128)(2,1)S(1)}, u32[]{:S(2)}, u32[]{:S(2)}) collective-permute-start(bf16[2,64,128]{2,1,0:T(8,128)(2,1)} %get-tuple-element.44.through_ref), channel_id=1, source_target_pairs={{0,32},{16,48},{32,0},{48,16},{64,96},{80,112},{96,64},{112,80},{1... | collective-permute-start | bytes 98312 | tf_op jit(solution)/shard_map/ppermute | solution.py:265
  88.8 0.6 copy-start.7
  93.3 5.5 %copy-start.5 = (bf16[2,64,128]{2,1,0:T(8,128)(2,1)S(1)}, bf16[2,64,128]{2,1,0:T(8,128)(2,1)}, u32[]{:S(2)}) copy-start(bf16[2,64,128]{2,1,0:T(8,128)(2,1)} %get-tuple-element.50.through_ref) | copy-start | bytes 98308
  93.3 27.7 %all-to-all-start.3 = ((bf16[16,384,128]{2,1,0:T(8,128)(2,1)}), bf16[16,384,128]{2,1,0:T(8,128)(2,1)}, u32[]{:S(2)}, u32[]{:S(2)}) async-start(bf16[16,384,128]{2,1,0:T(8,128)(2,1)} %expert_rows.2), calls=%async_computation.3 | async-start | bytes 3145728 | tf_op jit(solution)/shard_map/all_to_all | solution.py:356
  98.9 6.7 %collective-permute-start.2 = (bf16[2,64,128]{2,1,0:T(8,128)(2,1)S(1)}, bf16[2,64,128]{2,1,0:T(8,128)(2,1)S(1)}, u32[]{:S(2)}, u32[]{:S(2)}) collective-permute-start(bf16[2,64,128]{2,1,0:T(8,128)(2,1)S(1)} %copy-done.5), channel_id=1, source_target_pairs={{0,64},{16,80},{32,96},{48,112},{64,0},{80,16},{96,32},{112,48},{1... | collective-permute-start | bytes 98312 | tf_op jit(solution)/shard_map/ppermute | solution.py:265
  105.6 0.6 copy-start.8
  108.1 10.5 %collective-permute-start.3 = (bf16[2,64,128]{2,1,0:T(8,128)(2,1)}, bf16[2,64,128]{2,1,0:T(8,128)(2,1)S(1)}, u32[]{:S(2)}, u32[]{:S(2)}) collective-permute-start(bf16[2,64,128]{2,1,0:T(8,128)(2,1)} %get-tuple-element.52.through_ref), channel_id=1, source_target_pairs={{0,128},{16,144},{32,160},{48,176},{64,192},{80,208},{96,224},{112... | collective-permute-start | bytes 98312 | tf_op jit(solution)/shard_map/ppermute | solution.py:265
  118.6 0.6 copy-start.9
  121.0 7.1 %copy-start.11 = (bf16[2,64,128]{2,1,0:T(8,128)(2,1)S(1)}, bf16[2,64,128]{2,1,0:T(8,128)(2,1)}, u32[]{:S(2)}) copy-start(bf16[2,64,128]{2,1,0:T(8,128)(2,1)} %get-tuple-element.58) | copy-start | bytes 98308
  121.0 26.7 %all-to-all-start.4 = ((bf16[16,384,128]{2,1,0:T(8,128)(2,1)}), bf16[16,384,128]{2,1,0:T(8,128)(2,1)S(1)}, u32[]{:S(2)}, u32[]{:S(2)}) async-start(bf16[16,384,128]{2,1,0:T(8,128)(2,1)} %expert_rows.3), calls=%async_computation.4 | async-start | bytes 3145728 | tf_op jit(solution)/shard_map/all_to_all | solution.py:356
  128.2 13.4 %collective-permute-start.4 = (bf16[2,64,128]{2,1,0:T(8,128)(2,1)S(1)}, bf16[2,64,128]{2,1,0:T(8,128)(2,1)S(1)}, u32[]{:S(2)}, u32[]{:S(2)}) collective-permute-start(bf16[2,64,128]{2,1,0:T(8,128)(2,1)S(1)} %copy-done.11), channel_id=1, source_target_pairs={{0,256},{16,272},{32,288},{48,304},{64,320},{80,336},{96,352},{112... | collective-permute-start | bytes 98312 | tf_op jit(solution)/shard_map/ppermute | solution.py:265
  138.5 24.2 %copy-start.10 = (f32[64]{0:T(128)S(1)}, f32[64]{0:T(128)}, u32[]{:S(2)}) copy-start(f32[64]{0:T(128)} %param.18) | copy-start | bytes 772
  138.5 24.3 %copy-start = (f32[64,1024]{1,0:T(8,128)S(1)}, f32[64,1024]{1,0:T(8,128)}, u32[]{:S(2)}) copy-start(f32[64,1024]{1,0:T(8,128)} %get-tuple-element.61.oloc_ref) | copy-start | bytes 786436
  138.5 24.3 %copy-start.1 = (bf16[128,1024]{1,0:T(8,128)(2,1)S(1)}, bf16[128,1024]{1,0:T(8,128)(2,1)}, u32[]{:S(2)}) copy-start(bf16[128,1024]{1,0:T(8,128)(2,1)} %get-tuple-element.62.qp_ref) | copy-start | bytes 786436
  138.5 24.3 %copy-start.2 = (f32[2,64,128]{2,1,0:T(8,128)S(1)}, f32[2,64,128]{2,1,0:T(8,128)}, u32[]{:S(2)}) copy-start(f32[2,64,128]{2,1,0:T(8,128)} %get-tuple-element.60.past_ref) | copy-start | bytes 196612
  138.5 43.0 %copy-start.3 = (bf16[768,256]{1,0:T(8,128)(2,1)S(1)}, bf16[768,256]{1,0:T(8,128)(2,1)}, u32[]{:S(2)}) copy-start(bf16[768,256]{1,0:T(8,128)(2,1)} %get-tuple-element.63) | copy-start | bytes 1179652
  148.7 32.8 %all-to-all-start.5 = ((bf16[32,24,128]{2,1,0:T(8,128)(2,1)}), bf16[32,24,128]{2,1,0:T(8,128)(2,1)S(1)}, u32[]{:S(2)}, u32[]{:S(2)}) async-start(bf16[32,24,128]{2,1,0:T(8,128)(2,1)} %bitcast.19), calls=%async_computation.5 | async-start | bytes 393216 | tf_op jit(solution)/shard_map/all_to_all | solution.py:356

commit v7 on v5

--- a/solution.py
+++ b/solution.py
@@ -212,7 +212,7 @@
     ] * count
 
 
-def scan_step(upper, arrived, through, past):
+def scan_step(upper, arrived, through, past, grant):
     return pl.pallas_call(
         step_kernel,
         out_shape=(
@@ -224,7 +224,7 @@
         cost_estimate=pl.CostEstimate(
             flops=6 * 128**3, bytes_accessed=6 * 2 * past.size, transcendentals=0
         ),
-        compiler_params=pltpu.CompilerParams(vmem_limit_bytes=66000000),
+        compiler_params=pltpu.CompilerParams(vmem_limit_bytes=grant),
         name="scan_step",
     )(upper, arrived, through, past)
 
@@ -272,8 +272,8 @@
 def expert_kernel(rows_ref, gate_ref, up_ref, down_ref, out_ref):
     parts = rows_ref.shape[0]
     rows = jnp.concatenate([rows_ref[j] for j in range(parts)], axis=1)
-    gate = mm(rows, gate_ref[...])
-    up = mm(rows, up_ref[...])
+    gate = mm_nt(rows, gate_ref[...])
+    up = mm_nt(rows, up_ref[...])
     hidden = (gate / (1.0 + jnp.exp(-gate)) * up).astype(jnp.bfloat16)
     result = mm(hidden, down_ref[...]).astype(jnp.bfloat16)
     for j in range(parts):
@@ -282,7 +282,7 @@
 
 def expert_rows(rows, gate, up, down):
     parts, total, lanes = rows.shape
-    tile = 128 if total % 128 == 0 else total
+    tile = 192 if total % 192 == 0 else total
     block = pl.BlockSpec((parts, tile, lanes), lambda i: (0, i, 0))
     fixed = lambda array: pl.BlockSpec(array.shape, lambda i: (0, 0))
     return pl.pallas_call(
@@ -294,7 +294,7 @@
         cost_estimate=pl.CostEstimate(
             flops=6 * total * gate.size,
             bytes_accessed=2 * (2 * rows.size + 3 * gate.size),
-            transcendentals=total * gate.shape[1],
+            transcendentals=total * gate.shape[0],
         ),
         compiler_params=pltpu.CompilerParams(vmem_limit_bytes=66000000),
         name="expert_rows",
@@ -399,11 +399,12 @@
     copies[0], own_maps = lax.optimization_barrier((copies[0], own_maps))
     shared_a = spread(copies[0], "tp")
     past, through = jnp.zeros(own_maps.shape, jnp.float32), own_maps
-    weights = [gate_weight[0], up_weight[0], down_weight[0]]
+    weights = [gate_weight[0].T, up_weight[0].T, down_weight[0]]
 
     def scanned(steps, past, through):
         for step in steps:
-            past, through = scan_step(side(step), swapped(through, step), through, past)
+            grant = 66000000 if step < 4 else 4 * 2**20
+            past, through = scan_step(side(step), swapped(through, step), through, past, grant)
         return past, through
 
     past, through = scanned((1,), past, through)

time: 184 us -> 183 us (level)
  waiting for transfers between devices: 48.8 us -> 56.9 us
  Pallas kernels: 37.5 us -> 33.3 us
  local copies, waits for them, and re-layouts: 8.22 us -> 4.34 us
    all_to_all x6, waiting for transfers between devices: 44 us -> 52.1 us  [spread(): return lax.all_to_all(array, axis, 0, 0, tiled=True)]
    unnamed x34 -> x20, local copies, waits for them, and re-layouts: 4.55 us -> 0.65 us
    pallas_call x4, Pallas kernels: 7.35 us -> 4.33 us  [scan_step(): pl.pallas_call(step_kernel, out_shape=(jax.ShapeDtypeStruct(past.shape, j...]
  transfers between devices with their start and end apart: 11 -> 11, of which waited for: 9 -> 9; matrix products, arithmetic and copies ran while one was open for 4% -> 2% of each run, Pallas kernels for 19% -> 17%
where the time goes in v7:
time: 183 us; the launch traced here: 182 us
  starting transfers between devices  83.3 us (46%)
  waiting for transfers between devices  56.9 us (31%)
  Pallas kernels  33.3 us (18%)
  local copies, waits for them, and re-layouts  4.34 us (2%)
  other arithmetic  2.56 us (1%)
    all_to_all x6, starting transfers between devices, spread(): return lax.all_to_all(array, axis, 0, 0, tiled=True)  56.3 us
    all_to_all x6, waiting for transfers between devices, spread(): return lax.all_to_all(array, axis, 0, 0, tiled=True)  52.1 us
    ppermute x5, starting transfers between devices, swapped(): lax.ppermute(through, 'ep', [(i, i ^ distance) for i in range(count)])  27 us
    pallas_call x1, Pallas kernels, local_half(): pl.pallas_call(local_kernel, out_shape=(full(jnp.float32), jax.ShapeDtype...  15.4 us
    pallas_call x2, Pallas kernels, expert_rows(): pl.pallas_call(expert_kernel, grid=(total // tile,), in_specs=[block, fix...  9.88 us
    ppermute x5, waiting for transfers between devices, swapped(): lax.ppermute(through, 'ep', [(i, i ^ distance) for i in range(count)])  4.81 us
    pallas_call x4, Pallas kernels, scan_step(): pl.pallas_call(step_kernel, out_shape=(jax.ShapeDtypeStruct(past.shape, j...  4.33 us
  transfers between devices with their start and end apart: 11, of which 9 were waited for; matrix products, arithmetic and copies ran while one was open for 2% of the time, Pallas kernels for 17%

profile of v7, /device:TPU:1, one launch (start us, length us, event | category | flops | bytes accessed | tf_op | source)
XLA Modules:
  0.0 182.2 jit_solution(14338018733351302842)
XLA Ops:
  0.6 2.6 %route_rows.1 = (bf16[768,128]{1,0:T(8,128)(2,1)}, bf16[768,256]{1,0:T(8,128)(2,1)}) custom-call(s32[1]{0:T(128)} %bitcast.1.at_ref, bf16[256,2048]{1,0:T(8,128)(2,1)} %rows_ref.1, f32[1,2048]{1,0:T(1,128)} %bitcast.32, s32[2,256]{1,0:T(2,128)} %bitcast.33, f32[2,256]{1,0:T(2,128)} %bitcast.34), custom_call_target="tpu_custom_call" | custom-call | flops 100663296 | bytes 1048576 | tf_op jit(solution)/shard_map/route_rows/pallas_call | solution.py:336
  3.2 16.7 %all-to-all-start = ((bf16[32,24,128]{2,1,0:T(8,128)(2,1)}), bf16[32,24,128]{2,1,0:T(8,128)(2,1)S(1)}, u32[]{:S(2)}, u32[]{:S(2)}) async-start(bf16[32,24,128]{2,1,0:T(8,128)(2,1)} %bitcast.31), calls=%async_computation | async-start | bytes 393216 | tf_op jit(solution)/shard_map/all_to_all | solution.py:356
  20.0 15.4 %mixer_local.1 = (f32[64,1024]{1,0:T(8,128)}, bf16[128,1024]{1,0:T(8,128)(2,1)}, bf16[2,64,128]{2,1,0:T(8,128)(2,1)}) custom-call(bf16[64,1024]{1,0:T(8,128)(2,1)} %q_ref.1, bf16[64,1024]{1,0:T(8,128)(2,1)} %k_ref.1, bf16[64,1024]{1,0:T(8,128)(2,1)} %v_ref.1, bf16[64,1024]{1,0:T(8,128)(2,1)} %e_ref.1, bf16[64,1024]{1,0:T(8,128)(2,1)} %d_ref.1), custom_call_target="tpu_custom_call" | custom-call | flops 1476395008 | bytes 1179648 | tf_op jit(solution)/shard_map/mixer_local/pallas_call | solution.py:155
  35.3 3.4 %all-to-all-done = bf16[32,24,128]{2,1,0:T(8,128)(2,1)S(1)} async-done(((bf16[32,24,128]{2,1,0:T(8,128)(2,1)}), bf16[32,24,128]{2,1,0:T(8,128)(2,1)S(1)}, u32[]{:S(2)}, u32[]{:S(2)}) %all-to-all-start) | async-done | bytes 196640 | tf_op jit(solution)/shard_map/all_to_all | solution.py:356
  38.8 1.5 broadcast_in_dim.22
  40.2 0.0 copy-start.5
  40.2 6.9 %all-to-all-start.1 = ((bf16[16,384,128]{2,1,0:T(8,128)(2,1)}), bf16[16,384,128]{2,1,0:T(8,128)(2,1)}, u32[]{:S(2)}, u32[]{:S(2)}) async-start(bf16[16,384,128]{2,1,0:T(8,128)(2,1)} %broadcast_in_dim.22), calls=%async_computation.1 | async-start | bytes 3145728 | tf_op jit(solution)/shard_map/all_to_all | solution.py:356
  47.2 0.0 copy-done.5
  47.2 3.6 %collective-permute-start = (bf16[2,64,128]{2,1,0:T(8,128)(2,1)S(1)}, bf16[2,64,128]{2,1,0:T(8,128)(2,1)S(1)}, u32[]{:S(2)}, u32[]{:S(2)}) collective-permute-start(bf16[2,64,128]{2,1,0:T(8,128)(2,1)S(1)} %copy-done.5), channel_id=1, source_target_pairs={{0,16},{16,0},{32,48},{48,32},{64,80},{80,64},{96,112},{112,96},{1... | collective-permute-start | bytes 98312 | tf_op jit(solution)/shard_map/ppermute | solution.py:265
  50.8 0.8 collective-permute-done.arrived_ref
  51.7 0.0 copy-start.7
  51.7 0.6 broadcast_in_dim.24.past_ref
  52.3 0.0 copy-done.7
  52.3 1.8 %scan_step.4 = (f32[2,64,128]{2,1,0:T(8,128)}, bf16[2,64,128]{2,1,0:T(8,128)(2,1)}) custom-call(s32[1]{0:T(128)} %bitcast.7.upper_ref, bf16[2,64,128]{2,1,0:T(8,128)(2,1)} %copy-done.7, bf16[2,64,128]{2,1,0:T(8,128)(2,1)} %get-tuple-element.42.through_ref, f32[2,64,128]{2,1,0:T(8,128)} %broadcast_in_dim.24.past_ref), custom_call_target="tpu_custom_call" | custom-call | flops 12582912 | bytes 196608 | tf_op jit(solution)/shard_map/scan_step/pallas_call | solution.py:216
  54.2 0.0 copy-start.6
  54.2 1.5 broadcast_in_dim.23
  55.6 0.0 copy-done.6
  55.6 1.9 %collective-permute-start.1 = (bf16[2,64,128]{2,1,0:T(8,128)(2,1)S(1)}, bf16[2,64,128]{2,1,0:T(8,128)(2,1)S(1)}, u32[]{:S(2)}, u32[]{:S(2)}) collective-permute-start(bf16[2,64,128]{2,1,0:T(8,128)(2,1)S(1)} %copy-done.6), channel_id=1, source_target_pairs={{0,32},{16,48},{32,0},{48,16},{64,96},{80,112},{96,64},{112,80},{1... | collective-permute-start | bytes 98312 | tf_op jit(solution)/shard_map/ppermute | solution.py:265
  57.6 3.1 %collective-permute-done.1.arrived_ref = bf16[2,64,128]{2,1,0:T(8,128)(2,1)S(1)} collective-permute-done((bf16[2,64,128]{2,1,0:T(8,128)(2,1)S(1)}, bf16[2,64,128]{2,1,0:T(8,128)(2,1)S(1)}, u32[]{:S(2)}, u32[]{:S(2)}) %collective-permute-start.1) | collective-permute-done | bytes 32800 | tf_op jit(solution)/shard_map/ppermute | solution.py:265
  60.7 0.0 copy-start.8
  60.7 0.6 copy-done.8
  61.3 1.8 %scan_step.5 = (f32[2,64,128]{2,1,0:T(8,128)}, bf16[2,64,128]{2,1,0:T(8,128)(2,1)}) custom-call(s32[1]{0:T(128)} %bitcast.8.upper_ref, bf16[2,64,128]{2,1,0:T(8,128)(2,1)} %copy-done.8, bf16[2,64,128]{2,1,0:T(8,128)(2,1)} %get-tuple-element.46.through_ref, f32[2,64,128]{2,1,0:T(8,128)} %get-tuple-element.47.past_ref), custom_call_target="tpu_custom_call" | custom-call | flops 12582912 | bytes 196608 | tf_op jit(solution)/shard_map/scan_step/pallas_call | solution.py:216
  63.1 5.0 %all-to-all-done.1.rows_ref = bf16[16,384,128]{2,1,0:T(8,128)(2,1)} async-done(((bf16[16,384,128]{2,1,0:T(8,128)(2,1)}), bf16[16,384,128]{2,1,0:T(8,128)(2,1)}, u32[]{:S(2)}, u32[]{:S(2)}) %all-to-all-start.1) | async-done | bytes 1572896 | tf_op jit(solution)/shard_map/all_to_all | solution.py:356
  68.1 0.0 copy-start.3
  68.1 6.4 %all-to-all-start.2 = ((bf16[16,384,128]{2,1,0:T(8,128)(2,1)}), bf16[16,384,128]{2,1,0:T(8,128)(2,1)}, u32[]{:S(2)}, u32[]{:S(2)}) async-start(bf16[16,384,128]{2,1,0:T(8,128)(2,1)} %broadcast_in_dim.23), calls=%async_computation.2 | async-start | bytes 3145728 | tf_op jit(solution)/shard_map/all_to_all | solution.py:356
  74.5 0.0 copy-done.3
  74.5 5.2 %collective-permute-start.2 = (bf16[2,64,128]{2,1,0:T(8,128)(2,1)S(1)}, bf16[2,64,128]{2,1,0:T(8,128)(2,1)S(1)}, u32[]{:S(2)}, u32[]{:S(2)}) collective-permute-start(bf16[2,64,128]{2,1,0:T(8,128)(2,1)S(1)} %copy-done.3), channel_id=1, source_target_pairs={{0,64},{16,80},{32,96},{48,112},{64,0},{80,16},{96,32},{112,48},{1... | collective-permute-start | bytes 98312 | tf_op jit(solution)/shard_map/ppermute | solution.py:265
  79.7 0.0 copy-start.2
  79.7 4.9 %expert_rows.2 = bf16[16,384,128]{2,1,0:T(8,128)(2,1)} custom-call(bf16[16,384,128]{2,1,0:T(8,128)(2,1)} %all-to-all-done.1.rows_ref, bf16[224,2048]{1,0:T(8,128)(2,1)} %bitcast.23, bf16[224,2048]{1,0:T(8,128)(2,1)} %bitcast.25, bf16[224,2048]{1,0:T(8,128)(2,1)} %bitcast.27), custom_call_target="tpu_custom_call" | custom-call | flops 1056964608 | bytes 5898240 | tf_op jit(solution)/shard_map/expert_rows/pallas_call | solution.py:288
  84.6 0.0 collective-permute-done.2.arrived_ref
  84.6 0.0 copy-done.2
  84.6 0.3 scan_step.6
  85.0 10.2 %all-to-all-done.2.rows_ref = bf16[16,384,128]{2,1,0:T(8,128)(2,1)} async-done(((bf16[16,384,128]{2,1,0:T(8,128)(2,1)}), bf16[16,384,128]{2,1,0:T(8,128)(2,1)}, u32[]{:S(2)}, u32[]{:S(2)}) %all-to-all-start.2) | async-done | bytes 1572896 | tf_op jit(solution)/shard_map/all_to_all | solution.py:356
  95.2 5.7 %all-to-all-start.3 = ((bf16[16,384,128]{2,1,0:T(8,128)(2,1)}), bf16[16,384,128]{2,1,0:T(8,128)(2,1)}, u32[]{:S(2)}, u32[]{:S(2)}) async-start(bf16[16,384,128]{2,1,0:T(8,128)(2,1)} %expert_rows.2), calls=%async_computation.3 | async-start | bytes 3145728 | tf_op jit(solution)/shard_map/all_to_all | solution.py:356
  100.9 5.5 %collective-permute-start.3 = (bf16[2,64,128]{2,1,0:T(8,128)(2,1)S(1)}, bf16[2,64,128]{2,1,0:T(8,128)(2,1)S(1)}, u32[]{:S(2)}, u32[]{:S(2)}) collective-permute-start(bf16[2,64,128]{2,1,0:T(8,128)(2,1)S(1)} %get-tuple-element.58.through_ref), channel_id=1, source_target_pairs={{0,128},{16,144},{32,160},{48,176},{64,192},{80,208},{96,224},{112... | collective-permute-start | bytes 98312 | tf_op jit(solution)/shard_map/ppermute | solution.py:265
  106.4 4.9 %expert_rows.3 = bf16[16,384,128]{2,1,0:T(8,128)(2,1)} custom-call(bf16[16,384,128]{2,1,0:T(8,128)(2,1)} %all-to-all-done.2.rows_ref, bf16[224,2048]{1,0:T(8,128)(2,1)} %bitcast.24, bf16[224,2048]{1,0:T(8,128)(2,1)} %bitcast.26, bf16[224,2048]{1,0:T(8,128)(2,1)} %bitcast.28), custom_call_target="tpu_custom_call" | custom-call | flops 1056964608 | bytes 5898240 | tf_op jit(solution)/shard_map/expert_rows/pallas_call | solution.py:288
  111.4 0.0 collective-permute-done.3.arrived_ref
  111.4 0.3 scan_step.7
  111.7 9.4 %all-to-all-done.3 = bf16[16,384,128]{2,1,0:T(8,128)(2,1)} async-done(((bf16[16,384,128]{2,1,0:T(8,128)(2,1)}), bf16[16,384,128]{2,1,0:T(8,128)(2,1)}, u32[]{:S(2)}, u32[]{:S(2)}) %all-to-all-start.3) | async-done | bytes 1572896 | tf_op jit(solution)/shard_map/all_to_all | solution.py:356
  121.0 5.4 %all-to-all-start.4 = ((bf16[16,384,128]{2,1,0:T(8,128)(2,1)}), bf16[16,384,128]{2,1,0:T(8,128)(2,1)S(1)}, u32[]{:S(2)}, u32[]{:S(2)}) async-start(bf16[16,384,128]{2,1,0:T(8,128)(2,1)} %expert_rows.3), calls=%async_computation.4 | async-start | bytes 3145728 | tf_op jit(solution)/shard_map/all_to_all | solution.py:356
  126.5 10.8 %collective-permute-start.4 = (bf16[2,64,128]{2,1,0:T(8,128)(2,1)S(1)}, bf16[2,64,128]{2,1,0:T(8,128)(2,1)S(1)}, u32[]{:S(2)}, u32[]{:S(2)}) collective-permute-start(bf16[2,64,128]{2,1,0:T(8,128)(2,1)S(1)} %get-tuple-element.64), channel_id=1, source_target_pairs={{0,256},{16,272},{32,288},{48,304},{64,320},{80,336},{96,352},{112... | collective-permute-start | bytes 98312 | tf_op jit(solution)/shard_map/ppermute | solution.py:265
  137.3 1.6 reduce_sum.24
  138.9 0.0 copy-start.9
  139.0 0.0 copy-start
  139.0 0.0 copy-start.1
  139.0 0.0 copy-start.4
  139.0 0.8 collective-permute-done.4.arrived_ref
  139.8 6.6 %all-to-all-done.4 = bf16[16,384,128]{2,1,0:T(8,128)(2,1)S(1)} async-done(((bf16[16,384,128]{2,1,0:T(8,128)(2,1)}), bf16[16,384,128]{2,1,0:T(8,128)(2,1)S(1)}, u32[]{:S(2)}, u32[]{:S(2)}) %all-to-all-start.4) | async-done | bytes 1572896 | tf_op jit(solution)/shard_map/all_to_all | solution.py:356
  146.4 0.2 reduce_sum.25
  146.7 0.7 pad_maximum_fusion
  147.4 15.1 %all-to-all-start.5 = ((bf16[32,24,128]{2,1,0:T(8,128)(2,1)}), bf16[32,24,128]{2,1,0:T(8,128)(2,1)S(1)}, u32[]{:S(2)}, u32[]{:S(2)}) async-start(bf16[32,24,128]{2,1,0:T(8,128)(2,1)} %bitcast.19), calls=%async_computation.5 | async-start | bytes 393216 | tf_op jit(solution)/shard_map/all_to_all | solution.py:356
  162.5 0.0 copy-done.9
  162.5 0.1 copy.15.gain_ref
  162.6 0.0 copy-done
  162.6 0.0 copy-done.1
  162.6 1.2 mixer_finish.1
  163.8 17.5 %all-to-all-done.5 = bf16[32,24,128]{2,1,0:T(8,128)(2,1)S(1)} async-done(((bf16[32,24,128]{2,1,0:T(8,128)(2,1)}), bf16[32,24,128]{2,1,0:T(8,128)(2,1)S(1)}, u32[]{:S(2)}, u32[]{:S(2)}) %all-to-all-start.5) | async-done | bytes 196640 | tf_op jit(solution)/shard_map/all_to_all | solution.py:356
  181.3 0.0 copy-done.4
  181.3 0.9 convolution_convert_fusion
  (1 shorter events, 0.0 us)
Async XLA Ops:
  3.2 35.5 %all-to-all-start = ((bf16[32,24,128]{2,1,0:T(8,128)(2,1)}), bf16[32,24,128]{2,1,0:T(8,128)(2,1)S(1)}, u32[]{:S(2)}, u32[]{:S(2)}) async-start(bf16[32,24,128]{2,1,0:T(8,128)(2,1)} %bitcast.31), calls=%async_computation | async-start | bytes 393216 | tf_op jit(solution)/shard_map/all_to_all | solution.py:356
  40.2 6.9 %copy-start.5 = (bf16[2,64,128]{2,1,0:T(8,128)(2,1)S(1)}, bf16[2,64,128]{2,1,0:T(8,128)(2,1)}, u32[]{:S(2)}) copy-start(bf16[2,64,128]{2,1,0:T(8,128)(2,1)} %get-tuple-element.42.through_ref) | copy-start | bytes 98308
  40.2 27.9 %all-to-all-start.1 = ((bf16[16,384,128]{2,1,0:T(8,128)(2,1)}), bf16[16,384,128]{2,1,0:T(8,128)(2,1)}, u32[]{:S(2)}, u32[]{:S(2)}) async-start(bf16[16,384,128]{2,1,0:T(8,128)(2,1)} %broadcast_in_dim.22), calls=%async_computation.1 | async-start | bytes 3145728 | tf_op jit(solution)/shard_map/all_to_all | solution.py:356
  47.2 4.5 %collective-permute-start = (bf16[2,64,128]{2,1,0:T(8,128)(2,1)S(1)}, bf16[2,64,128]{2,1,0:T(8,128)(2,1)S(1)}, u32[]{:S(2)}, u32[]{:S(2)}) collective-permute-start(bf16[2,64,128]{2,1,0:T(8,128)(2,1)S(1)} %copy-done.5), channel_id=1, source_target_pairs={{0,16},{16,0},{32,48},{48,32},{64,80},{80,64},{96,112},{112,96},{1... | collective-permute-start | bytes 98312 | tf_op jit(solution)/shard_map/ppermute | solution.py:265
  51.7 0.6 copy-start.7
  54.2 1.5 copy-start.6
  55.6 5.0 %collective-permute-start.1 = (bf16[2,64,128]{2,1,0:T(8,128)(2,1)S(1)}, bf16[2,64,128]{2,1,0:T(8,128)(2,1)S(1)}, u32[]{:S(2)}, u32[]{:S(2)}) collective-permute-start(bf16[2,64,128]{2,1,0:T(8,128)(2,1)S(1)} %copy-done.6), channel_id=1, source_target_pairs={{0,32},{16,48},{32,0},{48,16},{64,96},{80,112},{96,64},{112,80},{1... | collective-permute-start | bytes 98312 | tf_op jit(solution)/shard_map/ppermute | solution.py:265
  60.7 0.6 copy-start.8
  68.1 6.4 %copy-start.3 = (bf16[2,64,128]{2,1,0:T(8,128)(2,1)S(1)}, bf16[2,64,128]{2,1,0:T(8,128)(2,1)}, u32[]{:S(2)}) copy-start(bf16[2,64,128]{2,1,0:T(8,128)(2,1)} %get-tuple-element.52.through_ref) | copy-start | bytes 98308
  68.1 27.0 %all-to-all-start.2 = ((bf16[16,384,128]{2,1,0:T(8,128)(2,1)}), bf16[16,384,128]{2,1,0:T(8,128)(2,1)}, u32[]{:S(2)}, u32[]{:S(2)}) async-start(bf16[16,384,128]{2,1,0:T(8,128)(2,1)} %broadcast_in_dim.23), calls=%async_computation.2 | async-start | bytes 3145728 | tf_op jit(solution)/shard_map/all_to_all | solution.py:356
  74.5 10.1 %collective-permute-start.2 = (bf16[2,64,128]{2,1,0:T(8,128)(2,1)S(1)}, bf16[2,64,128]{2,1,0:T(8,128)(2,1)S(1)}, u32[]{:S(2)}, u32[]{:S(2)}) collective-permute-start(bf16[2,64,128]{2,1,0:T(8,128)(2,1)S(1)} %copy-done.3), channel_id=1, source_target_pairs={{0,64},{16,80},{32,96},{48,112},{64,0},{80,16},{96,32},{112,48},{1... | collective-permute-start | bytes 98312 | tf_op jit(solution)/shard_map/ppermute | solution.py:265
  79.7 5.0 %copy-start.2 = (f32[2,64,128]{2,1,0:T(8,128)S(1)}, f32[2,64,128]{2,1,0:T(8,128)}, u32[]{:S(2)}) copy-start(f32[2,64,128]{2,1,0:T(8,128)} %get-tuple-element.53.past_ref) | copy-start | bytes 196612
  95.2 25.9 %all-to-all-start.3 = ((bf16[16,384,128]{2,1,0:T(8,128)(2,1)}), bf16[16,384,128]{2,1,0:T(8,128)(2,1)}, u32[]{:S(2)}, u32[]{:S(2)}) async-start(bf16[16,384,128]{2,1,0:T(8,128)(2,1)} %expert_rows.2), calls=%async_computation.3 | async-start | bytes 3145728 | tf_op jit(solution)/shard_map/all_to_all | solution.py:356
  100.9 10.4 %collective-permute-start.3 = (bf16[2,64,128]{2,1,0:T(8,128)(2,1)S(1)}, bf16[2,64,128]{2,1,0:T(8,128)(2,1)S(1)}, u32[]{:S(2)}, u32[]{:S(2)}) collective-permute-start(bf16[2,64,128]{2,1,0:T(8,128)(2,1)S(1)} %get-tuple-element.58.through_ref), channel_id=1, source_target_pairs={{0,128},{16,144},{32,160},{48,176},{64,192},{80,208},{96,224},{112... | collective-permute-start | bytes 98312 | tf_op jit(solution)/shard_map/ppermute | solution.py:265
  121.0 25.4 %all-to-all-start.4 = ((bf16[16,384,128]{2,1,0:T(8,128)(2,1)}), bf16[16,384,128]{2,1,0:T(8,128)(2,1)S(1)}, u32[]{:S(2)}, u32[]{:S(2)}) async-start(bf16[16,384,128]{2,1,0:T(8,128)(2,1)} %expert_rows.3), calls=%async_computation.4 | async-start | bytes 3145728 | tf_op jit(solution)/shard_map/all_to_all | solution.py:356
  126.5 13.4 %collective-permute-start.4 = (bf16[2,64,128]{2,1,0:T(8,128)(2,1)S(1)}, bf16[2,64,128]{2,1,0:T(8,128)(2,1)S(1)}, u32[]{:S(2)}, u32[]{:S(2)}) collective-permute-start(bf16[2,64,128]{2,1,0:T(8,128)(2,1)S(1)} %get-tuple-element.64), channel_id=1, source_target_pairs={{0,256},{16,272},{32,288},{48,304},{64,320},{80,336},{96,352},{112... | collective-permute-start | bytes 98312 | tf_op jit(solution)/shard_map/ppermute | solution.py:265
  138.9 23.6 %copy-start.9 = (f32[64]{0:T(128)S(1)}, f32[64]{0:T(128)}, u32[]{:S(2)}) copy-start(f32[64]{0:T(128)} %param.18) | copy-start | bytes 772
  139.0 23.7 %copy-start = (f32[64,1024]{1,0:T(8,128)S(1)}, f32[64,1024]{1,0:T(8,128)}, u32[]{:S(2)}) copy-start(f32[64,1024]{1,0:T(8,128)} %get-tuple-element.67.oloc_ref) | copy-start | bytes 786436
  139.0 23.7 %copy-start.1 = (bf16[128,1024]{1,0:T(8,128)(2,1)S(1)}, bf16[128,1024]{1,0:T(8,128)(2,1)}, u32[]{:S(2)}) copy-start(bf16[128,1024]{1,0:T(8,128)(2,1)} %get-tuple-element.68.qp_ref) | copy-start | bytes 786436
  139.0 42.3 %copy-start.4 = (bf16[768,256]{1,0:T(8,128)(2,1)S(1)}, bf16[768,256]{1,0:T(8,128)(2,1)}, u32[]{:S(2)}) copy-start(bf16[768,256]{1,0:T(8,128)(2,1)} %get-tuple-element.69) | copy-start | bytes 1179652
  147.4 33.9 %all-to-all-start.5 = ((bf16[32,24,128]{2,1,0:T(8,128)(2,1)}), bf16[32,24,128]{2,1,0:T(8,128)(2,1)S(1)}, u32[]{:S(2)}, u32[]{:S(2)}) async-start(bf16[32,24,128]{2,1,0:T(8,128)(2,1)} %bitcast.19), calls=%async_computation.5 | async-start | bytes 393216 | tf_op jit(solution)/shard_map/all_to_all | solution.py:356

commit v8 on v6

--- a/solution.py
+++ b/solution.py
@@ -224,7 +224,7 @@
         cost_estimate=pl.CostEstimate(
             flops=6 * 128**3, bytes_accessed=6 * 2 * past.size, transcendentals=0
         ),
-        compiler_params=pltpu.CompilerParams(vmem_limit_bytes=66000000),
+        compiler_params=pltpu.CompilerParams(vmem_limit_bytes=4 * 2**20),
         name="scan_step",
     )(upper, arrived, through, past)
 
@@ -282,7 +282,7 @@
 
 def expert_rows(rows, gate, up, down):
     parts, total, lanes = rows.shape
-    tile = 128 if total % 128 == 0 else total
+    tile = 256 if total % 256 == 0 else total
     block = pl.BlockSpec((parts, tile, lanes), lambda i: (0, i, 0))
     fixed = lambda array: pl.BlockSpec(array.shape, lambda i: (0, 0))
     return pl.pallas_call(
@@ -348,8 +348,32 @@
     )(at, rows, gain, routes, weight)
 
 
+def sum_kernel(pieces_ref, out_ref):
+    parts, total, _ = pieces_ref.shape
+    tile = 64 if total % 64 == 0 else total
+
+    def body(step, carry):
+        at = pl.ds(pl.multiple_of(step * tile, tile), tile)
+        whole = pieces_ref[0, at, :].astype(jnp.float32)
+        for j in range(1, parts):
+            whole += pieces_ref[j, at, :].astype(jnp.float32)
+        out_ref[at, :] = whole.astype(jnp.bfloat16)
+        return carry
+
+    lax.fori_loop(0, total // tile, body, 0)
+
+
 def summed_pieces(pieces):
-    return jnp.sum(pieces.astype(jnp.float32), axis=0).astype(jnp.bfloat16)
+    return pl.pallas_call(
+        sum_kernel,
+        out_shape=jax.ShapeDtypeStruct(pieces.shape[1:], jnp.bfloat16),
+        in_specs=in_vmem(1, 0),
+        cost_estimate=pl.CostEstimate(
+            flops=pieces.size, bytes_accessed=2 * pieces.size, transcendentals=0
+        ),
+        compiler_params=pltpu.CompilerParams(vmem_limit_bytes=4 * 2**20),
+        name="sum_pieces",
+    )(pieces)
 
 
 def spread(array, axis):
@@ -391,40 +415,27 @@
     )
     oloc, qp, own_maps = local_half(query_in, key_in, value_in, erase_pre, decay_pre)
     arrived, own_maps = lax.optimization_barrier((arrived, own_maps))
-    middle = slot_total // 2
-    copies = [
-        jnp.broadcast_to(part[None], (shares, *part.shape))
-        for part in (arrived[:middle], arrived[middle:])
-    ]
+    copies = jnp.broadcast_to(arrived[None], (shares, *arrived.shape))
     copies, own_maps = lax.optimization_barrier((copies, own_maps))
-    shared_a = spread(copies[0], "tp")
+    shared = spread(copies, "tp")
+    past, through = jnp.zeros(own_maps.shape, jnp.float32), own_maps
     weights = [gate_weight[0].T, up_weight[0].T, down_weight[0]]
-    shared_a, copies, own_maps = lax.optimization_barrier((shared_a, copies, own_maps))
-    past, through = jnp.zeros(own_maps.shape, jnp.float32), own_maps
 
     def scanned(steps, past, through):
         for step in steps:
             past, through = scan_step(side(step), swapped(through, step), through, past)
         return past, through
 
-    shared_b = spread(copies[1], "tp")
-    partial_a = expert_rows(shared_a, *weights)
-    past, through = scanned((1, 2), past, through)
-    shared_b, partial_a, past, through = lax.optimization_barrier(
-        (shared_b, partial_a, past, through)
-    )
-    pieces_a = spread(partial_a, "tp")
-    partial_b = expert_rows(shared_b, *weights)
-    past, through = scanned((4, 8), past, through)
-    pieces_a, partial_b, past, through = lax.optimization_barrier(
-        (pieces_a, partial_b, past, through)
-    )
-    pieces_b = spread(partial_b, "tp")
-    summed_a = summed_pieces(pieces_a)
+    past, through = scanned((1, 2, 4), past, through)
+    shared, past, through = lax.optimization_barrier((shared, past, through))
+    partial = expert_rows(shared, *weights)
+    partial, past, through = lax.optimization_barrier((partial, past, through))
+    pieces = spread(partial, "tp")
+    past, through = scanned((8,), past, through)
     distance = experts_n // 2
     crossing = swapped(through, distance)
-    pieces_b, summed_a, crossing = lax.optimization_barrier((pieces_b, summed_a, crossing))
-    summed = jnp.concatenate([summed_a, summed_pieces(pieces_b)], axis=0)
+    pieces, crossing = lax.optimization_barrier((pieces, crossing))
+    summed = summed_pieces(pieces)
     returned = spread(summed.reshape(experts_n, capacity, col_count), "ep").reshape(
         slot_total, col_count
     )

time: 184 us -> 185 us (level)
  waiting for transfers between devices: 34.3 us -> 73.2 us
  blocking collectives: 28 us -> 0 us
  Pallas kernels: 38.6 us -> 28.4 us
  other arithmetic: 2.56 us -> 0 us
    all_to_all x5 -> x4, waiting for transfers between devices: 29.1 us -> 62.5 us  [spread(): return lax.all_to_all(array, axis, 0, 0, tiled=True)]
    all_to_all x1 -> x0, blocking collectives: 28 us -> none  [spread(): return lax.all_to_all(array, axis, 0, 0, tiled=True)]
    pallas_call x4, Pallas kernels: 7.35 us -> 1.29 us  [scan_step(): pl.pallas_call(step_kernel, out_shape=(jax.ShapeDtypeStruct(past.shape, j...]
    ppermute x5, waiting for transfers between devices: 5.2 us -> 10.7 us  [swapped(): lax.ppermute(through, 'ep', [(i, i ^ distance) for i in range(count)])]
    pallas_call x2 -> x1, Pallas kernels: 12.1 us -> 6.91 us  [expert_rows(): pl.pallas_call(expert_kernel, grid=(total // tile,), in_specs=[block, fix...]
    ppermute x5, starting transfers between devices: 24.8 us -> 28.4 us  [swapped(): lax.ppermute(through, 'ep', [(i, i ^ distance) for i in range(count)])]
    all_to_all x5 -> x4, starting transfers between devices: 48 us -> 45.7 us  [spread(): return lax.all_to_all(array, axis, 0, 0, tiled=True)]
  transfers between devices with their start and end apart: 10 -> 9, of which waited for: 7 -> 9; matrix products, arithmetic and copies ran while one was open for 1% -> 0% of each run, Pallas kernels for 20% -> 10%
where the time goes in v8:
time: 185 us; the launch traced here: 184 us
  starting transfers between devices  74.1 us (40%)
  waiting for transfers between devices  73.2 us (40%)
  Pallas kernels  28.4 us (15%)
  local copies, waits for them, and re-layouts  5.43 us (3%)
  matrix products  1.93 us (1%)
    all_to_all x4, waiting for transfers between devices, spread(): return lax.all_to_all(array, axis, 0, 0, tiled=True)  62.5 us
    all_to_all x4, starting transfers between devices, spread(): return lax.all_to_all(array, axis, 0, 0, tiled=True)  45.7 us
    ppermute x5, starting transfers between devices, swapped(): lax.ppermute(through, 'ep', [(i, i ^ distance) for i in range(count)])  28.4 us
    pallas_call x1, Pallas kernels, local_half(): pl.pallas_call(local_kernel, out_shape=(full(jnp.float32), jax.ShapeDtype...  15.3 us
    ppermute x5, waiting for transfers between devices, swapped(): lax.ppermute(through, 'ep', [(i, i ^ distance) for i in range(count)])  10.7 us
    pallas_call x1, Pallas kernels, expert_rows(): pl.pallas_call(expert_kernel, grid=(total // tile,), in_specs=[block, fix...  6.91 us
  transfers between devices with their start and end apart: 9, of which 9 were waited for; matrix products, arithmetic and copies ran while one was open for 0% of the time, Pallas kernels for 10%

profile of v8, /device:TPU:1, one launch (start us, length us, event | category | flops | bytes accessed | tf_op | source)
XLA Modules:
  0.0 183.9 jit_solution(12463554179886461333)
XLA Ops:
  0.6 2.6 %route_rows.1 = (bf16[768,128]{1,0:T(8,128)(2,1)}, bf16[768,256]{1,0:T(8,128)(2,1)}) custom-call(s32[1]{0:T(128)} %bitcast.1.at_ref, bf16[256,2048]{1,0:T(8,128)(2,1)} %rows_ref.1, f32[1,2048]{1,0:T(1,128)} %bitcast.29, s32[2,256]{1,0:T(2,128)} %bitcast.30, f32[2,256]{1,0:T(2,128)} %bitcast.31), custom_call_target="tpu_custom_call" | custom-call | flops 100663296 | bytes 1048576 | tf_op jit(solution)/shard_map/route_rows/pallas_call | solution.py:336
  3.2 16.7 %all-to-all-start = ((bf16[32,24,128]{2,1,0:T(8,128)(2,1)}), bf16[32,24,128]{2,1,0:T(8,128)(2,1)S(1)}, u32[]{:S(2)}, u32[]{:S(2)}) async-start(bf16[32,24,128]{2,1,0:T(8,128)(2,1)} %bitcast.28), calls=%async_computation | async-start | bytes 393216 | tf_op jit(solution)/shard_map/all_to_all | solution.py:380
  20.0 15.3 %mixer_local.1 = (f32[64,1024]{1,0:T(8,128)}, bf16[128,1024]{1,0:T(8,128)(2,1)}, bf16[2,64,128]{2,1,0:T(8,128)(2,1)}) custom-call(bf16[64,1024]{1,0:T(8,128)(2,1)} %q_ref.1, bf16[64,1024]{1,0:T(8,128)(2,1)} %k_ref.1, bf16[64,1024]{1,0:T(8,128)(2,1)} %v_ref.1, bf16[64,1024]{1,0:T(8,128)(2,1)} %e_ref.1, bf16[64,1024]{1,0:T(8,128)(2,1)} %d_ref.1), custom_call_target="tpu_custom_call" | custom-call | flops 1476395008 | bytes 1179648 | tf_op jit(solution)/shard_map/mixer_local/pallas_call | solution.py:155
  35.3 3.5 %all-to-all-done = bf16[32,24,128]{2,1,0:T(8,128)(2,1)S(1)} async-done(((bf16[32,24,128]{2,1,0:T(8,128)(2,1)}), bf16[32,24,128]{2,1,0:T(8,128)(2,1)S(1)}, u32[]{:S(2)}, u32[]{:S(2)}) %all-to-all-start) | async-done | bytes 196640 | tf_op jit(solution)/shard_map/all_to_all | solution.py:380
  38.7 2.2 %broadcast_in_dim.16 = bf16[16,768,128]{2,1,0:T(8,128)(2,1)} broadcast(bf16[768,128]{1,0:T(8,128)(2,1)S(1)} %bitcast.26), dimensions={1,2} | broadcast | bytes 3342336 | tf_op jit(solution)/shard_map/broadcast_in_dim | solution.py:418
  41.0 0.0 copy-start.2
  41.0 6.9 %all-to-all-start.1 = ((bf16[16,768,128]{2,1,0:T(8,128)(2,1)}), bf16[16,768,128]{2,1,0:T(8,128)(2,1)}, u32[]{:S(2)}, u32[]{:S(2)}) async-start(bf16[16,768,128]{2,1,0:T(8,128)(2,1)} %broadcast_in_dim.16), calls=%async_computation.1 | async-start | bytes 6291456 | tf_op jit(solution)/shard_map/all_to_all | solution.py:380
  47.9 0.0 copy-done.2
  47.9 3.6 %collective-permute-start = (bf16[2,64,128]{2,1,0:T(8,128)(2,1)S(1)}, bf16[2,64,128]{2,1,0:T(8,128)(2,1)S(1)}, u32[]{:S(2)}, u32[]{:S(2)}) collective-permute-start(bf16[2,64,128]{2,1,0:T(8,128)(2,1)S(1)} %copy-done.2), channel_id=1, source_target_pairs={{0,16},{16,0},{32,48},{48,32},{64,80},{80,64},{96,112},{112,96},{1... | collective-permute-start | bytes 98312 | tf_op jit(solution)/shard_map/ppermute | solution.py:265
  51.6 0.8 collective-permute-done.arrived_ref
  52.4 0.3 scan_step.4
  52.7 1.9 %collective-permute-start.1 = (bf16[2,64,128]{2,1,0:T(8,128)(2,1)S(1)}, bf16[2,64,128]{2,1,0:T(8,128)(2,1)S(1)}, u32[]{:S(2)}, u32[]{:S(2)}) collective-permute-start(bf16[2,64,128]{2,1,0:T(8,128)(2,1)S(1)} %get-tuple-element.33.through_ref), channel_id=1, source_target_pairs={{0,32},{16,48},{32,0},{48,16},{64,96},{80,112},{96,64},{112,80},{1... | collective-permute-start | bytes 98312 | tf_op jit(solution)/shard_map/ppermute | solution.py:265
  54.7 3.1 %collective-permute-done.1.arrived_ref = bf16[2,64,128]{2,1,0:T(8,128)(2,1)S(1)} collective-permute-done((bf16[2,64,128]{2,1,0:T(8,128)(2,1)S(1)}, bf16[2,64,128]{2,1,0:T(8,128)(2,1)S(1)}, u32[]{:S(2)}, u32[]{:S(2)}) %collective-permute-start.1) | collective-permute-done | bytes 32800 | tf_op jit(solution)/shard_map/ppermute | solution.py:265
  57.8 0.3 scan_step.5
  58.1 1.9 %collective-permute-start.2 = (bf16[2,64,128]{2,1,0:T(8,128)(2,1)S(1)}, bf16[2,64,128]{2,1,0:T(8,128)(2,1)S(1)}, u32[]{:S(2)}, u32[]{:S(2)}) collective-permute-start(bf16[2,64,128]{2,1,0:T(8,128)(2,1)S(1)} %get-tuple-element.35.through_ref), channel_id=1, source_target_pairs={{0,64},{16,80},{32,96},{48,112},{64,0},{80,16},{96,32},{112,48},{1... | collective-permute-start | bytes 98312 | tf_op jit(solution)/shard_map/ppermute | solution.py:265
  60.1 4.1 %collective-permute-done.2.arrived_ref = bf16[2,64,128]{2,1,0:T(8,128)(2,1)S(1)} collective-permute-done((bf16[2,64,128]{2,1,0:T(8,128)(2,1)S(1)}, bf16[2,64,128]{2,1,0:T(8,128)(2,1)S(1)}, u32[]{:S(2)}, u32[]{:S(2)}) %collective-permute-start.2) | collective-permute-done | bytes 32800 | tf_op jit(solution)/shard_map/ppermute | solution.py:265
  64.2 0.3 scan_step.6
  64.5 0.0 copy-start.3
  64.5 27.7 %all-to-all-done.1.rows_ref = bf16[16,768,128]{2,1,0:T(8,128)(2,1)} async-done(((bf16[16,768,128]{2,1,0:T(8,128)(2,1)}), bf16[16,768,128]{2,1,0:T(8,128)(2,1)}, u32[]{:S(2)}, u32[]{:S(2)}) %all-to-all-start.1) | async-done | bytes 3145760 | tf_op jit(solution)/shard_map/all_to_all | solution.py:380
  92.3 6.9 %expert_rows.1 = bf16[16,768,128]{2,1,0:T(8,128)(2,1)} custom-call(bf16[16,768,128]{2,1,0:T(8,128)(2,1)} %all-to-all-done.1.rows_ref, bf16[224,2048]{1,0:T(8,128)(2,1)} %bitcast.23, bf16[224,2048]{1,0:T(8,128)(2,1)} %bitcast.24, bf16[224,2048]{1,0:T(8,128)(2,1)} %bitcast.25), custom_call_target="tpu_custom_call" | custom-call | flops 2113929216 | bytes 9043968 | tf_op jit(solution)/shard_map/expert_rows/pallas_call | solution.py:288
  99.2 0.0 copy-start.7
  99.2 3.9 %all-to-all-start.2 = ((bf16[16,768,128]{2,1,0:T(8,128)(2,1)}), bf16[16,768,128]{2,1,0:T(8,128)(2,1)S(1)}, u32[]{:S(2)}, u32[]{:S(2)}) async-start(bf16[16,768,128]{2,1,0:T(8,128)(2,1)} %expert_rows.1), calls=%async_computation.2 | async-start | bytes 6291456 | tf_op jit(solution)/shard_map/all_to_all | solution.py:380
  103.1 0.0 copy-done.3
  103.1 0.0 copy-start
  103.1 7.5 %collective-permute-start.3 = (bf16[2,64,128]{2,1,0:T(8,128)(2,1)S(1)}, bf16[2,64,128]{2,1,0:T(8,128)(2,1)S(1)}, u32[]{:S(2)}, u32[]{:S(2)}) collective-permute-start(bf16[2,64,128]{2,1,0:T(8,128)(2,1)S(1)} %get-tuple-element.43.through_ref), channel_id=1, source_target_pairs={{0,128},{16,144},{32,160},{48,176},{64,192},{80,208},{96,224},{112... | collective-permute-start | bytes 98312 | tf_op jit(solution)/shard_map/ppermute | solution.py:265
  110.6 1.3 collective-permute-done.3.arrived_ref
  111.9 0.0 copy-start.5
  111.9 0.6 copy-done.5
  112.5 0.0 copy-start.4
  112.5 0.8 copy-done.4
  113.2 0.0 copy-start.6
  113.2 0.8 copy-done.6
  114.0 0.3 scan_step.7
  114.3 13.4 %collective-permute-start.4 = (bf16[2,64,128]{2,1,0:T(8,128)(2,1)S(1)}, bf16[2,64,128]{2,1,0:T(8,128)(2,1)S(1)}, u32[]{:S(2)}, u32[]{:S(2)}) collective-permute-start(bf16[2,64,128]{2,1,0:T(8,128)(2,1)S(1)} %get-tuple-element.45), channel_id=1, source_target_pairs={{0,256},{16,272},{32,288},{48,304},{64,320},{80,336},{96,352},{112... | collective-permute-start | bytes 98312 | tf_op jit(solution)/shard_map/ppermute | solution.py:265
  127.8 1.4 collective-permute-done.4.arrived_ref
  129.2 14.7 %all-to-all-done.2.pieces_ref = bf16[16,768,128]{2,1,0:T(8,128)(2,1)S(1)} async-done(((bf16[16,768,128]{2,1,0:T(8,128)(2,1)}), bf16[16,768,128]{2,1,0:T(8,128)(2,1)S(1)}, u32[]{:S(2)}, u32[]{:S(2)}) %all-to-all-start.2) | async-done | bytes 3145760 | tf_op jit(solution)/shard_map/all_to_all | solution.py:380
  143.9 1.2 sum_pieces.1
  145.1 18.2 %all-to-all-start.3 = ((bf16[32,24,128]{2,1,0:T(8,128)(2,1)}), bf16[32,24,128]{2,1,0:T(8,128)(2,1)S(1)}, u32[]{:S(2)}, u32[]{:S(2)}) async-start(bf16[32,24,128]{2,1,0:T(8,128)(2,1)} %bitcast.17), calls=%async_computation.3 | async-start | bytes 393216 | tf_op jit(solution)/shard_map/all_to_all | solution.py:380
  163.2 0.0 copy-done.7
  163.2 0.1 copy.15.gain_ref
  163.3 0.0 copy-done
  163.3 0.0 copy-start.1
  163.3 0.9 copy-done.1
  164.3 1.2 mixer_finish.1
  165.4 16.6 %all-to-all-done.3 = bf16[32,24,128]{2,1,0:T(8,128)(2,1)S(1)} async-done(((bf16[32,24,128]{2,1,0:T(8,128)(2,1)}), bf16[32,24,128]{2,1,0:T(8,128)(2,1)S(1)}, u32[]{:S(2)}, u32[]{:S(2)}) %all-to-all-start.3) | async-done | bytes 196640 | tf_op jit(solution)/shard_map/all_to_all | solution.py:380
  182.0 1.9 %convolution_convert_fusion = bf16[256,128]{1,0:T(8,128)(2,1)} fusion(bf16[768,256]{1,0:T(8,128)(2,1)} %get-tuple-element.50, bf16[768,128]{1,0:T(8,128)(2,1)S(1)} %bitcast.27), kind=kOutput, calls=%fused_computation | convolution fusion | flops 50364416 | bytes 655360 | tf_op jit(solution)/shard_map/dot_general | solution.py:24
  (1 shorter events, 0.0 us)
Async XLA Ops:
  3.2 35.5 %all-to-all-start = ((bf16[32,24,128]{2,1,0:T(8,128)(2,1)}), bf16[32,24,128]{2,1,0:T(8,128)(2,1)S(1)}, u32[]{:S(2)}, u32[]{:S(2)}) async-start(bf16[32,24,128]{2,1,0:T(8,128)(2,1)} %bitcast.28), calls=%async_computation | async-start | bytes 393216 | tf_op jit(solution)/shard_map/all_to_all | solution.py:380
  41.0 6.9 %copy-start.2 = (bf16[2,64,128]{2,1,0:T(8,128)(2,1)S(1)}, bf16[2,64,128]{2,1,0:T(8,128)(2,1)}, u32[]{:S(2)}) copy-start(bf16[2,64,128]{2,1,0:T(8,128)(2,1)} %get-tuple-element.32.through_ref) | copy-start | bytes 98308
  41.0 51.3 %all-to-all-start.1 = ((bf16[16,768,128]{2,1,0:T(8,128)(2,1)}), bf16[16,768,128]{2,1,0:T(8,128)(2,1)}, u32[]{:S(2)}, u32[]{:S(2)}) async-start(bf16[16,768,128]{2,1,0:T(8,128)(2,1)} %broadcast_in_dim.16), calls=%async_computation.1 | async-start | bytes 6291456 | tf_op jit(solution)/shard_map/all_to_all | solution.py:380
  47.9 4.5 %collective-permute-start = (bf16[2,64,128]{2,1,0:T(8,128)(2,1)S(1)}, bf16[2,64,128]{2,1,0:T(8,128)(2,1)S(1)}, u32[]{:S(2)}, u32[]{:S(2)}) collective-permute-start(bf16[2,64,128]{2,1,0:T(8,128)(2,1)S(1)} %copy-done.2), channel_id=1, source_target_pairs={{0,16},{16,0},{32,48},{48,32},{64,80},{80,64},{96,112},{112,96},{1... | collective-permute-start | bytes 98312 | tf_op jit(solution)/shard_map/ppermute | solution.py:265
  52.7 5.1 %collective-permute-start.1 = (bf16[2,64,128]{2,1,0:T(8,128)(2,1)S(1)}, bf16[2,64,128]{2,1,0:T(8,128)(2,1)S(1)}, u32[]{:S(2)}, u32[]{:S(2)}) collective-permute-start(bf16[2,64,128]{2,1,0:T(8,128)(2,1)S(1)} %get-tuple-element.33.through_ref), channel_id=1, source_target_pairs={{0,32},{16,48},{32,0},{48,16},{64,96},{80,112},{96,64},{112,80},{1... | collective-permute-start | bytes 98312 | tf_op jit(solution)/shard_map/ppermute | solution.py:265
  58.1 6.0 %collective-permute-start.2 = (bf16[2,64,128]{2,1,0:T(8,128)(2,1)S(1)}, bf16[2,64,128]{2,1,0:T(8,128)(2,1)S(1)}, u32[]{:S(2)}, u32[]{:S(2)}) collective-permute-start(bf16[2,64,128]{2,1,0:T(8,128)(2,1)S(1)} %get-tuple-element.35.through_ref), channel_id=1, source_target_pairs={{0,64},{16,80},{32,96},{48,112},{64,0},{80,16},{96,32},{112,48},{1... | collective-permute-start | bytes 98312 | tf_op jit(solution)/shard_map/ppermute | solution.py:265
  64.5 38.5 %copy-start.3 = (bf16[2,64,128]{2,1,0:T(8,128)(2,1)}, bf16[2,64,128]{2,1,0:T(8,128)(2,1)S(1)}, u32[]{:S(2)}) copy-start(bf16[2,64,128]{2,1,0:T(8,128)(2,1)S(1)} %get-tuple-element.43.through_ref) | copy-start | bytes 98308
  99.2 64.1 %copy-start.7 = (f32[64]{0:T(128)S(1)}, f32[64]{0:T(128)}, u32[]{:S(2)}) copy-start(f32[64]{0:T(128)} %param.18) | copy-start | bytes 772
  99.2 44.7 %all-to-all-start.2 = ((bf16[16,768,128]{2,1,0:T(8,128)(2,1)}), bf16[16,768,128]{2,1,0:T(8,128)(2,1)S(1)}, u32[]{:S(2)}, u32[]{:S(2)}) async-start(bf16[16,768,128]{2,1,0:T(8,128)(2,1)} %expert_rows.1), calls=%async_computation.2 | async-start | bytes 6291456 | tf_op jit(solution)/shard_map/all_to_all | solution.py:380
  103.1 60.3 %copy-start = (f32[64,1024]{1,0:T(8,128)S(1)}, f32[64,1024]{1,0:T(8,128)}, u32[]{:S(2)}) copy-start(f32[64,1024]{1,0:T(8,128)} %get-tuple-element.48.oloc_ref) | copy-start | bytes 786436
  103.1 8.8 %collective-permute-start.3 = (bf16[2,64,128]{2,1,0:T(8,128)(2,1)S(1)}, bf16[2,64,128]{2,1,0:T(8,128)(2,1)S(1)}, u32[]{:S(2)}, u32[]{:S(2)}) collective-permute-start(bf16[2,64,128]{2,1,0:T(8,128)(2,1)S(1)} %get-tuple-element.43.through_ref), channel_id=1, source_target_pairs={{0,128},{16,144},{32,160},{48,176},{64,192},{80,208},{96,224},{112... | collective-permute-start | bytes 98312 | tf_op jit(solution)/shard_map/ppermute | solution.py:265
  111.9 0.6 copy-start.5
  112.5 0.8 copy-start.4
  113.2 0.8 copy-start.6
  114.3 14.8 %collective-permute-start.4 = (bf16[2,64,128]{2,1,0:T(8,128)(2,1)S(1)}, bf16[2,64,128]{2,1,0:T(8,128)(2,1)S(1)}, u32[]{:S(2)}, u32[]{:S(2)}) collective-permute-start(bf16[2,64,128]{2,1,0:T(8,128)(2,1)S(1)} %get-tuple-element.45), channel_id=1, source_target_pairs={{0,256},{16,272},{32,288},{48,304},{64,320},{80,336},{96,352},{112... | collective-permute-start | bytes 98312 | tf_op jit(solution)/shard_map/ppermute | solution.py:265
  145.1 37.0 %all-to-all-start.3 = ((bf16[32,24,128]{2,1,0:T(8,128)(2,1)}), bf16[32,24,128]{2,1,0:T(8,128)(2,1)S(1)}, u32[]{:S(2)}, u32[]{:S(2)}) async-start(bf16[32,24,128]{2,1,0:T(8,128)(2,1)} %bitcast.17), calls=%async_computation.3 | async-start | bytes 393216 | tf_op jit(solution)/shard_map/all_to_all | solution.py:380
  163.3 1.0 copy-start.1
